TPU v7x, 512 devices: a whole 4x4x16 slice. The times are simulated.
512 devices in a mesh: ep: 32 (over z, core), tp: 16 (over y, x).
Axes of the slice: x: 4, y: 4, z: 16, core: 2. Of those that a mesh axis runs over, the one named last changes fastest.
Arguments:
- queries: bfloat16 [8192, 2048], P('ep', 'tp'), may hold values from -6 to 6
- key_rows: bfloat16 [8192, 1024], P('ep', 'tp'), may hold values from -6 to 6
- values: bfloat16 [8192, 1024], P('ep', 'tp'), may hold values from -140 to 140
- query_gain: float32 [64], replicated, may hold values from 0.55 to 7.5
- key_gain: float32 [64], replicated, may hold values from 0.55 to 7.5
- mix_gain: float32 [2048], replicated, may hold values from 0.1 to 1.9
- out_weight: bfloat16 [2048, 4096], P(None, 'tp'), may hold values from -0.125 to 0.125
- expert_input: bfloat16 [8192, 4096], P('ep', 'tp'), may hold values from -140 to 140
- expert_gain: float32 [4096], replicated, may hold values from 0.1 to 1.9
- route_ids: int32 [8192, 2], P('ep'), may hold values from 0 to 31, as said below
- route_weights: float32 [8192, 2], P('ep'), may hold values from 0.3 to 1.7
- expert_gate: bfloat16 [32, 4096, 2048], P('ep', None, 'tp'), may hold values from -0.09375 to 0.09375
- expert_up: bfloat16 [32, 4096, 2048], P('ep', None, 'tp'), may hold values from -0.09375 to 0.09375
- expert_down: bfloat16 [32, 2048, 4096], P('ep', None, 'tp'), may hold values from -0.125 to 0.125
Outputs:
- attended: bfloat16 [8192, 4096], P('ep', 'tp')
- expert_mix: bfloat16 [8192, 4096], P('ep', 'tp')
Inputs may be any that keep to these rules, and one draw needn't show every extreme that they name: `route_ids`: the 2 experts of a row differ. In every aligned block of 256 rows no expert is named more than 22 times, and one expert, the same for all blocks, is named exactly 22 times in every block.
All inputs are finite; a program needn't handle non-finite values.
Results may differ from a plain program's by a relative error of at most 0.01.
The roundings to bfloat16 on the way count: a program that leaves them out, or rounds other values in their place, can miss the bound.
Values may be sent and summed in bfloat16 or wider, within the bound.
No kernel may reach another device: no remote copies, remote signals or barrier semaphores. Data moves between devices by JAX's collectives and lax.ppermute only.
A program may use at most 64 MiB of HBM per device.

v0:
```python
import math

import jax
import jax.numpy as jnp
from jax import lax
from jax.sharding import Mesh
from jax.sharding import PartitionSpec as P

Q_HEADS = 32
KV_HEADS = 16
HEAD = 64
GRID_W = 64
EP = ("ep_0", "ep_1")


EPS = 1e-06
THETA = 10000.0


def in_one_piece(arrays, axis, dim, along):
    widths = [a.shape[along] for a in arrays]
    both = jnp.concatenate(arrays, axis=along)
    filled = lax.all_gather(both, axis, axis=dim, tiled=True)
    return tuple(jnp.split(filled, [sum(widths[:k]) for k in range(1, len(widths))], axis=along))


def split_up(array, dim, length):
    before, after = (array.shape[:dim], array.shape[dim + 1 :])
    return jnp.moveaxis(array.reshape(*before, length, -1, *after), dim, 0)


def joined_along(blocks, dim):
    lengths = list(blocks.shape[1:])
    lengths[dim] *= blocks.shape[0]
    return jnp.moveaxis(blocks, 0, dim).reshape(lengths)


def exchange_in_order(blocks, axes, order):
    inside = blocks.shape[1:]
    filled = blocks.reshape(*(lax.axis_size(a) for a in axes), *inside)
    for k in order:
        filled = lax.all_to_all(filled, axes[k], k, k, tiled=True)
    return filled.reshape(-1, *inside)


def exchange_by_chip(array, groups, order, split_dim, concat_dim):
    length = lax.axis_size(groups[0]) * lax.axis_size(groups[1])
    blocks = split_up(array, split_dim, length)
    return joined_along(exchange_in_order(blocks, groups, order), concat_dim)


def turn_tables(offset, length):
    half_width = HEAD // 2
    inverse = THETA ** (-jnp.arange(0, half_width, 2, dtype=jnp.float32) / half_width)
    positions = offset + jnp.arange(length, dtype=jnp.int32)
    grid_rows = (positions // GRID_W).astype(jnp.float32)
    grid_cols = (positions % GRID_W).astype(jnp.float32)
    angles = jnp.concatenate([grid_rows[:, None] * inverse, grid_cols[:, None] * inverse], axis=-1)
    return (jnp.cos(angles), jnp.sin(angles))


def norm_turn(source, scale_gain, cosine_table, sine_table):
    length = source.shape[0]
    head_rows = source.astype(jnp.float32).reshape(length, -1, HEAD)
    head_rows = (
        head_rows
        * lax.rsqrt(jnp.mean(head_rows * head_rows, axis=-1, keepdims=True) + EPS)
        * scale_gain
    )
    pair_view = head_rows.reshape(length, head_rows.shape[1], HEAD // 2, 2)
    even_part = pair_view[..., 0]
    odd_part = pair_view[..., 1]
    cosine_part = cosine_table[:, None, :]
    sine_part = sine_table[:, None, :]
    turned = jnp.stack(
        [
            even_part * cosine_part - odd_part * sine_part,
            even_part * sine_part + odd_part * cosine_part,
        ],
        axis=-1,
    )
    return turned.reshape(length, -1).astype(jnp.bfloat16)


def shards(
    queries,
    key_rows,
    values,
    query_gain,
    key_gain,
    mix_gain,
    out_weight,
    expert_input,
    expert_gain,
    route_ids,
    route_weights,
    expert_gate,
    expert_up,
    expert_down,
):
    length = queries.shape[0]
    experts_count = lax.axis_size(EP)
    offset = lax.axis_index(EP) * length
    cosine_table, sine_table = turn_tables(offset, length)
    query_turned = norm_turn(queries, query_gain, cosine_table, sine_table)
    key_turned = norm_turn(key_rows, key_gain, cosine_table, sine_table)
    kv_local = key_rows.shape[1] // HEAD
    group_size = Q_HEADS // KV_HEADS
    query_heads = query_turned.reshape(length, kv_local, group_size, HEAD)
    start_state = (
        jnp.full((kv_local, group_size, length), -jnp.inf, jnp.float32),
        jnp.zeros((kv_local, group_size, length), jnp.float32),
        jnp.zeros((length, kv_local, group_size, HEAD), jnp.float32),
    )
    key_piece, value_piece = in_one_piece((key_turned, values), EP, 0, 1)
    piece_rows = key_piece.shape[0]
    step_rows = 1024
    key_blocks = key_piece.reshape(piece_rows // step_rows, step_rows, kv_local, HEAD)
    value_blocks = value_piece.reshape(piece_rows // step_rows, step_rows, kv_local, HEAD)

    def absorb(current, block_pair):
        running_max, running_sum, running_acc = current
        key_block, value_block = block_pair
        scores = jnp.einsum(
            "rhgd,nhd->hgrn", query_heads, key_block, preferred_element_type=jnp.float32
        ) / math.sqrt(HEAD)
        new_max = jnp.maximum(running_max, jnp.max(scores, axis=-1))
        factor = jnp.exp(running_max - new_max)
        raw_weights = jnp.exp(scores - new_max[..., None])
        new_sum = running_sum * factor + jnp.sum(raw_weights, axis=-1)
        rounded = raw_weights.astype(jnp.bfloat16)
        increment = jnp.einsum(
            "hgrn,nhd->rhgd", rounded, value_block, preferred_element_type=jnp.float32
        )
        new_acc = running_acc * jnp.transpose(factor, (2, 0, 1))[..., None] + increment
        return ((new_max, new_sum, new_acc), None)

    result, unused = lax.scan(absorb, start_state, (key_blocks, value_blocks))
    heads_out = (
        (result[2] / jnp.transpose(result[1], (2, 0, 1))[..., None])
        .reshape(length, -1)
        .astype(jnp.bfloat16)
    )
    top_count = route_ids.shape[1]
    copies = route_ids.shape[0] * top_count
    capacity = (4 * copies + 3 * experts_count - 1) // (3 * experts_count)
    slot_total = experts_count * capacity
    flat_ids = route_ids.reshape(copies)
    hit_marks = (flat_ids[:, None] == jnp.arange(experts_count, dtype=jnp.int32)[None, :]).astype(
        jnp.int32
    )
    earlier = jnp.cumsum(hit_marks, axis=0) - hit_marks
    places = jnp.sum(earlier * hit_marks, axis=1)
    slot_index = flat_ids * capacity + places
    slot_rows = (
        jnp.full((slot_total,), route_ids.shape[0], jnp.int32)
        .at[slot_index]
        .set(jnp.arange(copies, dtype=jnp.int32) // top_count)
    )
    width_local = expert_input.shape[1]
    padded = jnp.concatenate([expert_input, jnp.zeros((1, width_local), jnp.bfloat16)], axis=0)
    outgoing = padded[slot_rows].reshape(experts_count, capacity, width_local)
    arrived = exchange_by_chip(outgoing, ("ep_0", "ep_1"), (1, 0), 0, 0).reshape(
        slot_total, width_local
    )
    piece_float = lax.all_gather(arrived, "tp", axis=1, tiled=True).astype(jnp.float32)
    gain_piece = expert_gain
    scaled_piece = (piece_float * gain_piece).astype(jnp.bfloat16)
    gate_rows = expert_gate[0]
    up_rows = expert_up[0]
    gate_sum = jnp.dot(scaled_piece, gate_rows, preferred_element_type=jnp.float32)
    up_sum = jnp.dot(scaled_piece, up_rows, preferred_element_type=jnp.float32)
    square_sum = jnp.sum(piece_float * piece_float, axis=1)
    row_stat = lax.rsqrt(square_sum / expert_gain.shape[0] + EPS)
    gate_value = gate_sum * row_stat[:, None]
    up_value = up_sum * row_stat[:, None]
    hidden = (jax.nn.silu(gate_value) * up_value).astype(jnp.bfloat16)
    width_out = out_weight.shape[1]
    head_piece, hidden_piece = in_one_piece((heads_out, hidden), "tp", 1, 0)
    head_float = head_piece.astype(jnp.float32)
    gain_piece = mix_gain
    mix_in = (head_float * gain_piece).astype(jnp.bfloat16)
    down_rows = expert_down[0]
    mix_sum = jnp.dot(mix_in, out_weight, preferred_element_type=jnp.float32)
    mix_squares = jnp.sum(head_float * head_float, axis=1)
    expert_sum = jnp.dot(hidden_piece, down_rows, preferred_element_type=jnp.float32)
    attended = (mix_sum * lax.rsqrt(mix_squares / mix_gain.shape[0] + EPS)[:, None]).astype(
        jnp.bfloat16
    )
    expert_back = expert_sum.astype(jnp.bfloat16).reshape(experts_count, capacity, width_out)
    returned = lax.all_to_all(expert_back, EP, split_axis=0, concat_axis=0, tiled=True).reshape(
        slot_total, width_out
    )
    picked = returned[slot_index].astype(jnp.float32) * route_weights.reshape(copies)[:, None]
    expert_mix = jnp.sum(picked.reshape(route_ids.shape[0], top_count, width_out), axis=1).astype(
        jnp.bfloat16
    )
    return (attended, expert_mix)


def solution(mesh):
    torus = Mesh(mesh.devices.reshape(16, 2, mesh.shape["tp"]), ("ep_0", "ep_1", "tp"))
    return jax.shard_map(
        shards,
        mesh=torus,
        in_specs=(
            P(EP, "tp"),
            P(EP, "tp"),
            P(EP, "tp"),
            P(),
            P(),
            P(),
            P(None, "tp"),
            P(EP, "tp"),
            P(),
            P(EP, None),
            P(EP, None),
            P(EP, None, "tp"),
            P(EP, None, "tp"),
            P(EP, None, "tp"),
        ),
        out_specs=(P(EP, "tp"), P(EP, "tp")),
        check_vma=False,
    )
```

profile of v0, /device:TPU:1, one launch (start us, length us, event | category | flops | bytes accessed | tf_op | source)
XLA Modules:
  0.0 310.1 jit_solution(1185379400146651329)
XLA Ops:
  7.2 0.9 fusion.50
  8.1 0.8 fusion.51
  9.4 1.4 pad_maximum_fusion.1
  10.8 0.8 copy.42
  11.9 0.7 broadcast_multiply_fusion.2
  12.9 1.2 reduce-window.6
  14.1 0.2 slice_reduce_fusion
  14.3 0.9 concatenate.47
  15.4 2.4 scatter_custom_fusion
  17.9 2.8 gather_fusion
  20.9 10.5 %all_to_all.15 = bf16[16,2,1,22,256]{4,0,3,2,1:T(8,128)(2,1)S(1)} all-to-all(bf16[16,2,1,22,256]{4,0,3,2,1:T(8,128)(2,1)S(1)} %copy.45), channel_id=1, replica_groups=mesh['ep_0'=16,'ep_1'=2,'tp'=16] {'ep_1'}, dimensions={1} | all-to-all | bytes 720896 | tf_op jit(solution)/shard_map/all_to_all | solution.py:42
  31.4 1.1 copy.46
  32.5 9.6 %all-to-all-start.1 = ((bf16[16,2,1,22,256]{4,1,3,2,0:T(2,128)(2,1)}), bf16[16,2,1,22,256]{4,1,3,2,0:T(2,128)(2,1)S(1)}, u32[]{:S(2)}, u32[]{:S(2)}) async-start(bf16[16,2,1,22,256]{4,1,3,2,0:T(2,128)(2,1)} %copy.46), calls=%async_computation.1 | async-start | bytes 720896 | tf_op jit(solution)/shard_map/all_to_all | solution.py:42
  42.8 0.2 subtract_convert_fusion
  43.2 20.0 %all-to-all-done.1 = bf16[16,2,1,22,256]{4,1,3,2,0:T(2,128)(2,1)S(1)} async-done(((bf16[16,2,1,22,256]{4,1,3,2,0:T(2,128)(2,1)}), bf16[16,2,1,22,256]{4,1,3,2,0:T(2,128)(2,1)S(1)}, u32[]{:S(2)}, u32[]{:S(2)}) %all-to-all-start.1) | async-done | bytes 360480 | tf_op jit(solution)/shard_map/all_to_all | solution.py:42
  63.2 0.8 reshape_reshape_reshape.7
  64.0 0.2 all-gather.8.cloned.1.call-start
  64.3 35.3 %all-gather.4.cloned.1.call-done = bf16[8192,128]{0,1:T(8,128)(2,1)} async-done(((bf16[256,128]{0,1:T(8,128)(2,1)}), bf16[8192,128]{0,1:T(8,128)(2,1)}) %all-gather.4.cloned.1.call-update) | async-done | bytes 2097168 | tf_op jit(solution)/shard_map/all_gather | solution.py:23
  99.5 1.7 fusion.70
  101.2 0.6 copy.54
  101.8 1.6 copy.39
  103.4 0.6 copy.55
  104.0 1.5 copy.40
  105.5 25.7 %while.15 = (s32[]{:T(128)}, f32[1,2,256]{2,1,0:T(2,128)S(1)}, f32[1,2,256]{2,1,0:T(2,128)S(1)}, f32[256,1,2,64]{0,3,2,1:T(8,128)S(1)}, bf16[8,1024,1,64]{1,3,2,...) while((s32[]{:T(128)}, f32[1,2,256]{2,1,0:T(2,128)S(1)}, ...), condition=%wide.region_5.6_spmd.clone, body=%wide.region_2.5_spmd.clone.sunk | while | flops 138513408 | bytes 6914169 | solution.py:138
  105.5 1.4 bitcast_reduce_fusion.3
  106.9 0.4 fusion.81
  107.3 1.4 fusion.82
  108.7 1.4 bitcast_reduce_fusion.3
  110.1 0.4 fusion.81
  110.5 1.4 fusion.82
  111.9 1.4 bitcast_reduce_fusion.3
  113.4 0.4 fusion.81
  113.7 1.4 fusion.82
  115.2 1.4 bitcast_reduce_fusion.3
  116.6 0.4 fusion.81
  117.0 1.4 fusion.82
  118.4 1.4 bitcast_reduce_fusion.3
  119.8 0.4 fusion.81
  120.2 1.4 fusion.82
  121.6 1.4 bitcast_reduce_fusion.3
  123.0 0.4 fusion.81
  123.4 1.4 fusion.82
  124.8 1.4 bitcast_reduce_fusion.3
  126.2 0.4 fusion.81
  126.6 1.4 fusion.82
  128.0 1.4 bitcast_reduce_fusion.3
  129.4 0.4 fusion.81
  129.8 1.4 fusion.82
  131.4 42.5 %all-gather.6.cloned.1.call-done = bf16[704,4096]{1,0:T(8,128)(2,1)} async-done(((bf16[704,256]{1,0:T(8,128)(2,1)}), bf16[704,4096]{1,0:T(8,128)(2,1)}) %all-gather.6.cloned.1.call-update) | async-done | bytes 5767184 | tf_op jit(solution)/shard_map/all_gather | solution.py:166
  173.9 4.0 %fusion.19 = f32[704]{0:T(1024)S(1)} fusion(bf16[704,4096]{1,0:T(8,128)(2,1)} %all-gather.6.cloned.1.call-done), kind=kLoop, calls=%fused_computation.32 | loop fusion | flops 8650048 | bytes 5769984 | tf_op jit(solution)/shard_map/reduce_sum | solution.py:173
  177.9 0.3 copy-done.1
  178.2 3.0 fusion.31
  181.2 1.7 fusion.40
  182.9 0.7 pad_maximum_fusion
  183.7 70.5 %all-gather.8.cloned.1.call-done = bf16[960,2048]{1,0:T(8,128)(2,1)} async-done(((bf16[960,128]{1,0:T(8,128)(2,1)}), bf16[960,2048]{1,0:T(8,128)(2,1)}) %all-gather.8.cloned.1.call-update) | async-done | bytes 3932176 | tf_op jit(solution)/shard_map/all_gather | solution.py:23
  254.2 2.7 fusion.28
  256.9 0.8 reshape.435
  257.8 14.4 %all-to-all-start.2 = ((bf16[32,22,256]{2,1,0:T(8,128)(2,1)}), bf16[32,22,256]{2,1,0:T(8,128)(2,1)S(1)}, u32[]{:S(2)}, u32[]{:S(2)}) async-start(bf16[32,22,256]{2,1,0:T(8,128)(2,1)} %reshape.435), calls=%async_computation.2 | async-start | bytes 786432 | tf_op jit(solution)/shard_map/all_to_all | solution.py:191
  272.3 1.5 fusion.27
  273.8 2.3 fusion.43
  276.2 23.7 %all-to-all-done.2 = bf16[32,22,256]{2,1,0:T(8,128)(2,1)S(1)} async-done(((bf16[32,22,256]{2,1,0:T(8,128)(2,1)}), bf16[32,22,256]{2,1,0:T(8,128)(2,1)S(1)}, u32[]{:S(2)}, u32[]{:S(2)}) %all-to-all-start.2) | async-done | bytes 360480 | tf_op jit(solution)/shard_map/all_to_all | solution.py:191
  300.0 2.0 gather_fusion.1
  301.9 0.3 reshape.437
  302.2 1.4 multiply_reduce_fusion
  (90 shorter events, 3.0 us)
Async XLA Ops:
  7.2 247.0 %copy-start = (bf16[1,2048,256]{2,1,0:T(8,128)(2,1)S(1)}, bf16[1,2048,256]{2,1,0:T(8,128)(2,1)}, u32[]{:S(2)}) copy-start(bf16[1,2048,256]{2,1,0:T(8,128)(2,1)} %param.29) | copy-start | bytes 3145732
  7.2 92.3 %all-gather.4.cloned.1.call-start = ((), (), s32[]{:S(2)}) async-start(), calls=%async_computation.3 | async-start | bytes 2162688 | tf_op jit(solution)/shard_map/all_gather | solution.py:23
  17.9 24.3 %copy-start.2 = (bf16[256,128]{1,0:T(8,128)(2,1)S(1)}, bf16[256,128]{1,0:T(8,128)(2,1)}, u32[]{:S(2)}) copy-start(bf16[256,128]{1,0:T(8,128)(2,1)} %param.16) | copy-start | bytes 196612
  17.9 24.5 %copy-start.4 = (f32[64]{0:T(128)S(1)}, f32[64]{0:T(128)}, u32[]{:S(2)}) copy-start(f32[64]{0:T(128)} %param.19) | copy-start | bytes 772
  32.5 30.6 %all-to-all-start.1 = ((bf16[16,2,1,22,256]{4,1,3,2,0:T(2,128)(2,1)}), bf16[16,2,1,22,256]{4,1,3,2,0:T(2,128)(2,1)S(1)}, u32[]{:S(2)}, u32[]{:S(2)}) async-start(bf16[16,2,1,22,256]{4,1,3,2,0:T(2,128)(2,1)} %copy.46), calls=%async_computation.1 | async-start | bytes 720896 | tf_op jit(solution)/shard_map/all_to_all | solution.py:42
  42.1 131.8 %all-gather.6.cloned.1.call-start = ((), (), s32[]{:S(2)}) async-start(), calls=%async_computation.4 | async-start | bytes 6127616 | tf_op jit(solution)/shard_map/all_gather | solution.py:166
  64.0 190.1 %all-gather.8.cloned.1.call-start = ((), (), s32[]{:S(2)}) async-start(), calls=%async_computation.5 | async-start | bytes 4177920 | tf_op jit(solution)/shard_map/all_gather | solution.py:23
  131.2 46.7 %copy-start.7 = (f32[4096]{0:T(1024)S(1)}, f32[4096]{0:T(1024)}, u32[]{:S(2)}) copy-start(f32[4096]{0:T(1024)} %param.24) | copy-start | bytes 49156
  173.9 4.3 %copy-start.1 = (bf16[704,4096]{1,0:T(8,128)(2,1)S(1)}, bf16[704,4096]{1,0:T(8,128)(2,1)}, u32[]{:S(2)}) copy-start(bf16[704,4096]{1,0:T(8,128)(2,1)} %all-gather.6.cloned.1.call-done) | copy-start | bytes 17301508
  178.2 3.0 copy-start.5
  183.7 88.5 %copy-start.3 = (f32[256,2]{0,1:T(2,128)S(1)}, f32[256,2]{0,1:T(2,128)}, u32[]{:S(2)}) copy-start(f32[256,2]{0,1:T(2,128)} %param.26) | copy-start | bytes 6148
  183.7 90.1 %copy-start.6 = (bf16[2048,256]{1,0:T(8,128)(2,1)S(1)}, bf16[2048,256]{1,0:T(8,128)(2,1)}, u32[]{:S(2)}) copy-start(bf16[2048,256]{1,0:T(8,128)(2,1)} %param.22) | copy-start | bytes 3145732
  183.7 90.1 %copy-start.8 = (f32[2048]{0:T(1024)S(1)}, f32[2048]{0:T(1024)}, u32[]{:S(2)}) copy-start(f32[2048]{0:T(1024)} %param.21) | copy-start | bytes 24580
  257.8 42.1 %all-to-all-start.2 = ((bf16[32,22,256]{2,1,0:T(8,128)(2,1)}), bf16[32,22,256]{2,1,0:T(8,128)(2,1)S(1)}, u32[]{:S(2)}, u32[]{:S(2)}) async-start(bf16[32,22,256]{2,1,0:T(8,128)(2,1)} %reshape.435), calls=%async_computation.2 | async-start | bytes 786432 | tf_op jit(solution)/shard_map/all_to_all | solution.py:191
Sparse Core Ops, SparseCore 0:
  10.9 88.5 all-gather.3
  102.5 71.3 all-gather.5
  183.8 70.3 all-gather.7
where the time goes:
time: 311 us; the launch traced here: 310 us
  waiting for transfers between devices  192 us (62%)
  matrix products  31.9 us (10%)
  starting transfers between devices  24.3 us (8%)
  local copies, waits for them, and re-layouts  20.2 us (6%)
  other arithmetic  16.7 us (5%)
  between operations  14.2 us (5%)
  blocking collectives  10.5 us (3%)
    all_gather x2, waiting for transfers between devices, in_one_piece(): filled = lax.all_gather(both, axis, axis=dim, tiled=True)  106 us
    all_gather x1, waiting for transfers between devices, shards(): lax.all_gather(arrived, 'tp', axis=1, tiled=True).astype(jnp.float32)  42.5 us
    all_to_all x1, waiting for transfers between devices, shards(): lax.all_to_all(expert_back, EP, split_axis=0, concat_axis=0, tiled=True)  23.7 us
    all_to_all x1, waiting for transfers between devices, exchange_in_order(): filled = lax.all_to_all(filled, axes[k], k, k, tiled=True)  20 us
    all_to_all x1, starting transfers between devices, shards(): lax.all_to_all(expert_back, EP, split_axis=0, concat_axis=0, tiled=True)  14.4 us
    dot_general x8, matrix products, absorb(): jnp.einsum('hgrn,nhd->rhgd', rounded, value_block, preferred_element_type...  11.1 us
    dot_general x8, matrix products, absorb(): jnp.einsum('rhgd,nhd->hgrn', query_heads, key_block, preferred_element_ty...  11 us
    all_to_all x1, blocking collectives, exchange_in_order(): filled = lax.all_to_all(filled, axes[k], k, k, tiled=True)  10.5 us
  transfers between devices with their start and end apart: 5, of which 5 were waited for; matrix products, arithmetic and copies ran while one was open for 16% of the time, Pallas kernels for 0%

commit v1 on v0

v1 whole, which is shorter than its diff:
```python
import jax
import jax.numpy as jnp
from jax import lax
from jax.experimental import pallas as pl
from jax.experimental.pallas import tpu as pltpu
from jax.sharding import Mesh
from jax.sharding import PartitionSpec as P


HEAD = 64
GRID_W = 64
EPS = 1e-06
THETA = 10000.0
EP = ("z", "c")
TP = ("y", "x")
SIDE = 4
CAP = 22
KEY_STEP = 2048

F32 = jnp.float32
BF16 = jnp.bfloat16


def turn_tables(offset, length):
    half_width = HEAD // 2
    inverse = THETA ** (-jnp.arange(0, half_width, 2, dtype=F32) / half_width)
    positions = offset + jnp.arange(length, dtype=jnp.int32)
    grid_rows = (positions // GRID_W).astype(F32)
    grid_cols = (positions % GRID_W).astype(F32)
    angles = jnp.concatenate([grid_rows[:, None] * inverse, grid_cols[:, None] * inverse], axis=-1)
    return (jnp.cos(angles), jnp.sin(angles))


def norm_turn(source, scale_gain, cosine_table, sine_table):
    length = source.shape[0]
    head_rows = source.astype(F32).reshape(length, -1, HEAD)
    head_rows = (
        head_rows
        * lax.rsqrt(jnp.mean(head_rows * head_rows, axis=-1, keepdims=True) + EPS)
        * scale_gain
    )
    pair_view = head_rows.reshape(length, head_rows.shape[1], HEAD // 2, 2)
    even_part = pair_view[..., 0]
    odd_part = pair_view[..., 1]
    cosine_part = cosine_table[:, None, :]
    sine_part = sine_table[:, None, :]
    turned = jnp.stack(
        [
            even_part * cosine_part - odd_part * sine_part,
            even_part * sine_part + odd_part * cosine_part,
        ],
        axis=-1,
    )
    return turned.reshape(length, -1).astype(BF16)


def attend_body(q_ref, mine_ref, other_ref, out_ref):
    rows = q_ref.shape[0]
    lanes = lax.broadcasted_iota(jnp.int32, (rows, 2 * HEAD), 1)
    both = q_ref[...].astype(F32)
    low = jnp.where(lanes < HEAD, both, 0.0)
    high = pltpu.roll(jnp.where(lanes < HEAD, 0.0, both), HEAD, 1)
    wide = (jnp.concatenate([low, high], axis=0) * 0.125).astype(BF16)
    top = jnp.full((2 * rows, 1), -jnp.inf, F32)
    total = jnp.zeros((2 * rows, 1), F32)
    acc = jnp.zeros((2 * rows, 2 * HEAD), F32)
    steps = [
        (ref, at) for ref in (mine_ref, other_ref) for at in range(0, ref.shape[0], KEY_STEP)
    ]
    for ref, at in steps:
        block = ref[at : at + KEY_STEP, :]
        scores = lax.dot_general(wide, block, (((1,), (1,)), ((), ())), preferred_element_type=F32)
        new_top = jnp.maximum(top, jnp.max(scores, axis=1, keepdims=True))
        factor = jnp.exp(top - new_top)
        raw = jnp.exp(scores - new_top)
        total = total * factor + jnp.sum(raw, axis=1, keepdims=True)
        acc = acc * factor + jnp.dot(raw.astype(BF16), block, preferred_element_type=F32)
        top = new_top
    done = acc / total
    first = pltpu.roll(done[:rows], HEAD, 1)
    out_ref[...] = jnp.where(lanes < HEAD, first, done[rows:]).astype(BF16)


def attend(query_turned, mine, other):
    rows = query_turned.shape[0]
    keys = mine.shape[0] + other.shape[0]
    return pl.pallas_call(
        attend_body,
        out_shape=jax.ShapeDtypeStruct(query_turned.shape, BF16),
        compiler_params=pltpu.CompilerParams(vmem_limit_bytes=48 * 1024 * 1024),
        cost_estimate=pl.CostEstimate(
            flops=16 * rows * keys * HEAD,
            bytes_accessed=keys * 4 * HEAD,
            transcendentals=2 * rows * keys,
        ),
        name="attend",
    )(query_turned, mine, other)


def two_parts(value):
    high = lax.reduce_precision(value, 8, 7)
    return high.astype(BF16), (value - high).astype(BF16)


def stat_rows(sums, count):
    width = 256
    flat = jnp.pad(sums, (0, count * width - sums.shape[0])).reshape(count, width)
    high, low = two_parts(flat)
    return jnp.concatenate([high, low], axis=0)


def read_stat(rows, count, size):
    whole = rows.astype(F32)
    return jnp.sum(whole[:, :count] + whole[:, count:], axis=0).reshape(-1)[:size]


def copies_to(array, axis):
    wide = jnp.broadcast_to(array[None], (SIDE,) + array.shape)
    return lax.all_to_all(wide, axis, 0, 0, tiled=True)


def swap(array, axis):
    return lax.all_to_all(array, axis, 0, 0, tiled=True)


def shift(array, axis, by):
    size = lax.axis_size(axis)
    return lax.ppermute(array, axis, [(k, (k + by) % size) for k in range(size)])


def keys_everywhere(block):
    far = [block] + [shift(block, "z", by) for by in (4, 12, 8)]
    strided = jnp.concatenate(far, axis=0)
    near = [strided] + [shift(strided, "z", by) for by in (1, 15, 2)]
    mine = jnp.concatenate(near, axis=0)
    return mine, shift(mine, "c", 1)


def deal(chunk_for, axis):
    place = lax.axis_index(axis)
    landed = [chunk_for(place)]
    for by in range(1, SIDE):
        landed.append(shift(chunk_for((place + by) % SIDE), axis, by))
    return in_order(jnp.stack(landed), place)


def in_order(landed, place):
    return jnp.stack(
        [
            lax.dynamic_index_in_dim(landed, (place - k) % SIDE, 0, keepdims=False)
            for k in range(SIDE)
        ]
    )


def forward(
    queries,
    key_rows,
    values,
    query_gain,
    key_gain,
    mix_gain,
    out_weight,
    expert_input,
    expert_gain,
    route_ids,
    route_weights,
    expert_gate,
    expert_up,
    expert_down,
):
    length = queries.shape[0]
    experts_count = lax.axis_size(EP)
    place_x = lax.axis_index("x")
    place_y = lax.axis_index("y")
    slot_total = experts_count * CAP
    features = expert_gain.shape[0]
    piece = expert_input.shape[1]
    hid = expert_gate.shape[2]

    cosine_table, sine_table = turn_tables(lax.axis_index(EP) * length, length)
    key_turned = norm_turn(key_rows, key_gain, cosine_table, sine_table)
    mine, other = keys_everywhere(jnp.concatenate([key_turned, values], axis=1))
    query_turned = norm_turn(queries, query_gain, cosine_table, sine_table)

    copies = length * 2
    flat_ids = route_ids.reshape(copies)
    hit_marks = (flat_ids[:, None] == jnp.arange(experts_count, dtype=jnp.int32)[None, :]).astype(
        jnp.int32
    )
    earlier = jnp.cumsum(hit_marks, axis=0) - hit_marks
    places = jnp.sum(earlier * hit_marks, axis=1)
    slot_index = (flat_ids * CAP + places).reshape(length, 2)
    slot_axis = jnp.arange(slot_total, dtype=jnp.int32)
    pick = (
        (slot_index[:, 0][None, :] == slot_axis[:, None])
        | (slot_index[:, 1][None, :] == slot_axis[:, None])
    ).astype(BF16)
    outgoing = jnp.dot(pick, expert_input, preferred_element_type=F32).astype(BF16)
    arrived = swap(outgoing.reshape(experts_count, CAP, piece), EP).reshape(slot_total, piece)

    gate_view = expert_gate.reshape(SIDE, SIDE, piece, hid)
    up_view = expert_up.reshape(SIDE, SIDE, piece, hid)

    def first_chunk(k):
        pair = [lax.dynamic_index_in_dim(w, k, 1, keepdims=False) for w in (gate_view, up_view)]
        return jnp.concatenate(pair, axis=2).reshape(SIDE * piece, 2 * hid)

    def second_chunk(k):
        down = lax.dynamic_slice_in_dim(expert_down[0], k * SIDE * hid, SIDE * hid, 0)
        out = lax.dynamic_slice_in_dim(out_weight, k * SIDE * 2 * HEAD, SIDE * 2 * HEAD, 0)
        return jnp.concatenate([down, out], axis=0)

    first_weights = deal(first_chunk, "x")
    second_weights = deal(second_chunk, "y")

    gathered = copies_to(arrived, "y")
    gains = lax.dynamic_index_in_dim(
        expert_gain.reshape(SIDE, SIDE, piece), place_x, axis=1, keepdims=False
    )
    gathered_float = gathered.astype(F32)
    scaled = (gathered_float * gains[:, None, :]).astype(BF16)
    squares = jnp.sum(gathered_float * gathered_float, axis=(0, 2))
    partial = jnp.einsum(
        "ysf,xyfh->xsh",
        scaled,
        first_weights.reshape(SIDE, SIDE, piece, 2 * hid),
        preferred_element_type=F32,
    ).astype(BF16)
    stat_count = -(-slot_total // piece)
    stats = jnp.broadcast_to(stat_rows(squares, stat_count)[None], (SIDE, 2 * stat_count, piece))
    received = swap(jnp.concatenate([partial, stats], axis=1), "x")
    sums = jnp.sum(received[:, :slot_total].astype(F32), axis=0)
    square_sum = read_stat(received[:, slot_total:], stat_count, slot_total)
    row_stat = lax.rsqrt(square_sum / features + EPS)
    gate_value = sums[:, :hid] * row_stat[:, None]
    up_value = sums[:, hid:] * row_stat[:, None]
    hidden = (jax.nn.silu(gate_value) * up_value).astype(BF16)

    hidden_all = copies_to(hidden, "x")
    down_rows = second_weights[:, : SIDE * hid].reshape(SIDE, SIDE, hid, piece)
    out_rows = second_weights[:, SIDE * hid :].reshape(SIDE, SIDE, 2 * HEAD, piece)
    expert_partial = jnp.einsum(
        "xsh,yxhf->ysf", hidden_all, down_rows, preferred_element_type=F32
    ).astype(BF16)
    landed = swap(expert_partial, "y")
    expert_out = jnp.sum(landed.astype(F32), axis=0).astype(BF16)

    heads_out = attend(query_turned, mine, other)
    near = jnp.stack([heads_out] + [shift(heads_out, "x", by) for by in range(1, SIDE)])
    heads = in_order(near, place_x)
    head_float = heads.astype(F32)
    mix_gains = lax.dynamic_index_in_dim(
        mix_gain.reshape(SIDE, SIDE, 2 * HEAD), place_y, axis=0, keepdims=False
    )
    mix_in = (head_float * mix_gains[:, None, :]).astype(BF16)
    mix_squares = jnp.sum(head_float * head_float, axis=(0, 2))
    mix_partial = jnp.einsum(
        "xsh,yxhf->ysf", mix_in, out_rows, preferred_element_type=F32
    ).astype(BF16)
    mix_stats = jnp.broadcast_to(stat_rows(mix_squares, 1)[None], (SIDE, 2, piece))
    payload = jnp.concatenate([mix_partial, mix_stats], axis=1)

    def payload_of(k):
        return lax.dynamic_index_in_dim(payload, k, 0, keepdims=False)

    parts = [payload_of(place_y)] + [
        shift(payload_of((place_y + by) % SIDE), "y", by) for by in range(1, SIDE)
    ]
    mix_sum = sum(part[:length].astype(F32) for part in parts)
    mix_square_sum = read_stat(jnp.stack([part[length:] for part in parts]), 1, length)
    mix_scale = lax.rsqrt(mix_square_sum / mix_gain.shape[0] + EPS)
    attended = (mix_sum * mix_scale[:, None]).astype(BF16)

    returned = swap(expert_out.reshape(experts_count, CAP, piece), EP).reshape(slot_total, piece)
    slots = slot_axis[None, :]
    first = jnp.dot(
        (slot_index[:, :1] == slots).astype(BF16), returned, preferred_element_type=F32
    )
    second = jnp.dot(
        (slot_index[:, 1:] == slots).astype(BF16), returned, preferred_element_type=F32
    )
    expert_mix = (first * route_weights[:, :1] + second * route_weights[:, 1:]).astype(BF16)
    return (attended, expert_mix)


def solution(mesh):
    torus = Mesh(mesh.devices.reshape(-1, 2, SIDE, SIDE), ("z", "c", "y", "x"))
    return jax.shard_map(
        forward,
        mesh=torus,
        in_specs=(
            P(EP, TP),
            P(EP, TP),
            P(EP, TP),
            P(),
            P(),
            P(),
            P(None, TP),
            P(EP, TP),
            P(),
            P(EP, None),
            P(EP, None),
            P(EP, None, TP),
            P(EP, None, TP),
            P(EP, None, TP),
        ),
        out_specs=(P(EP, TP), P(EP, TP)),
        check_vma=False,
    )
```

time: 311 us -> 250 us (0.80)
  waiting for transfers between devices: 192 us -> 70.5 us
  starting transfers between devices: 24.3 us -> 116 us
  matrix products: 31.9 us -> 8.77 us
  between operations: 14.2 us -> 1.76 us
  blocking collectives: 10.5 us -> 0 us
  other arithmetic: 16.7 us -> 26.6 us
  Pallas kernels: 0 us -> 5.71 us
    all_gather x3 -> x0, waiting for transfers between devices: 148 us -> none  [the longest x2 106 us: in_one_piece(): filled = lax.all_gather(both, axis, axis=dim, tiled=True)]
    ppermute x0 -> x19, starting transfers between devices: none -> 79.7 us  [shift(): lax.ppermute(array, axis, [(k, (k + by) % size) for k in range(size)])]
    dot_general x20 -> x6, matrix products: 31.9 us -> 8.77 us  [the longest x1 3.52 us: forward(): jnp.einsum('xsh,yxhf->ysf', hidden_all, down_rows, preferred_element_type...]
    ppermute x0 -> x19, waiting for transfers between devices: none -> 21.5 us  [shift(): lax.ppermute(array, axis, [(k, (k + by) % size) for k in range(size)])]
    all_to_all x2 -> x6, starting transfers between devices: 24 us -> 35.9 us  [the longest x4 27.1 us: swap(): return lax.all_to_all(array, axis, 0, 0, tiled=True)]
    all_to_all x1 -> x0, blocking collectives: 10.5 us -> none  [exchange_in_order(): filled = lax.all_to_all(filled, axes[k], k, k, tiled=True)]
    concatenate x2 -> x12, other arithmetic: 2.12 us -> 9.4 us  [the longest x3 4.49 us: second_chunk(): return jnp.concatenate([down, out], axis=0)]
    another operation x4 -> x10, other arithmetic: 1.52 us -> 8.5 us  [the longest x3 3.2 us: deal(): return in_order(jnp.stack(landed), place)]
  transfers between devices with their start and end apart: 5 -> 25, of which waited for: 5 -> 7; matrix products, arithmetic and copies ran while one was open for 16% -> 20% of each run, Pallas kernels for 0% -> 2%
where the time goes in v1:
time: 250 us; the launch traced here: 248 us
  starting transfers between devices  116 us (46%)
  waiting for transfers between devices  70.5 us (28%)
  other arithmetic  26.6 us (11%)
  local copies, waits for them, and re-layouts  19.2 us (8%)
  matrix products  8.77 us (4%)
  Pallas kernels  5.71 us (2%)
    ppermute x19, starting transfers between devices, shift(): lax.ppermute(array, axis, [(k, (k + by) % size) for k in range(size)])  79.7 us
    all_to_all x4, waiting for transfers between devices, swap(): return lax.all_to_all(array, axis, 0, 0, tiled=True)  49 us
    all_to_all x4, starting transfers between devices, swap(): return lax.all_to_all(array, axis, 0, 0, tiled=True)  27.1 us
    ppermute x19, waiting for transfers between devices, shift(): lax.ppermute(array, axis, [(k, (k + by) % size) for k in range(size)])  21.5 us
    all_to_all x2, starting transfers between devices, copies_to(): return lax.all_to_all(wide, axis, 0, 0, tiled=True)  8.77 us
    pallas_call x1, Pallas kernels, attend(): pl.pallas_call(attend_body, out_shape=jax.ShapeDtypeStruct(query_turned.s...  5.71 us
  transfers between devices with their start and end apart: 25, of which 7 were waited for; matrix products, arithmetic and copies ran while one was open for 20% of the time, Pallas kernels for 2%

profile of v1, /device:TPU:1, one launch (start us, length us, event | category | flops | bytes accessed | tf_op | source)
XLA Modules:
  0.0 248.0 jit_solution(7129459594921092253)
XLA Ops:
  0.7 0.9 fusion.36
  2.9 0.9 copy.45
  4.5 9.6 %collective-permute-start.3 = (bf16[256,128]{1,0:T(8,128)(2,1)}, bf16[256,128]{1,0:T(8,128)(2,1)}, u32[]{:S(2)}, u32[]{:S(2)}) collective-permute-start(bf16[256,128]{1,0:T(8,128)(2,1)} %get-tuple-element.3), channel_id=1, source_target_pairs={{0,128},{32,160},{64,192},{96,224},{128,256},{160,288},{192,320},{... | collective-permute-start | bytes 196616 | tf_op jit(solution)/shard_map/ppermute | solution.py:128
  14.2 5.6 %collective-permute-start.4 = (bf16[256,128]{1,0:T(8,128)(2,1)}, bf16[256,128]{1,0:T(8,128)(2,1)}, u32[]{:S(2)}, u32[]{:S(2)}) collective-permute-start(bf16[256,128]{1,0:T(8,128)(2,1)} %get-tuple-element.3), channel_id=1, source_target_pairs={{0,384},{32,416},{64,448},{96,480},{128,0},{160,32},{192,64},{224,... | collective-permute-start | bytes 196616 | tf_op jit(solution)/shard_map/ppermute | solution.py:128
  19.8 2.2 constant_dynamic-slice_fusion.11
  22.0 0.9 pad_maximum_fusion.8
  22.8 3.1 %collective-permute-start.16 = (bf16[1024,256]{1,0:T(8,128)(2,1)}, bf16[1024,256]{1,0:T(8,128)(2,1)}, u32[]{:S(2)}, u32[]{:S(2)}) collective-permute-start(bf16[1024,256]{1,0:T(8,128)(2,1)} %pad_maximum_fusion.8), channel_id=1, source_target_pairs={{0,1},{1,2},{2,3},{3,0},{4,5},{5,6},{6,7},{7,4},{8,9},{9,10},{10,1... | collective-permute-start | bytes 1572872 | tf_op jit(solution)/shard_map/ppermute | solution.py:128
  26.0 0.9 pad_maximum_fusion.9
  26.8 4.3 %collective-permute-start.17 = (bf16[1024,256]{1,0:T(8,128)(2,1)}, bf16[1024,256]{1,0:T(8,128)(2,1)}, u32[]{:S(2)}, u32[]{:S(2)}) collective-permute-start(bf16[1024,256]{1,0:T(8,128)(2,1)} %pad_maximum_fusion.9), channel_id=1, source_target_pairs={{0,2},{1,3},{2,0},{3,1},{4,6},{5,7},{6,4},{7,5},{8,10},{9,11},{10,... | collective-permute-start | bytes 1572872 | tf_op jit(solution)/shard_map/ppermute | solution.py:128
  31.2 0.9 pad_maximum_fusion.10
  32.1 3.2 %collective-permute-start.18 = (bf16[1024,256]{1,0:T(8,128)(2,1)}, bf16[1024,256]{1,0:T(8,128)(2,1)}, u32[]{:S(2)}, u32[]{:S(2)}) collective-permute-start(bf16[1024,256]{1,0:T(8,128)(2,1)} %pad_maximum_fusion.10), channel_id=1, source_target_pairs={{0,3},{1,0},{2,1},{3,2},{4,7},{5,4},{6,5},{7,6},{8,11},{9,8},{10,9... | collective-permute-start | bytes 1572872 | tf_op jit(solution)/shard_map/ppermute | solution.py:128
  35.7 1.2 reduce-window.6
  37.8 0.9 reshape.443
  38.7 12.1 %all-to-all-start = ((bf16[32,22,256]{2,1,0:T(8,128)(2,1)}), bf16[32,22,256]{2,1,0:T(8,128)(2,1)S(1)}, u32[]{:S(2)}, u32[]{:S(2)}) async-start(bf16[32,22,256]{2,1,0:T(8,128)(2,1)} %reshape.443), calls=%async_computation | async-start | bytes 786432 | tf_op jit(solution)/shard_map/all_to_all | solution.py:123
  52.7 0.9 dynamic-slice_bitcast_fusion.3
  53.8 0.9 constant_dynamic-slice_fusion.25
  57.2 21.4 %all-to-all-done = bf16[32,22,256]{2,1,0:T(8,128)(2,1)S(1)} async-done(((bf16[32,22,256]{2,1,0:T(8,128)(2,1)}), bf16[32,22,256]{2,1,0:T(8,128)(2,1)S(1)}, u32[]{:S(2)}, u32[]{:S(2)}) %all-to-all-start) | async-done | bytes 360480 | tf_op jit(solution)/shard_map/all_to_all | solution.py:123
  78.7 1.2 broadcast_in_dim.12
  79.9 4.3 %all-to-all-start.1 = ((bf16[4,704,256]{2,1,0:T(8,128)(2,1)}), bf16[4,704,256]{2,1,0:T(8,128)(2,1)S(1)}, u32[]{:S(2)}, u32[]{:S(2)}) async-start(bf16[4,704,256]{2,1,0:T(8,128)(2,1)} %broadcast_in_dim.12), calls=%async_computation.1 | async-start | bytes 2883584 | tf_op jit(solution)/shard_map/all_to_all | solution.py:119
  84.2 1.9 pad_maximum_fusion.6
  86.1 1.8 pad_maximum_fusion.7
  87.9 2.2 collective-permute-start.5
  90.1 3.4 %collective-permute-start = (bf16[1024,256]{1,0:T(8,128)(2,1)}, bf16[1024,256]{1,0:T(8,128)(2,1)}, u32[]{:S(2)}, u32[]{:S(2)}) collective-permute-start(bf16[1024,256]{1,0:T(8,128)(2,1)} %pad_maximum_fusion.5), channel_id=1, source_target_pairs={{0,4},{4,8},{8,12},{12,0},{1,5},{5,9},{9,13},{13,1},{2,6},{6,10},{... | collective-permute-start | bytes 1572872 | tf_op jit(solution)/shard_map/ppermute | solution.py:128
  93.5 8.5 %collective-permute-done.5 = bf16[256,128]{1,0:T(8,128)(2,1)S(1)} collective-permute-done((bf16[256,128]{1,0:T(8,128)(2,1)}, bf16[256,128]{1,0:T(8,128)(2,1)S(1)}, u32[]{:S(2)}, u32[]{:S(2)}) %collective-permute-start.5) | collective-permute-done | bytes 65568 | tf_op jit(solution)/shard_map/ppermute | solution.py:128
  102.0 4.9 %collective-permute-start.1 = (bf16[1024,256]{1,0:T(8,128)(2,1)}, bf16[1024,256]{1,0:T(8,128)(2,1)}, u32[]{:S(2)}, u32[]{:S(2)}) collective-permute-start(bf16[1024,256]{1,0:T(8,128)(2,1)} %pad_maximum_fusion.6), channel_id=1, source_target_pairs={{0,8},{4,12},{8,0},{12,4},{1,9},{5,13},{9,1},{13,5},{2,10},{6,14},... | collective-permute-start | bytes 1572872 | tf_op jit(solution)/shard_map/ppermute | solution.py:128
  106.9 1.0 pad_maximum_fusion.11
  107.9 2.8 %collective-permute-start.2 = (bf16[1024,256]{1,0:T(8,128)(2,1)}, bf16[1024,256]{1,0:T(8,128)(2,1)}, u32[]{:S(2)}, u32[]{:S(2)}) collective-permute-start(bf16[1024,256]{1,0:T(8,128)(2,1)} %pad_maximum_fusion.7), channel_id=1, source_target_pairs={{0,12},{4,0},{8,4},{12,8},{1,13},{5,1},{9,5},{13,9},{2,14},{6,2},{... | collective-permute-start | bytes 1572872 | tf_op jit(solution)/shard_map/ppermute | solution.py:128
  110.7 1.9 collective-permute-start.6
  112.7 1.5 pad_maximum_fusion.2
  114.4 1.6 pad_maximum_fusion.3
  116.4 3.2 %fusion.2 = bf16[4,704,256]{2,1,0:T(8,128)(2,1)S(1)} fusion(bf16[4,4,256,256]{3,2,1,0:T(8,128)(2,1)} %bitcast.133, bf16[4,704,256]{2,1,0:T(8,128)(2,1)S(1)} %all-to-all-done.1, f32[4,256]{1,0:T(4,128)S(1)} %bitcast.150), kind=kOutput, calls=%fused_computation.11 | convolution fusion | flops 1479278592 | bytes 4984832 | tf_op jit(solution)/shard_map/ysf,xyfh->xsh/dot_general | solution.py:224
  119.7 1.2 pad_maximum_fusion.4
  120.9 4.5 %all-to-all-start.2 = ((bf16[4,710,256]{2,1,0:T(8,128)(2,1)}), bf16[4,710,256]{2,1,0:T(8,128)(2,1)}, u32[]{:S(2)}, u32[]{:S(2)}) async-start(bf16[4,710,256]{2,1,0:T(8,128)(2,1)} %pad_maximum_fusion.4), calls=%async_computation.2 | async-start | bytes 2916352 | tf_op jit(solution)/shard_map/all_to_all | solution.py:123
  125.8 4.6 %collective-permute-start.7 = (bf16[1024,128]{1,0:T(8,128)(2,1)S(1)}, bf16[1024,128]{1,0:T(8,128)(2,1)S(1)}, u32[]{:S(2)}, u32[]{:S(2)}) collective-permute-start(bf16[1024,128]{1,0:T(8,128)(2,1)S(1)} %pad_maximum_fusion.11), channel_id=1, source_target_pairs={{0,480},{32,0},{64,32},{96,64},{128,96},{160,128},{192,160},{224,1... | collective-permute-start | bytes 786440 | tf_op jit(solution)/shard_map/ppermute | solution.py:128
  130.4 0.9 constant_dynamic-update-slice_fusion.5
  131.2 0.9 constant_dynamic-update-slice_fusion.4
  132.1 1.9 collective-permute-start.8
  134.1 1.0 constant_dynamic-update-slice_fusion.2
  135.1 8.3 %collective-permute-done.8 = bf16[1024,128]{1,0:T(8,128)(2,1)S(1)} collective-permute-done((bf16[1024,128]{1,0:T(8,128)(2,1)S(1)}, bf16[1024,128]{1,0:T(8,128)(2,1)S(1)}, u32[]{:S(2)}, u32[]{:S(2)}) %collective-permute-start.8) | collective-permute-done | bytes 262176 | tf_op jit(solution)/shard_map/ppermute | solution.py:128
  143.5 10.0 %collective-permute-start.9 = (bf16[4096,128]{1,0:T(8,128)(2,1)S(1)}, bf16[4096,128]{1,0:T(8,128)(2,1)S(1)}, u32[]{:S(2)}, u32[]{:S(2)}) collective-permute-start(bf16[4096,128]{1,0:T(8,128)(2,1)S(1)} %constant_dynamic-update-slice_fusion.mine_ref), channel_id=1, source_target_pairs={{0,16},{16,0},{1,17},{17,1},{2,18},{18,2},{3,19},{19,3},{4,20},{20... | collective-permute-start | bytes 3145736 | tf_op jit(solution)/shard_map/ppermute | solution.py:128
  153.5 1.6 pad_maximum_fusion
  155.2 1.2 constant_dynamic-slice_fusion.21
  156.4 1.6 convert_reduce_fusion
  159.0 1.0 broadcast_in_dim.14
  160.0 4.5 %all-to-all-start.3 = ((bf16[4,704,128]{2,1,0:T(8,128)(2,1)}), bf16[4,704,128]{2,1,0:T(8,128)(2,1)}, u32[]{:S(2)}, u32[]{:S(2)}) async-start(bf16[4,704,128]{2,1,0:T(8,128)(2,1)} %broadcast_in_dim.14), calls=%async_computation.3 | async-start | bytes 1441792 | tf_op jit(solution)/shard_map/all_to_all | solution.py:119
  164.4 1.5 pad_maximum_fusion.1
  165.9 1.4 fusion.57
  167.3 5.7 %attend.1 = bf16[256,128]{1,0:T(8,128)(2,1)S(1)} custom-call(bf16[256,128]{1,0:T(8,128)(2,1)S(1)} %copy.46.q_ref, bf16[4096,128]{1,0:T(8,128)(2,1)S(1)} %constant_dynamic-update-slice_fusion.mine_ref, bf16[4096,128]{1,0:T(8,128)(2,1)S(1)} %collective-permute-done.9.other_ref), custom_call_target="tpu_custom_call" | custom-call | flops 2147483648 | bytes 2097152 | tf_op jit(solution)/shard_map/attend/pallas_call | solution.py:87
  173.1 3.5 %collective-permute-start.10 = (bf16[256,128]{1,0:T(8,128)(2,1)S(1)}, bf16[256,128]{1,0:T(8,128)(2,1)S(1)}, u32[]{:S(2)}, u32[]{:S(2)}) collective-permute-start(bf16[256,128]{1,0:T(8,128)(2,1)S(1)} %attend.1), channel_id=1, source_target_pairs={{0,1},{1,2},{2,3},{3,0},{4,5},{5,6},{6,7},{7,4},{8,9},{9,10},{10,1... | collective-permute-start | bytes 196616 | tf_op jit(solution)/shard_map/ppermute | solution.py:128
  176.6 4.3 %collective-permute-start.11 = (bf16[256,128]{1,0:T(8,128)(2,1)S(1)}, bf16[256,128]{1,0:T(8,128)(2,1)S(1)}, u32[]{:S(2)}, u32[]{:S(2)}) collective-permute-start(bf16[256,128]{1,0:T(8,128)(2,1)S(1)} %attend.1), channel_id=1, source_target_pairs={{0,2},{1,3},{2,0},{3,1},{4,6},{5,7},{6,4},{7,5},{8,10},{9,11},{10,... | collective-permute-start | bytes 196616 | tf_op jit(solution)/shard_map/ppermute | solution.py:128
  180.9 3.1 %collective-permute-start.12 = (bf16[256,128]{1,0:T(8,128)(2,1)S(1)}, bf16[256,128]{1,0:T(8,128)(2,1)S(1)}, u32[]{:S(2)}, u32[]{:S(2)}) collective-permute-start(bf16[256,128]{1,0:T(8,128)(2,1)S(1)} %attend.1), channel_id=1, source_target_pairs={{0,3},{1,0},{2,1},{3,2},{4,7},{5,4},{6,5},{7,6},{8,11},{9,8},{10,9... | collective-permute-start | bytes 196616 | tf_op jit(solution)/shard_map/ppermute | solution.py:128
  184.0 3.5 %fusion.3 = bf16[4,704,256]{2,1,0:T(8,128)(2,1)} fusion(bf16[4,4,128,256]{3,2,1,0:T(8,128)(2,1)} %bitcast.137, bf16[4,704,128]{2,1,0:T(8,128)(2,1)} %all-to-all-done.3), kind=kOutput, calls=%fused_computation.12 | convolution fusion | flops 738918400 | bytes 3211264 | tf_op jit(solution)/shard_map/xsh,yxhf->ysf/dot_general | solution.py:243
  187.5 4.5 %all-to-all-start.4 = ((bf16[4,704,256]{2,1,0:T(8,128)(2,1)}), bf16[4,704,256]{2,1,0:T(8,128)(2,1)}, u32[]{:S(2)}, u32[]{:S(2)}) async-start(bf16[4,704,256]{2,1,0:T(8,128)(2,1)} %fusion.3), calls=%async_computation.4 | async-start | bytes 2883584 | tf_op jit(solution)/shard_map/all_to_all | solution.py:123
  193.5 4.5 %collective-permute-start.15 = (bf16[258,256]{1,0:T(8,128)(2,1)S(1)}, bf16[258,256]{1,0:T(8,128)(2,1)S(1)}, u32[]{:S(2)}, u32[]{:S(2)}) collective-permute-start(bf16[258,256]{1,0:T(8,128)(2,1)S(1)} %get-tuple-element.33), channel_id=1, source_target_pairs={{0,12},{4,0},{8,4},{12,8},{1,13},{5,1},{9,5},{13,9},{2,14},{6,2},{... | collective-permute-start | bytes 396296 | tf_op jit(solution)/shard_map/ppermute | solution.py:128
  198.0 12.2 %all-to-all-done.4 = bf16[4,704,256]{2,1,0:T(8,128)(2,1)} async-done(((bf16[4,704,256]{2,1,0:T(8,128)(2,1)}), bf16[4,704,256]{2,1,0:T(8,128)(2,1)}, u32[]{:S(2)}, u32[]{:S(2)}) %all-to-all-start.4) | async-done | bytes 1441824 | tf_op jit(solution)/shard_map/all_to_all | solution.py:123
  210.2 1.7 reduce_sum.98
  211.9 0.9 reshape.447
  212.8 6.0 %all-to-all-start.5 = ((bf16[32,22,256]{2,1,0:T(8,128)(2,1)}), bf16[32,22,256]{2,1,0:T(8,128)(2,1)S(1)}, u32[]{:S(2)}, u32[]{:S(2)}) async-start(bf16[32,22,256]{2,1,0:T(8,128)(2,1)} %reshape.447), calls=%async_computation.5 | async-start | bytes 786432 | tf_op jit(solution)/shard_map/all_to_all | solution.py:123
  218.9 2.2 collective-permute-start.14
  221.1 4.6 %collective-permute-start.13 = (bf16[258,256]{1,0:T(8,128)(2,1)S(1)}, bf16[258,256]{1,0:T(8,128)(2,1)S(1)}, u32[]{:S(2)}, u32[]{:S(2)}) collective-permute-start(bf16[258,256]{1,0:T(8,128)(2,1)S(1)} %get-tuple-element.31), channel_id=1, source_target_pairs={{0,4},{4,8},{8,12},{12,0},{1,5},{5,9},{9,13},{13,1},{2,6},{6,10},{... | collective-permute-start | bytes 396296 | tf_op jit(solution)/shard_map/ppermute | solution.py:128
  225.7 1.5 collective-permute-done.14
  227.2 3.1 %collective-permute-done.13 = bf16[258,256]{1,0:T(8,128)(2,1)S(1)} collective-permute-done((bf16[258,256]{1,0:T(8,128)(2,1)S(1)}, bf16[258,256]{1,0:T(8,128)(2,1)S(1)}, u32[]{:S(2)}, u32[]{:S(2)}) %collective-permute-start.13) | collective-permute-done | bytes 132128 | tf_op jit(solution)/shard_map/ppermute | solution.py:128
  231.1 15.5 %all-to-all-done.5 = bf16[32,22,256]{2,1,0:T(8,128)(2,1)S(1)} async-done(((bf16[32,22,256]{2,1,0:T(8,128)(2,1)}), bf16[32,22,256]{2,1,0:T(8,128)(2,1)S(1)}, u32[]{:S(2)}, u32[]{:S(2)}) %all-to-all-start.5) | async-done | bytes 360480 | tf_op jit(solution)/shard_map/all_to_all | solution.py:123
  247.0 1.0 fusion.10
  (146 shorter events, 12.6 us)
Async XLA Ops:
  0.6 36.9 %copy-start = (bf16[256,256]{1,0:T(8,128)(2,1)S(1)}, bf16[256,256]{1,0:T(8,128)(2,1)}, u32[]{:S(2)}) copy-start(bf16[256,256]{1,0:T(8,128)(2,1)} %param.21) | copy-start | bytes 393220
  0.6 19.1 %copy-start.7 = (bf16[1,4096,128]{2,1,0:T(8,128)(2,1)S(1)}, bf16[1,4096,128]{2,1,0:T(8,128)(2,1)}, u32[]{:S(2)}) copy-start(bf16[1,4096,128]{2,1,0:T(8,128)(2,1)} %param.26) | copy-start | bytes 3145732
  4.5 83.4 %collective-permute-start.3 = (bf16[256,128]{1,0:T(8,128)(2,1)}, bf16[256,128]{1,0:T(8,128)(2,1)}, u32[]{:S(2)}, u32[]{:S(2)}) collective-permute-start(bf16[256,128]{1,0:T(8,128)(2,1)} %get-tuple-element.3), channel_id=1, source_target_pairs={{0,128},{32,160},{64,192},{96,224},{128,256},{160,288},{192,320},{... | collective-permute-start | bytes 196616 | tf_op jit(solution)/shard_map/ppermute | solution.py:128
  14.2 76.0 %collective-permute-start.4 = (bf16[256,128]{1,0:T(8,128)(2,1)}, bf16[256,128]{1,0:T(8,128)(2,1)}, u32[]{:S(2)}, u32[]{:S(2)}) collective-permute-start(bf16[256,128]{1,0:T(8,128)(2,1)} %get-tuple-element.3), channel_id=1, source_target_pairs={{0,384},{32,416},{64,448},{96,480},{128,0},{160,32},{192,64},{224,... | collective-permute-start | bytes 196616 | tf_op jit(solution)/shard_map/ppermute | solution.py:128
  22.0 13.3 %copy-start.18 = (s32[256,2]{0,1:T(2,128)S(1)}, s32[256,2]{0,1:T(2,128)}, u32[]{:S(2)}) copy-start(s32[256,2]{0,1:T(2,128)} %param.23) | copy-start | bytes 6148
  22.8 85.0 %collective-permute-start.16 = (bf16[1024,256]{1,0:T(8,128)(2,1)}, bf16[1024,256]{1,0:T(8,128)(2,1)}, u32[]{:S(2)}, u32[]{:S(2)}) collective-permute-start(bf16[1024,256]{1,0:T(8,128)(2,1)} %pad_maximum_fusion.8), channel_id=1, source_target_pairs={{0,1},{1,2},{2,3},{3,0},{4,5},{5,6},{6,7},{7,4},{8,9},{9,10},{10,1... | collective-permute-start | bytes 1572872 | tf_op jit(solution)/shard_map/ppermute | solution.py:128
  26.8 83.9 %collective-permute-start.17 = (bf16[1024,256]{1,0:T(8,128)(2,1)}, bf16[1024,256]{1,0:T(8,128)(2,1)}, u32[]{:S(2)}, u32[]{:S(2)}) collective-permute-start(bf16[1024,256]{1,0:T(8,128)(2,1)} %pad_maximum_fusion.9), channel_id=1, source_target_pairs={{0,2},{1,3},{2,0},{3,1},{4,6},{5,7},{6,4},{7,5},{8,10},{9,11},{10,... | collective-permute-start | bytes 1572872 | tf_op jit(solution)/shard_map/ppermute | solution.py:128
  31.2 19.7 %copy-start.17 = (f32[4096]{0:T(1024)S(1)}, f32[4096]{0:T(1024)}, u32[]{:S(2)}) copy-start(f32[4096]{0:T(1024)} %param.22) | copy-start | bytes 49156
  31.2 20.3 %copy-start.16 = (bf16[256,128]{1,0:T(8,128)(2,1)S(1)}, bf16[256,128]{1,0:T(8,128)(2,1)}, u32[]{:S(2)}) copy-start(bf16[256,128]{1,0:T(8,128)(2,1)} %param.14) | copy-start | bytes 196612
  32.1 20.3 %copy-start.24 = (f32[64]{0:T(128)S(1)}, f32[64]{0:T(128)}, u32[]{:S(2)}) copy-start(f32[64]{0:T(128)} %param.17) | copy-start | bytes 772
  32.1 20.6 %copy-start.2 = (bf16[1,2048,256]{2,1,0:T(8,128)(2,1)S(1)}, bf16[1,2048,256]{2,1,0:T(8,128)(2,1)}, u32[]{:S(2)}) copy-start(bf16[1,2048,256]{2,1,0:T(8,128)(2,1)} %param.27) | copy-start | bytes 3145732
  32.1 80.6 %collective-permute-start.18 = (bf16[1024,256]{1,0:T(8,128)(2,1)}, bf16[1024,256]{1,0:T(8,128)(2,1)}, u32[]{:S(2)}, u32[]{:S(2)}) collective-permute-start(bf16[1024,256]{1,0:T(8,128)(2,1)} %pad_maximum_fusion.10), channel_id=1, source_target_pairs={{0,3},{1,0},{2,1},{3,2},{4,7},{5,4},{6,5},{7,6},{8,11},{9,8},{10,9... | collective-permute-start | bytes 1572872 | tf_op jit(solution)/shard_map/ppermute | solution.py:128
  37.5 13.4 %copy-start.20 = (s32[256,1]{0,1:T(1,128)}, s32[256,1]{0,1:T(1,128)S(1)}, u32[]{:S(2)}) copy-start(s32[256,1]{0,1:T(1,128)S(1)} %get-tuple-element.51) | copy-start | bytes 3076
  37.5 13.4 %copy-start.22 = (s32[256,1]{0,1:T(1,128)}, s32[256,1]{0,1:T(1,128)S(1)}, u32[]{:S(2)}) copy-start(s32[256,1]{0,1:T(1,128)S(1)} %get-tuple-element.50) | copy-start | bytes 3076
  38.7 39.9 %all-to-all-start = ((bf16[32,22,256]{2,1,0:T(8,128)(2,1)}), bf16[32,22,256]{2,1,0:T(8,128)(2,1)S(1)}, u32[]{:S(2)}, u32[]{:S(2)}) async-start(bf16[32,22,256]{2,1,0:T(8,128)(2,1)} %reshape.443), calls=%async_computation | async-start | bytes 786432 | tf_op jit(solution)/shard_map/all_to_all | solution.py:123
  52.5 1.3 copy-start.3
  53.8 1.8 copy-start.11
  79.9 4.3 %copy-start.6 = (bf16[512,256]{1,0:T(8,128)(2,1)S(1)}, bf16[512,256]{1,0:T(8,128)(2,1)}, u32[]{:S(2)}) copy-start(bf16[512,256]{1,0:T(8,128)(2,1)} %get-tuple-element.25) | copy-start | bytes 786436
  79.9 6.2 %copy-start.5 = (bf16[512,256]{1,0:T(8,128)(2,1)S(1)}, bf16[512,256]{1,0:T(8,128)(2,1)}, u32[]{:S(2)}) copy-start(bf16[512,256]{1,0:T(8,128)(2,1)} %get-tuple-element.24) | copy-start | bytes 786436
  79.9 36.1 %all-to-all-start.1 = ((bf16[4,704,256]{2,1,0:T(8,128)(2,1)}), bf16[4,704,256]{2,1,0:T(8,128)(2,1)S(1)}, u32[]{:S(2)}, u32[]{:S(2)}) async-start(bf16[4,704,256]{2,1,0:T(8,128)(2,1)} %broadcast_in_dim.12), calls=%async_computation.1 | async-start | bytes 2883584 | tf_op jit(solution)/shard_map/all_to_all | solution.py:119
  84.2 5.9 %copy-start.4 = (bf16[512,256]{1,0:T(8,128)(2,1)S(1)}, bf16[512,256]{1,0:T(8,128)(2,1)}, u32[]{:S(2)}) copy-start(bf16[512,256]{1,0:T(8,128)(2,1)} %get-tuple-element.26) | copy-start | bytes 786436
  84.2 28.4 %copy-start.9 = (bf16[4,1,256,128]{3,2,1,0:T(8,128)(2,1)S(1)}, bf16[4,1,256,128]{3,2,1,0:T(8,128)(2,1)}, u32[]{:S(2)}) copy-start(bf16[4,1,256,128]{3,2,1,0:T(8,128)(2,1)} %get-tuple-element.18) | copy-start | bytes 786436
  84.2 28.4 %copy-start.10 = (bf16[4,1,256,128]{3,2,1,0:T(8,128)(2,1)S(1)}, bf16[4,1,256,128]{3,2,1,0:T(8,128)(2,1)}, u32[]{:S(2)}) copy-start(bf16[4,1,256,128]{3,2,1,0:T(8,128)(2,1)} %get-tuple-element.65) | copy-start | bytes 786436
  87.9 14.1 %collective-permute-start.5 = (bf16[256,128]{1,0:T(8,128)(2,1)}, bf16[256,128]{1,0:T(8,128)(2,1)S(1)}, u32[]{:S(2)}, u32[]{:S(2)}) collective-permute-start(bf16[256,128]{1,0:T(8,128)(2,1)} %get-tuple-element.3), channel_id=1, source_target_pairs={{0,256},{32,288},{64,320},{96,352},{128,384},{160,416},{192,448},{... | collective-permute-start | bytes 196616 | tf_op jit(solution)/shard_map/ppermute | solution.py:128
  90.1 63.4 %collective-permute-start = (bf16[1024,256]{1,0:T(8,128)(2,1)}, bf16[1024,256]{1,0:T(8,128)(2,1)}, u32[]{:S(2)}, u32[]{:S(2)}) collective-permute-start(bf16[1024,256]{1,0:T(8,128)(2,1)} %pad_maximum_fusion.5), channel_id=1, source_target_pairs={{0,4},{4,8},{8,12},{12,0},{1,5},{5,9},{9,13},{13,1},{2,6},{6,10},{... | collective-permute-start | bytes 1572872 | tf_op jit(solution)/shard_map/ppermute | solution.py:128
  102.0 10.6 %copy-start.14 = (bf16[256,128]{1,0:T(8,128)(2,1)}, bf16[256,128]{1,0:T(8,128)(2,1)S(1)}, u32[]{:S(2)}) copy-start(bf16[256,128]{1,0:T(8,128)(2,1)S(1)} %collective-permute-done.5) | copy-start | bytes 196612
  102.0 51.5 %collective-permute-start.1 = (bf16[1024,256]{1,0:T(8,128)(2,1)}, bf16[1024,256]{1,0:T(8,128)(2,1)}, u32[]{:S(2)}, u32[]{:S(2)}) collective-permute-start(bf16[1024,256]{1,0:T(8,128)(2,1)} %pad_maximum_fusion.6), channel_id=1, source_target_pairs={{0,8},{4,12},{8,0},{12,4},{1,9},{5,13},{9,1},{13,5},{2,10},{6,14},... | collective-permute-start | bytes 1572872 | tf_op jit(solution)/shard_map/ppermute | solution.py:128
  107.9 45.7 %collective-permute-start.2 = (bf16[1024,256]{1,0:T(8,128)(2,1)}, bf16[1024,256]{1,0:T(8,128)(2,1)}, u32[]{:S(2)}, u32[]{:S(2)}) collective-permute-start(bf16[1024,256]{1,0:T(8,128)(2,1)} %pad_maximum_fusion.7), channel_id=1, source_target_pairs={{0,12},{4,0},{8,4},{12,8},{1,13},{5,1},{9,5},{13,9},{2,14},{6,2},{... | collective-permute-start | bytes 1572872 | tf_op jit(solution)/shard_map/ppermute | solution.py:128
  110.7 21.4 %collective-permute-start.6 = (bf16[1024,128]{1,0:T(8,128)(2,1)S(1)}, bf16[1024,128]{1,0:T(8,128)(2,1)}, u32[]{:S(2)}, u32[]{:S(2)}) collective-permute-start(bf16[1024,128]{1,0:T(8,128)(2,1)S(1)} %pad_maximum_fusion.11), channel_id=1, source_target_pairs={{0,32},{32,64},{64,96},{96,128},{128,160},{160,192},{192,224},{224... | collective-permute-start | bytes 786440 | tf_op jit(solution)/shard_map/ppermute | solution.py:128
  120.9 4.5 %copy-start.12 = (bf16[256,2,32,1]{0,3,2,1:T(2,128)(2,1)S(1)}, bf16[256,2,32,1]{0,3,2,1:T(2,128)(2,1)}, u32[]{:S(2)}) copy-start(bf16[256,2,32,1]{0,3,2,1:T(2,128)(2,1)} %get-tuple-element.38) | copy-start | bytes 98308
  120.9 4.5 %copy-start.13 = (bf16[256,2,32,1]{0,3,2,1:T(2,128)(2,1)S(1)}, bf16[256,2,32,1]{0,3,2,1:T(2,128)(2,1)}, u32[]{:S(2)}) copy-start(bf16[256,2,32,1]{0,3,2,1:T(2,128)(2,1)} %get-tuple-element.39) | copy-start | bytes 98308
  120.9 13.2 %copy-start.15 = (bf16[256,128]{1,0:T(8,128)(2,1)S(1)}, bf16[256,128]{1,0:T(8,128)(2,1)}, u32[]{:S(2)}) copy-start(bf16[256,128]{1,0:T(8,128)(2,1)} %copy-done.14) | copy-start | bytes 196612
  120.9 35.5 %all-to-all-start.2 = ((bf16[4,710,256]{2,1,0:T(8,128)(2,1)}), bf16[4,710,256]{2,1,0:T(8,128)(2,1)}, u32[]{:S(2)}, u32[]{:S(2)}) async-start(bf16[4,710,256]{2,1,0:T(8,128)(2,1)} %pad_maximum_fusion.4), calls=%async_computation.2 | async-start | bytes 2916352 | tf_op jit(solution)/shard_map/all_to_all | solution.py:123
  125.8 9.2 %collective-permute-start.7 = (bf16[1024,128]{1,0:T(8,128)(2,1)S(1)}, bf16[1024,128]{1,0:T(8,128)(2,1)S(1)}, u32[]{:S(2)}, u32[]{:S(2)}) collective-permute-start(bf16[1024,128]{1,0:T(8,128)(2,1)S(1)} %pad_maximum_fusion.11), channel_id=1, source_target_pairs={{0,480},{32,0},{64,32},{96,64},{128,96},{160,128},{192,160},{224,1... | collective-permute-start | bytes 786440 | tf_op jit(solution)/shard_map/ppermute | solution.py:128
  132.1 11.3 %collective-permute-start.8 = (bf16[1024,128]{1,0:T(8,128)(2,1)S(1)}, bf16[1024,128]{1,0:T(8,128)(2,1)S(1)}, u32[]{:S(2)}, u32[]{:S(2)}) collective-permute-start(bf16[1024,128]{1,0:T(8,128)(2,1)S(1)} %pad_maximum_fusion.11), channel_id=1, source_target_pairs={{0,64},{32,96},{64,128},{96,160},{128,192},{160,224},{192,256},{22... | collective-permute-start | bytes 786440 | tf_op jit(solution)/shard_map/ppermute | solution.py:128
  143.5 23.9 %collective-permute-start.9 = (bf16[4096,128]{1,0:T(8,128)(2,1)S(1)}, bf16[4096,128]{1,0:T(8,128)(2,1)S(1)}, u32[]{:S(2)}, u32[]{:S(2)}) collective-permute-start(bf16[4096,128]{1,0:T(8,128)(2,1)S(1)} %constant_dynamic-update-slice_fusion.mine_ref), channel_id=1, source_target_pairs={{0,16},{16,0},{1,17},{17,1},{2,18},{18,2},{3,19},{19,3},{4,20},{20... | collective-permute-start | bytes 3145736 | tf_op jit(solution)/shard_map/ppermute | solution.py:128
  159.0 5.4 %copy-start.1 = (bf16[1,1024,256]{2,1,0:T(8,128)(2,1)S(1)}, bf16[1,1024,256]{2,1,0:T(8,128)(2,1)}, u32[]{:S(2)}) copy-start(bf16[1,1024,256]{2,1,0:T(8,128)(2,1)} %get-tuple-element.11) | copy-start | bytes 1572868
  160.0 24.0 %all-to-all-start.3 = ((bf16[4,704,128]{2,1,0:T(8,128)(2,1)}), bf16[4,704,128]{2,1,0:T(8,128)(2,1)}, u32[]{:S(2)}, u32[]{:S(2)}) async-start(bf16[4,704,128]{2,1,0:T(8,128)(2,1)} %broadcast_in_dim.14), calls=%async_computation.3 | async-start | bytes 1441792 | tf_op jit(solution)/shard_map/all_to_all | solution.py:119
  173.1 19.6 %collective-permute-start.10 = (bf16[256,128]{1,0:T(8,128)(2,1)S(1)}, bf16[256,128]{1,0:T(8,128)(2,1)S(1)}, u32[]{:S(2)}, u32[]{:S(2)}) collective-permute-start(bf16[256,128]{1,0:T(8,128)(2,1)S(1)} %attend.1), channel_id=1, source_target_pairs={{0,1},{1,2},{2,3},{3,0},{4,5},{5,6},{6,7},{7,4},{8,9},{9,10},{10,1... | collective-permute-start | bytes 196616 | tf_op jit(solution)/shard_map/ppermute | solution.py:128
  176.6 16.1 %collective-permute-start.11 = (bf16[256,128]{1,0:T(8,128)(2,1)S(1)}, bf16[256,128]{1,0:T(8,128)(2,1)S(1)}, u32[]{:S(2)}, u32[]{:S(2)}) collective-permute-start(bf16[256,128]{1,0:T(8,128)(2,1)S(1)} %attend.1), channel_id=1, source_target_pairs={{0,2},{1,3},{2,0},{3,1},{4,6},{5,7},{6,4},{7,5},{8,10},{9,11},{10,... | collective-permute-start | bytes 196616 | tf_op jit(solution)/shard_map/ppermute | solution.py:128
  180.9 11.8 %collective-permute-start.12 = (bf16[256,128]{1,0:T(8,128)(2,1)S(1)}, bf16[256,128]{1,0:T(8,128)(2,1)S(1)}, u32[]{:S(2)}, u32[]{:S(2)}) collective-permute-start(bf16[256,128]{1,0:T(8,128)(2,1)S(1)} %attend.1), channel_id=1, source_target_pairs={{0,3},{1,0},{2,1},{3,2},{4,7},{5,4},{6,5},{7,6},{8,11},{9,8},{10,9... | collective-permute-start | bytes 196616 | tf_op jit(solution)/shard_map/ppermute | solution.py:128
  187.5 5.4 %copy-start.8 = (bf16[4,512,256]{2,1,0:T(8,128)(2,1)S(1)}, bf16[4,512,256]{2,1,0:T(8,128)(2,1)}, u32[]{:S(2)}) copy-start(bf16[4,512,256]{2,1,0:T(8,128)(2,1)} %get-tuple-element.9) | copy-start | bytes 3145732
  187.5 22.7 %all-to-all-start.4 = ((bf16[4,704,256]{2,1,0:T(8,128)(2,1)}), bf16[4,704,256]{2,1,0:T(8,128)(2,1)}, u32[]{:S(2)}, u32[]{:S(2)}) async-start(bf16[4,704,256]{2,1,0:T(8,128)(2,1)} %fusion.3), calls=%async_computation.4 | async-start | bytes 2883584 | tf_op jit(solution)/shard_map/all_to_all | solution.py:123
  193.4 25.4 %copy-start.19 = (f32[256,2]{0,1:T(2,128)S(1)}, f32[256,2]{0,1:T(2,128)}, u32[]{:S(2)}) copy-start(f32[256,2]{0,1:T(2,128)} %param.24) | copy-start | bytes 6148
  193.5 53.2 %copy-start.23 = (s32[256,1]{0,1:T(1,128)S(1)}, s32[256,1]{0,1:T(1,128)}, u32[]{:S(2)}) copy-start(s32[256,1]{0,1:T(1,128)} %copy-done.22) | copy-start | bytes 3076
  193.5 32.2 %collective-permute-start.15 = (bf16[258,256]{1,0:T(8,128)(2,1)S(1)}, bf16[258,256]{1,0:T(8,128)(2,1)S(1)}, u32[]{:S(2)}, u32[]{:S(2)}) collective-permute-start(bf16[258,256]{1,0:T(8,128)(2,1)S(1)} %get-tuple-element.33), channel_id=1, source_target_pairs={{0,12},{4,0},{8,4},{12,8},{1,13},{5,1},{9,5},{13,9},{2,14},{6,2},{... | collective-permute-start | bytes 396296 | tf_op jit(solution)/shard_map/ppermute | solution.py:128
  211.9 35.1 %copy-start.21 = (s32[256,1]{0,1:T(1,128)S(1)}, s32[256,1]{0,1:T(1,128)}, u32[]{:S(2)}) copy-start(s32[256,1]{0,1:T(1,128)} %copy-done.20) | copy-start | bytes 3076
  212.8 33.8 %all-to-all-start.5 = ((bf16[32,22,256]{2,1,0:T(8,128)(2,1)}), bf16[32,22,256]{2,1,0:T(8,128)(2,1)S(1)}, u32[]{:S(2)}, u32[]{:S(2)}) async-start(bf16[32,22,256]{2,1,0:T(8,128)(2,1)} %reshape.447), calls=%async_computation.5 | async-start | bytes 786432 | tf_op jit(solution)/shard_map/all_to_all | solution.py:123
  218.9 8.3 %collective-permute-start.14 = (bf16[258,256]{1,0:T(8,128)(2,1)S(1)}, bf16[258,256]{1,0:T(8,128)(2,1)S(1)}, u32[]{:S(2)}, u32[]{:S(2)}) collective-permute-start(bf16[258,256]{1,0:T(8,128)(2,1)S(1)} %get-tuple-element.32), channel_id=1, source_target_pairs={{0,8},{4,12},{8,0},{12,4},{1,9},{5,13},{9,1},{13,5},{2,10},{6,14},... | collective-permute-start | bytes 396296 | tf_op jit(solution)/shard_map/ppermute | solution.py:128
  221.1 9.2 %collective-permute-start.13 = (bf16[258,256]{1,0:T(8,128)(2,1)S(1)}, bf16[258,256]{1,0:T(8,128)(2,1)S(1)}, u32[]{:S(2)}, u32[]{:S(2)}) collective-permute-start(bf16[258,256]{1,0:T(8,128)(2,1)S(1)} %get-tuple-element.31), channel_id=1, source_target_pairs={{0,4},{4,8},{8,12},{12,0},{1,5},{5,9},{9,13},{13,1},{2,6},{6,10},{... | collective-permute-start | bytes 396296 | tf_op jit(solution)/shard_map/ppermute | solution.py:128

commit v2 on v1

--- a/solution.py
+++ b/solution.py
@@ -54,7 +54,7 @@
     return turned.reshape(length, -1).astype(BF16)
 
 
-def attend_body(q_ref, mine_ref, other_ref, out_ref):
+def attend_body(q_ref, kv_ref, out_ref):
     rows = q_ref.shape[0]
     lanes = lax.broadcasted_iota(jnp.int32, (rows, 2 * HEAD), 1)
     both = q_ref[...].astype(F32)
@@ -64,11 +64,8 @@
     top = jnp.full((2 * rows, 1), -jnp.inf, F32)
     total = jnp.zeros((2 * rows, 1), F32)
     acc = jnp.zeros((2 * rows, 2 * HEAD), F32)
-    steps = [
-        (ref, at) for ref in (mine_ref, other_ref) for at in range(0, ref.shape[0], KEY_STEP)
-    ]
-    for ref, at in steps:
-        block = ref[at : at + KEY_STEP, :]
+    for at in range(0, kv_ref.shape[0], KEY_STEP):
+        block = kv_ref[at : at + KEY_STEP, :]
         scores = lax.dot_general(wide, block, (((1,), (1,)), ((), ())), preferred_element_type=F32)
         new_top = jnp.maximum(top, jnp.max(scores, axis=1, keepdims=True))
         factor = jnp.exp(top - new_top)
@@ -81,9 +78,9 @@
     out_ref[...] = jnp.where(lanes < HEAD, first, done[rows:]).astype(BF16)
 
 
-def attend(query_turned, mine, other):
+def attend(query_turned, key_value):
     rows = query_turned.shape[0]
-    keys = mine.shape[0] + other.shape[0]
+    keys = key_value.shape[0]
     return pl.pallas_call(
         attend_body,
         out_shape=jax.ShapeDtypeStruct(query_turned.shape, BF16),
@@ -94,7 +91,7 @@
             transcendentals=2 * rows * keys,
         ),
         name="attend",
-    )(query_turned, mine, other)
+    )(query_turned, key_value)
 
 
 def two_parts(value):
@@ -126,14 +123,6 @@
 def shift(array, axis, by):
     size = lax.axis_size(axis)
     return lax.ppermute(array, axis, [(k, (k + by) % size) for k in range(size)])
-
-
-def keys_everywhere(block):
-    far = [block] + [shift(block, "z", by) for by in (4, 12, 8)]
-    strided = jnp.concatenate(far, axis=0)
-    near = [strided] + [shift(strided, "z", by) for by in (1, 15, 2)]
-    mine = jnp.concatenate(near, axis=0)
-    return mine, shift(mine, "c", 1)
 
 
 def deal(chunk_for, axis):
@@ -180,7 +169,9 @@
 
     cosine_table, sine_table = turn_tables(lax.axis_index(EP) * length, length)
     key_turned = norm_turn(key_rows, key_gain, cosine_table, sine_table)
-    mine, other = keys_everywhere(jnp.concatenate([key_turned, values], axis=1))
+    key_value = jnp.concatenate([key_turned, values], axis=1)
+    key_value = lax.all_gather(key_value, EP, axis=0, tiled=False)
+    key_value = key_value.reshape(experts_count * length, 2 * HEAD)
     query_turned = norm_turn(queries, query_gain, cosine_table, sine_table)
 
     copies = length * 2
@@ -246,7 +237,7 @@
     landed = swap(expert_partial, "y")
     expert_out = jnp.sum(landed.astype(F32), axis=0).astype(BF16)
 
-    heads_out = attend(query_turned, mine, other)
+    heads_out = attend(query_turned, key_value)
     near = jnp.stack([heads_out] + [shift(heads_out, "x", by) for by in range(1, SIDE)])
     heads = in_order(near, place_x)
     head_float = heads.astype(F32)

time: 250 us -> 218 us (0.87)
  starting transfers between devices: 116 us -> 89.6 us
  between operations: 1.76 us -> 15.1 us
  other arithmetic: 26.6 us -> 16.6 us
  local copies, waits for them, and re-layouts: 19.2 us -> 12.8 us
    ppermute x19 -> x12, starting transfers between devices: 79.7 us -> 45.4 us  [shift(): lax.ppermute(array, axis, [(k, (k + by) % size) for k in range(size)])]
    ppermute x19 -> x12, waiting for transfers between devices: 21.5 us -> 5.12 us  [shift(): lax.ppermute(array, axis, [(k, (k + by) % size) for k in range(size)])]
    all_to_all x2, waiting for transfers between devices: 0.01 us -> 9.21 us  [copies_to(): return lax.all_to_all(wide, axis, 0, 0, tiled=True)]
    all_to_all x4, starting transfers between devices: 27.1 us -> 35.5 us  [swap(): return lax.all_to_all(array, axis, 0, 0, tiled=True)]
    all_to_all x4, waiting for transfers between devices: 49 us -> 54.2 us  [swap(): return lax.all_to_all(array, axis, 0, 0, tiled=True)]
  transfers between devices with their start and end apart: 25 -> 19, of which waited for: 7 -> 8; matrix products, arithmetic and copies ran while one was open for 20% -> 14% of each run, Pallas kernels for 2% -> 3%
where the time goes in v2:
time: 218 us; the launch traced here: 217 us
  starting transfers between devices  89.6 us (41%)
  waiting for transfers between devices  68.6 us (31%)
  other arithmetic  16.6 us (8%)
  between operations  15.1 us (7%)
  local copies, waits for them, and re-layouts  12.8 us (6%)
  matrix products  8.41 us (4%)
  Pallas kernels  5.69 us (3%)
    all_to_all x4, waiting for transfers between devices, swap(): return lax.all_to_all(array, axis, 0, 0, tiled=True)  54.2 us
    ppermute x12, starting transfers between devices, shift(): lax.ppermute(array, axis, [(k, (k + by) % size) for k in range(size)])  45.4 us
    all_to_all x4, starting transfers between devices, swap(): return lax.all_to_all(array, axis, 0, 0, tiled=True)  35.5 us
    all_to_all x2, waiting for transfers between devices, copies_to(): return lax.all_to_all(wide, axis, 0, 0, tiled=True)  9.21 us
    all_to_all x2, starting transfers between devices, copies_to(): return lax.all_to_all(wide, axis, 0, 0, tiled=True)  8.69 us
    pallas_call x1, Pallas kernels, attend(): pl.pallas_call(attend_body, out_shape=jax.ShapeDtypeStruct(query_turned.s...  5.69 us
    ppermute x12, waiting for transfers between devices, shift(): lax.ppermute(array, axis, [(k, (k + by) % size) for k in range(size)])  5.12 us
  transfers between devices with their start and end apart: 19, of which 8 were waited for; matrix products, arithmetic and copies ran while one was open for 14% of the time, Pallas kernels for 3%

profile of v2, /device:TPU:1, one launch (start us, length us, event | category | flops | bytes accessed | tf_op | source)
XLA Modules:
  0.0 217.0 jit_solution(9205868041314648350)
XLA Ops:
  7.2 2.5 %constant_dynamic-slice_fusion.11 = (bf16[4,1,256,128]{3,2,1,0:T(8,128)(2,1)}, bf16[4,1,256,128]{3,2,1,0:T(8,128)(2,1)S(1)}, bf16[4,1,256,128]{3,2,1,0:T(8,128)(...) fusion(bf16[4,4,256,128]{3,2,1,0:T(8,128)(2,1)} %bitcast.134, ...), kind=kLoop, calls=%fused_computation.121 | loop fusion | bytes 4194320 | tf_op jit(solution)/shard_map/jit(dynamic_index_in_dim)/dynamic_slice | solution.py:197
  9.7 0.9 pad_maximum_fusion.8
  10.6 3.9 %collective-permute-start.9 = (bf16[1024,256]{1,0:T(8,128)(2,1)}, bf16[1024,256]{1,0:T(8,128)(2,1)}, u32[]{:S(2)}, u32[]{:S(2)}) collective-permute-start(bf16[1024,256]{1,0:T(8,128)(2,1)} %pad_maximum_fusion.8), channel_id=1, source_target_pairs={{0,1},{1,2},{2,3},{3,0},{4,5},{5,6},{6,7},{7,4},{8,9},{9,10},{10,1... | collective-permute-start | bytes 1572872 | tf_op jit(solution)/shard_map/ppermute | solution.py:125
  14.6 0.8 pad_maximum_fusion.9
  15.4 4.3 %collective-permute-start.10 = (bf16[1024,256]{1,0:T(8,128)(2,1)}, bf16[1024,256]{1,0:T(8,128)(2,1)}, u32[]{:S(2)}, u32[]{:S(2)}) collective-permute-start(bf16[1024,256]{1,0:T(8,128)(2,1)} %pad_maximum_fusion.9), channel_id=1, source_target_pairs={{0,2},{1,3},{2,0},{3,1},{4,6},{5,7},{6,4},{7,5},{8,10},{9,11},{10,... | collective-permute-start | bytes 1572872 | tf_op jit(solution)/shard_map/ppermute | solution.py:125
  19.8 0.9 pad_maximum_fusion.10
  20.7 3.1 %collective-permute-start.11 = (bf16[1024,256]{1,0:T(8,128)(2,1)}, bf16[1024,256]{1,0:T(8,128)(2,1)}, u32[]{:S(2)}, u32[]{:S(2)}) collective-permute-start(bf16[1024,256]{1,0:T(8,128)(2,1)} %pad_maximum_fusion.10), channel_id=1, source_target_pairs={{0,3},{1,0},{2,1},{3,2},{4,7},{5,4},{6,5},{7,6},{8,11},{9,8},{10,9... | collective-permute-start | bytes 1572872 | tf_op jit(solution)/shard_map/ppermute | solution.py:125
  24.2 1.2 reduce-window.6
  25.3 0.2 slice_reduce_fusion
  26.0 0.3 convolution_convert_fusion
  26.3 0.9 reshape.447
  27.1 16.8 %all-to-all-start = ((bf16[32,22,256]{2,1,0:T(8,128)(2,1)}), bf16[32,22,256]{2,1,0:T(8,128)(2,1)S(1)}, u32[]{:S(2)}, u32[]{:S(2)}) async-start(bf16[32,22,256]{2,1,0:T(8,128)(2,1)} %reshape.447), calls=%async_computation | async-start | bytes 786432 | tf_op jit(solution)/shard_map/all_to_all | solution.py:120
  44.1 0.8 constant_dynamic-slice_fusion.25
  44.9 0.8 pad_maximum_fusion.5
  45.8 3.2 %collective-permute-start = (bf16[1024,256]{1,0:T(8,128)(2,1)}, bf16[1024,256]{1,0:T(8,128)(2,1)}, u32[]{:S(2)}, u32[]{:S(2)}) collective-permute-start(bf16[1024,256]{1,0:T(8,128)(2,1)} %pad_maximum_fusion.5), channel_id=1, source_target_pairs={{0,4},{4,8},{8,12},{12,0},{1,5},{5,9},{9,13},{13,1},{2,6},{6,10},{... | collective-permute-start | bytes 1572872 | tf_op jit(solution)/shard_map/ppermute | solution.py:125
  49.0 0.8 pad_maximum_fusion.6
  49.8 4.5 %collective-permute-start.1 = (bf16[1024,256]{1,0:T(8,128)(2,1)}, bf16[1024,256]{1,0:T(8,128)(2,1)}, u32[]{:S(2)}, u32[]{:S(2)}) collective-permute-start(bf16[1024,256]{1,0:T(8,128)(2,1)} %pad_maximum_fusion.6), channel_id=1, source_target_pairs={{0,8},{4,12},{8,0},{12,4},{1,9},{5,13},{9,1},{13,5},{2,10},{6,14},... | collective-permute-start | bytes 1572872 | tf_op jit(solution)/shard_map/ppermute | solution.py:125
  55.1 0.7 pad_maximum_fusion.14
  55.9 15.7 %all-to-all-done = bf16[32,22,256]{2,1,0:T(8,128)(2,1)S(1)} async-done(((bf16[32,22,256]{2,1,0:T(8,128)(2,1)}), bf16[32,22,256]{2,1,0:T(8,128)(2,1)S(1)}, u32[]{:S(2)}, u32[]{:S(2)}) %all-to-all-start) | async-done | bytes 360480 | tf_op jit(solution)/shard_map/all_to_all | solution.py:120
  71.8 1.2 broadcast_in_dim.12
  73.0 4.3 %all-to-all-start.1 = ((bf16[4,704,256]{2,1,0:T(8,128)(2,1)}), bf16[4,704,256]{2,1,0:T(8,128)(2,1)S(1)}, u32[]{:S(2)}, u32[]{:S(2)}) async-start(bf16[4,704,256]{2,1,0:T(8,128)(2,1)} %broadcast_in_dim.12), calls=%async_computation.1 | async-start | bytes 2883584 | tf_op jit(solution)/shard_map/all_to_all | solution.py:116
  77.8 0.9 pad_maximum_fusion.7
  78.7 4.6 %collective-permute-start.2 = (bf16[1024,256]{1,0:T(8,128)(2,1)}, bf16[1024,256]{1,0:T(8,128)(2,1)}, u32[]{:S(2)}, u32[]{:S(2)}) collective-permute-start(bf16[1024,256]{1,0:T(8,128)(2,1)} %pad_maximum_fusion.7), channel_id=1, source_target_pairs={{0,12},{4,0},{8,4},{12,8},{1,13},{5,1},{9,5},{13,9},{2,14},{6,2},{... | collective-permute-start | bytes 1572872 | tf_op jit(solution)/shard_map/ppermute | solution.py:125
  83.4 1.5 pad_maximum_fusion.2
  85.0 1.6 pad_maximum_fusion.3
  86.6 9.2 %all-to-all-done.1 = bf16[4,704,256]{2,1,0:T(8,128)(2,1)S(1)} async-done(((bf16[4,704,256]{2,1,0:T(8,128)(2,1)}), bf16[4,704,256]{2,1,0:T(8,128)(2,1)S(1)}, u32[]{:S(2)}, u32[]{:S(2)}) %all-to-all-start.1) | async-done | bytes 1441824 | tf_op jit(solution)/shard_map/all_to_all | solution.py:116
  95.8 0.4 fusion.1
  96.2 3.3 %fusion.2 = bf16[4,704,256]{2,1,0:T(8,128)(2,1)S(1)} fusion(bf16[4,4,256,256]{3,2,1,0:T(8,128)(2,1)} %bitcast.133, bf16[4,704,256]{2,1,0:T(8,128)(2,1)S(1)} %all-to-all-done.1, f32[4,256]{1,0:T(4,128)S(1)} %bitcast.150), kind=kOutput, calls=%fused_computation.11 | convolution fusion | flops 1479278592 | bytes 4984832 | tf_op jit(solution)/shard_map/ysf,xyfh->xsh/dot_general | solution.py:215
  99.5 1.2 pad_maximum_fusion.4
  100.7 3.6 %all-to-all-start.2 = ((bf16[4,710,256]{2,1,0:T(8,128)(2,1)}), bf16[4,710,256]{2,1,0:T(8,128)(2,1)S(1)}, u32[]{:S(2)}, u32[]{:S(2)}) async-start(bf16[4,710,256]{2,1,0:T(8,128)(2,1)} %pad_maximum_fusion.4), calls=%async_computation.2 | async-start | bytes 2916352 | tf_op jit(solution)/shard_map/all_to_all | solution.py:120
  104.6 0.2 subtract_convert_fusion
  104.8 0.2 pad_maximum_fusion.13
  105.2 0.5 collective-permute-done.2
  105.7 1.6 pad_maximum_fusion
  107.3 0.9 constant_dynamic-slice_fusion.21
  108.3 13.7 %all-to-all-done.2 = bf16[4,710,256]{2,1,0:T(8,128)(2,1)S(1)} async-done(((bf16[4,710,256]{2,1,0:T(8,128)(2,1)}), bf16[4,710,256]{2,1,0:T(8,128)(2,1)S(1)}, u32[]{:S(2)}, u32[]{:S(2)}) %all-to-all-start.2) | async-done | bytes 1454112 | tf_op jit(solution)/shard_map/all_to_all | solution.py:120
  122.0 0.2 convert_reduce_fusion
  122.3 0.2 fusion.19
  122.5 0.9 broadcast_in_dim.14
  123.4 4.4 %all-to-all-start.3 = ((bf16[4,704,128]{2,1,0:T(8,128)(2,1)}), bf16[4,704,128]{2,1,0:T(8,128)(2,1)}, u32[]{:S(2)}, u32[]{:S(2)}) async-start(bf16[4,704,128]{2,1,0:T(8,128)(2,1)} %broadcast_in_dim.14), calls=%async_computation.3 | async-start | bytes 1441792 | tf_op jit(solution)/shard_map/all_to_all | solution.py:116
  127.8 0.3 pad_maximum_fusion.1
  128.0 0.1 fusion.57
  128.2 1.6 copy-done.1
  129.8 5.7 %attend.1 = bf16[256,128]{1,0:T(8,128)(2,1)S(1)} custom-call(bf16[256,128]{1,0:T(8,128)(2,1)S(1)} %copy.46.q_ref, bf16[8192,128]{1,0:T(8,128)(2,1)S(1)} %copy-done.1), custom_call_target="tpu_custom_call" | custom-call | flops 2147483648 | bytes 2097152 | tf_op jit(solution)/shard_map/attend/pallas_call | solution.py:84
  135.5 3.1 %collective-permute-start.3 = (bf16[256,128]{1,0:T(8,128)(2,1)S(1)}, bf16[256,128]{1,0:T(8,128)(2,1)S(1)}, u32[]{:S(2)}, u32[]{:S(2)}) collective-permute-start(bf16[256,128]{1,0:T(8,128)(2,1)S(1)} %attend.1), channel_id=1, source_target_pairs={{0,1},{1,2},{2,3},{3,0},{4,5},{5,6},{6,7},{7,4},{8,9},{9,10},{10,1... | collective-permute-start | bytes 196616 | tf_op jit(solution)/shard_map/ppermute | solution.py:125
  138.7 4.3 %collective-permute-start.4 = (bf16[256,128]{1,0:T(8,128)(2,1)S(1)}, bf16[256,128]{1,0:T(8,128)(2,1)S(1)}, u32[]{:S(2)}, u32[]{:S(2)}) collective-permute-start(bf16[256,128]{1,0:T(8,128)(2,1)S(1)} %attend.1), channel_id=1, source_target_pairs={{0,2},{1,3},{2,0},{3,1},{4,6},{5,7},{6,4},{7,5},{8,10},{9,11},{10,... | collective-permute-start | bytes 196616 | tf_op jit(solution)/shard_map/ppermute | solution.py:125
  143.0 3.1 %collective-permute-start.5 = (bf16[256,128]{1,0:T(8,128)(2,1)S(1)}, bf16[256,128]{1,0:T(8,128)(2,1)S(1)}, u32[]{:S(2)}, u32[]{:S(2)}) collective-permute-start(bf16[256,128]{1,0:T(8,128)(2,1)S(1)} %attend.1), channel_id=1, source_target_pairs={{0,3},{1,0},{2,1},{3,2},{4,7},{5,4},{6,5},{7,6},{8,11},{9,8},{10,9... | collective-permute-start | bytes 196616 | tf_op jit(solution)/shard_map/ppermute | solution.py:125
  146.1 3.2 %fusion.3 = bf16[4,704,256]{2,1,0:T(8,128)(2,1)} fusion(bf16[4,4,128,256]{3,2,1,0:T(8,128)(2,1)S(1)} %bitcast.137, bf16[4,704,128]{2,1,0:T(8,128)(2,1)} %all-to-all-done.3), kind=kOutput, calls=%fused_computation.12 | convolution fusion | flops 738918400 | bytes 3211264 | tf_op jit(solution)/shard_map/xsh,yxhf->ysf/dot_general | solution.py:234
  149.2 3.5 %all-to-all-start.4 = ((bf16[4,704,256]{2,1,0:T(8,128)(2,1)}), bf16[4,704,256]{2,1,0:T(8,128)(2,1)S(1)}, u32[]{:S(2)}, u32[]{:S(2)}) async-start(bf16[4,704,256]{2,1,0:T(8,128)(2,1)} %fusion.3), calls=%async_computation.4 | async-start | bytes 2883584 | tf_op jit(solution)/shard_map/all_to_all | solution.py:120
  152.8 0.7 fusion.51
  153.7 0.4 fusion.8
  154.3 4.5 %collective-permute-start.8 = (bf16[258,256]{1,0:T(8,128)(2,1)S(1)}, bf16[258,256]{1,0:T(8,128)(2,1)S(1)}, u32[]{:S(2)}, u32[]{:S(2)}) collective-permute-start(bf16[258,256]{1,0:T(8,128)(2,1)S(1)} %get-tuple-element.31), channel_id=1, source_target_pairs={{0,12},{4,0},{8,4},{12,8},{1,13},{5,1},{9,5},{13,9},{2,14},{6,2},{... | collective-permute-start | bytes 396296 | tf_op jit(solution)/shard_map/ppermute | solution.py:125
  158.8 9.2 %all-to-all-done.4 = bf16[4,704,256]{2,1,0:T(8,128)(2,1)S(1)} async-done(((bf16[4,704,256]{2,1,0:T(8,128)(2,1)}), bf16[4,704,256]{2,1,0:T(8,128)(2,1)S(1)}, u32[]{:S(2)}, u32[]{:S(2)}) %all-to-all-start.4) | async-done | bytes 1441824 | tf_op jit(solution)/shard_map/all_to_all | solution.py:120
  168.1 0.4 reduce_sum.98
  168.5 0.8 reshape.451
  169.3 11.6 %all-to-all-start.5 = ((bf16[32,22,256]{2,1,0:T(8,128)(2,1)}), bf16[32,22,256]{2,1,0:T(8,128)(2,1)S(1)}, u32[]{:S(2)}, u32[]{:S(2)}) async-start(bf16[32,22,256]{2,1,0:T(8,128)(2,1)} %reshape.451), calls=%async_computation.5 | async-start | bytes 786432 | tf_op jit(solution)/shard_map/all_to_all | solution.py:120
  181.0 2.2 %collective-permute-start.7 = (bf16[258,256]{1,0:T(8,128)(2,1)S(1)}, bf16[258,256]{1,0:T(8,128)(2,1)S(1)}, u32[]{:S(2)}, u32[]{:S(2)}) collective-permute-start(bf16[258,256]{1,0:T(8,128)(2,1)S(1)} %get-tuple-element.30), channel_id=1, source_target_pairs={{0,8},{4,12},{8,0},{12,4},{1,9},{5,13},{9,1},{13,5},{2,10},{6,14},... | collective-permute-start | bytes 396296 | tf_op jit(solution)/shard_map/ppermute | solution.py:125
  183.2 4.5 %collective-permute-start.6 = (bf16[258,256]{1,0:T(8,128)(2,1)S(1)}, bf16[258,256]{1,0:T(8,128)(2,1)S(1)}, u32[]{:S(2)}, u32[]{:S(2)}) collective-permute-start(bf16[258,256]{1,0:T(8,128)(2,1)S(1)} %get-tuple-element.29), channel_id=1, source_target_pairs={{0,4},{4,8},{8,12},{12,0},{1,5},{5,9},{9,13},{13,1},{2,6},{6,10},{... | collective-permute-start | bytes 396296 | tf_op jit(solution)/shard_map/ppermute | solution.py:125
  187.8 1.5 collective-permute-done.7
  189.3 3.1 %collective-permute-done.6 = bf16[258,256]{1,0:T(8,128)(2,1)S(1)} collective-permute-done((bf16[258,256]{1,0:T(8,128)(2,1)S(1)}, bf16[258,256]{1,0:T(8,128)(2,1)S(1)}, u32[]{:S(2)}, u32[]{:S(2)}) %collective-permute-start.6) | collective-permute-done | bytes 132128 | tf_op jit(solution)/shard_map/ppermute | solution.py:125
  192.4 0.8 fusion.27
  193.2 15.5 %all-to-all-done.5 = bf16[32,22,256]{2,1,0:T(8,128)(2,1)S(1)} async-done(((bf16[32,22,256]{2,1,0:T(8,128)(2,1)}), bf16[32,22,256]{2,1,0:T(8,128)(2,1)S(1)}, u32[]{:S(2)}, u32[]{:S(2)}) %all-to-all-start.5) | async-done | bytes 360480 | tf_op jit(solution)/shard_map/all_to_all | solution.py:120
  208.8 0.3 convolution_multiply_fusion.1
  209.1 1.0 fusion.10
  (110 shorter events, 3.3 us)
Async XLA Ops:
  7.2 18.8 %copy-start = (bf16[256,256]{1,0:T(8,128)(2,1)S(1)}, bf16[256,256]{1,0:T(8,128)(2,1)}, u32[]{:S(2)}) copy-start(bf16[256,256]{1,0:T(8,128)(2,1)} %param.21) | copy-start | bytes 393220
  9.7 14.0 %copy-start.12 = (s32[256,2]{0,1:T(2,128)S(1)}, s32[256,2]{0,1:T(2,128)}, u32[]{:S(2)}) copy-start(s32[256,2]{0,1:T(2,128)} %param.23) | copy-start | bytes 6148
  10.6 68.1 %collective-permute-start.9 = (bf16[1024,256]{1,0:T(8,128)(2,1)}, bf16[1024,256]{1,0:T(8,128)(2,1)}, u32[]{:S(2)}, u32[]{:S(2)}) collective-permute-start(bf16[1024,256]{1,0:T(8,128)(2,1)} %pad_maximum_fusion.8), channel_id=1, source_target_pairs={{0,1},{1,2},{2,3},{3,0},{4,5},{5,6},{6,7},{7,4},{8,9},{9,10},{10,1... | collective-permute-start | bytes 1572872 | tf_op jit(solution)/shard_map/ppermute | solution.py:125
  15.4 67.9 %collective-permute-start.10 = (bf16[1024,256]{1,0:T(8,128)(2,1)}, bf16[1024,256]{1,0:T(8,128)(2,1)}, u32[]{:S(2)}, u32[]{:S(2)}) collective-permute-start(bf16[1024,256]{1,0:T(8,128)(2,1)} %pad_maximum_fusion.9), channel_id=1, source_target_pairs={{0,2},{1,3},{2,0},{3,1},{4,6},{5,7},{6,4},{7,5},{8,10},{9,11},{10,... | collective-permute-start | bytes 1572872 | tf_op jit(solution)/shard_map/ppermute | solution.py:125
  19.8 24.2 %copy-start.3 = (bf16[1,2048,256]{2,1,0:T(8,128)(2,1)S(1)}, bf16[1,2048,256]{2,1,0:T(8,128)(2,1)}, u32[]{:S(2)}) copy-start(bf16[1,2048,256]{2,1,0:T(8,128)(2,1)} %param.27) | copy-start | bytes 3145732
  20.7 62.7 %collective-permute-start.11 = (bf16[1024,256]{1,0:T(8,128)(2,1)}, bf16[1024,256]{1,0:T(8,128)(2,1)}, u32[]{:S(2)}, u32[]{:S(2)}) collective-permute-start(bf16[1024,256]{1,0:T(8,128)(2,1)} %pad_maximum_fusion.10), channel_id=1, source_target_pairs={{0,3},{1,0},{2,1},{3,2},{4,7},{5,4},{6,5},{7,6},{8,11},{9,8},{10,9... | collective-permute-start | bytes 1572872 | tf_op jit(solution)/shard_map/ppermute | solution.py:125
  26.0 18.1 %copy-start.4 = (bf16[2048,256]{1,0:T(8,128)(2,1)S(1)}, bf16[2048,256]{1,0:T(8,128)(2,1)}, u32[]{:S(2)}) copy-start(bf16[2048,256]{1,0:T(8,128)(2,1)} %param.20) | copy-start | bytes 3145732
  27.1 44.5 %all-to-all-start = ((bf16[32,22,256]{2,1,0:T(8,128)(2,1)}), bf16[32,22,256]{2,1,0:T(8,128)(2,1)S(1)}, u32[]{:S(2)}, u32[]{:S(2)}) async-start(bf16[32,22,256]{2,1,0:T(8,128)(2,1)} %reshape.447), calls=%async_computation | async-start | bytes 786432 | tf_op jit(solution)/shard_map/all_to_all | solution.py:120
  43.9 84.3 %all-gather.3.cloned.1.call-start = ((), (), s32[]{:S(2)}) async-start(), calls=%async_computation.6 | async-start | bytes 2162688 | tf_op jit(solution)/shard_map/all_gather | solution.py:173
  44.1 10.2 %copy-start.8 = (bf16[256,64]{0,1:T(8,128)(2,1)S(1)}, bf16[256,64]{0,1:T(8,128)(2,1)}, u32[]{:S(2)}) copy-start(bf16[256,64]{0,1:T(8,128)(2,1)} %param.15) | copy-start | bytes 98308
  44.1 10.2 %copy-start.14 = (f32[64]{0:T(128)S(1)}, f32[64]{0:T(128)}, u32[]{:S(2)}) copy-start(f32[64]{0:T(128)} %param.18) | copy-start | bytes 772
  44.1 10.9 %copy-start.10 = (bf16[256,64]{0,1:T(8,128)(2,1)S(1)}, bf16[256,64]{0,1:T(8,128)(2,1)}, u32[]{:S(2)}) copy-start(bf16[256,64]{0,1:T(8,128)(2,1)} %param.16) | copy-start | bytes 98308
  44.9 11.0 %copy-start.11 = (f32[4096]{0:T(1024)S(1)}, f32[4096]{0:T(1024)}, u32[]{:S(2)}) copy-start(f32[4096]{0:T(1024)} %param.22) | copy-start | bytes 49156
  45.8 59.4 %collective-permute-start = (bf16[1024,256]{1,0:T(8,128)(2,1)}, bf16[1024,256]{1,0:T(8,128)(2,1)}, u32[]{:S(2)}, u32[]{:S(2)}) collective-permute-start(bf16[1024,256]{1,0:T(8,128)(2,1)} %pad_maximum_fusion.5), channel_id=1, source_target_pairs={{0,4},{4,8},{8,12},{12,0},{1,5},{5,9},{9,13},{13,1},{2,6},{6,10},{... | collective-permute-start | bytes 1572872 | tf_op jit(solution)/shard_map/ppermute | solution.py:125
  49.8 55.4 %collective-permute-start.1 = (bf16[1024,256]{1,0:T(8,128)(2,1)}, bf16[1024,256]{1,0:T(8,128)(2,1)}, u32[]{:S(2)}, u32[]{:S(2)}) collective-permute-start(bf16[1024,256]{1,0:T(8,128)(2,1)} %pad_maximum_fusion.6), channel_id=1, source_target_pairs={{0,8},{4,12},{8,0},{12,4},{1,9},{5,13},{9,1},{13,5},{2,10},{6,14},... | collective-permute-start | bytes 1572872 | tf_op jit(solution)/shard_map/ppermute | solution.py:125
  71.8 5.7 %copy-start.9 = (bf16[256,128]{1,0:T(8,128)(2,1)S(1)}, bf16[256,128]{1,0:T(8,128)(2,1)}, u32[]{:S(2)}) copy-start(bf16[256,128]{1,0:T(8,128)(2,1)} %param.14) | copy-start | bytes 196612
  73.0 4.6 %copy-start.15 = (f32[64]{0:T(128)S(1)}, f32[64]{0:T(128)}, u32[]{:S(2)}) copy-start(f32[64]{0:T(128)} %param.17) | copy-start | bytes 772
  73.0 4.8 %copy-start.5 = (bf16[512,256]{1,0:T(8,128)(2,1)S(1)}, bf16[512,256]{1,0:T(8,128)(2,1)}, u32[]{:S(2)}) copy-start(bf16[512,256]{1,0:T(8,128)(2,1)} %get-tuple-element.26) | copy-start | bytes 786436
  73.0 10.3 %copy-start.6 = (bf16[4,1,256,128]{3,2,1,0:T(8,128)(2,1)S(1)}, bf16[4,1,256,128]{3,2,1,0:T(8,128)(2,1)}, u32[]{:S(2)}) copy-start(bf16[4,1,256,128]{3,2,1,0:T(8,128)(2,1)} %get-tuple-element.16) | copy-start | bytes 786436
  73.0 10.3 %copy-start.7 = (bf16[4,1,256,128]{3,2,1,0:T(8,128)(2,1)S(1)}, bf16[4,1,256,128]{3,2,1,0:T(8,128)(2,1)}, u32[]{:S(2)}) copy-start(bf16[4,1,256,128]{3,2,1,0:T(8,128)(2,1)} %get-tuple-element.63) | copy-start | bytes 786436
  73.0 22.8 %all-to-all-start.1 = ((bf16[4,704,256]{2,1,0:T(8,128)(2,1)}), bf16[4,704,256]{2,1,0:T(8,128)(2,1)S(1)}, u32[]{:S(2)}, u32[]{:S(2)}) async-start(bf16[4,704,256]{2,1,0:T(8,128)(2,1)} %broadcast_in_dim.12), calls=%async_computation.1 | async-start | bytes 2883584 | tf_op jit(solution)/shard_map/all_to_all | solution.py:116
  78.7 27.0 %collective-permute-start.2 = (bf16[1024,256]{1,0:T(8,128)(2,1)}, bf16[1024,256]{1,0:T(8,128)(2,1)}, u32[]{:S(2)}, u32[]{:S(2)}) collective-permute-start(bf16[1024,256]{1,0:T(8,128)(2,1)} %pad_maximum_fusion.7), channel_id=1, source_target_pairs={{0,12},{4,0},{8,4},{12,8},{1,13},{5,1},{9,5},{13,9},{2,14},{6,2},{... | collective-permute-start | bytes 1572872 | tf_op jit(solution)/shard_map/ppermute | solution.py:125
  100.7 21.3 %all-to-all-start.2 = ((bf16[4,710,256]{2,1,0:T(8,128)(2,1)}), bf16[4,710,256]{2,1,0:T(8,128)(2,1)S(1)}, u32[]{:S(2)}, u32[]{:S(2)}) async-start(bf16[4,710,256]{2,1,0:T(8,128)(2,1)} %pad_maximum_fusion.4), calls=%async_computation.2 | async-start | bytes 2916352 | tf_op jit(solution)/shard_map/all_to_all | solution.py:120
  122.2 5.5 %copy-start.2 = (bf16[1,1024,256]{2,1,0:T(8,128)(2,1)S(1)}, bf16[1,1024,256]{2,1,0:T(8,128)(2,1)}, u32[]{:S(2)}) copy-start(bf16[1,1024,256]{2,1,0:T(8,128)(2,1)} %get-tuple-element.11) | copy-start | bytes 1572868
  123.4 22.7 %all-to-all-start.3 = ((bf16[4,704,128]{2,1,0:T(8,128)(2,1)}), bf16[4,704,128]{2,1,0:T(8,128)(2,1)}, u32[]{:S(2)}, u32[]{:S(2)}) async-start(bf16[4,704,128]{2,1,0:T(8,128)(2,1)} %broadcast_in_dim.14), calls=%async_computation.3 | async-start | bytes 1441792 | tf_op jit(solution)/shard_map/all_to_all | solution.py:116
  128.2 1.6 copy-start.1
  135.5 18.0 %collective-permute-start.3 = (bf16[256,128]{1,0:T(8,128)(2,1)S(1)}, bf16[256,128]{1,0:T(8,128)(2,1)S(1)}, u32[]{:S(2)}, u32[]{:S(2)}) collective-permute-start(bf16[256,128]{1,0:T(8,128)(2,1)S(1)} %attend.1), channel_id=1, source_target_pairs={{0,1},{1,2},{2,3},{3,0},{4,5},{5,6},{6,7},{7,4},{8,9},{9,10},{10,1... | collective-permute-start | bytes 196616 | tf_op jit(solution)/shard_map/ppermute | solution.py:125
  138.7 14.8 %collective-permute-start.4 = (bf16[256,128]{1,0:T(8,128)(2,1)S(1)}, bf16[256,128]{1,0:T(8,128)(2,1)S(1)}, u32[]{:S(2)}, u32[]{:S(2)}) collective-permute-start(bf16[256,128]{1,0:T(8,128)(2,1)S(1)} %attend.1), channel_id=1, source_target_pairs={{0,2},{1,3},{2,0},{3,1},{4,6},{5,7},{6,4},{7,5},{8,10},{9,11},{10,... | collective-permute-start | bytes 196616 | tf_op jit(solution)/shard_map/ppermute | solution.py:125
  143.0 10.5 %collective-permute-start.5 = (bf16[256,128]{1,0:T(8,128)(2,1)S(1)}, bf16[256,128]{1,0:T(8,128)(2,1)S(1)}, u32[]{:S(2)}, u32[]{:S(2)}) collective-permute-start(bf16[256,128]{1,0:T(8,128)(2,1)S(1)} %attend.1), channel_id=1, source_target_pairs={{0,3},{1,0},{2,1},{3,2},{4,7},{5,4},{6,5},{7,6},{8,11},{9,8},{10,9... | collective-permute-start | bytes 196616 | tf_op jit(solution)/shard_map/ppermute | solution.py:125
  149.2 18.8 %all-to-all-start.4 = ((bf16[4,704,256]{2,1,0:T(8,128)(2,1)}), bf16[4,704,256]{2,1,0:T(8,128)(2,1)S(1)}, u32[]{:S(2)}, u32[]{:S(2)}) async-start(bf16[4,704,256]{2,1,0:T(8,128)(2,1)} %fusion.3), calls=%async_computation.4 | async-start | bytes 2883584 | tf_op jit(solution)/shard_map/all_to_all | solution.py:120
  154.2 26.8 %copy-start.13 = (f32[256,2]{0,1:T(2,128)S(1)}, f32[256,2]{0,1:T(2,128)}, u32[]{:S(2)}) copy-start(f32[256,2]{0,1:T(2,128)} %param.24) | copy-start | bytes 6148
  154.3 33.5 %collective-permute-start.8 = (bf16[258,256]{1,0:T(8,128)(2,1)S(1)}, bf16[258,256]{1,0:T(8,128)(2,1)S(1)}, u32[]{:S(2)}, u32[]{:S(2)}) collective-permute-start(bf16[258,256]{1,0:T(8,128)(2,1)S(1)} %get-tuple-element.31), channel_id=1, source_target_pairs={{0,12},{4,0},{8,4},{12,8},{1,13},{5,1},{9,5},{13,9},{2,14},{6,2},{... | collective-permute-start | bytes 396296 | tf_op jit(solution)/shard_map/ppermute | solution.py:125
  169.3 39.4 %all-to-all-start.5 = ((bf16[32,22,256]{2,1,0:T(8,128)(2,1)}), bf16[32,22,256]{2,1,0:T(8,128)(2,1)S(1)}, u32[]{:S(2)}, u32[]{:S(2)}) async-start(bf16[32,22,256]{2,1,0:T(8,128)(2,1)} %reshape.451), calls=%async_computation.5 | async-start | bytes 786432 | tf_op jit(solution)/shard_map/all_to_all | solution.py:120
  181.0 8.3 %collective-permute-start.7 = (bf16[258,256]{1,0:T(8,128)(2,1)S(1)}, bf16[258,256]{1,0:T(8,128)(2,1)S(1)}, u32[]{:S(2)}, u32[]{:S(2)}) collective-permute-start(bf16[258,256]{1,0:T(8,128)(2,1)S(1)} %get-tuple-element.30), channel_id=1, source_target_pairs={{0,8},{4,12},{8,0},{12,4},{1,9},{5,13},{9,1},{13,5},{2,10},{6,14},... | collective-permute-start | bytes 396296 | tf_op jit(solution)/shard_map/ppermute | solution.py:125
  183.2 9.2 %collective-permute-start.6 = (bf16[258,256]{1,0:T(8,128)(2,1)S(1)}, bf16[258,256]{1,0:T(8,128)(2,1)S(1)}, u32[]{:S(2)}, u32[]{:S(2)}) collective-permute-start(bf16[258,256]{1,0:T(8,128)(2,1)S(1)} %get-tuple-element.29), channel_id=1, source_target_pairs={{0,4},{4,8},{8,12},{12,0},{1,5},{5,9},{9,13},{13,1},{2,6},{6,10},{... | collective-permute-start | bytes 396296 | tf_op jit(solution)/shard_map/ppermute | solution.py:125
Sparse Core Ops, SparseCore 0:
  56.0 68.7 all-gather.2

commit v3 on v2

--- a/solution.py
+++ b/solution.py
@@ -1,3 +1,5 @@
+import functools
+
 import jax
 import jax.numpy as jnp
 from jax import lax
@@ -15,6 +17,7 @@
 TP = ("y", "x")
 SIDE = 4
 CAP = 22
+STAT_ROWS = 16
 KEY_STEP = 2048
 
 F32 = jnp.float32
@@ -25,33 +28,44 @@
     half_width = HEAD // 2
     inverse = THETA ** (-jnp.arange(0, half_width, 2, dtype=F32) / half_width)
     positions = offset + jnp.arange(length, dtype=jnp.int32)
-    grid_rows = (positions // GRID_W).astype(F32)
-    grid_cols = (positions % GRID_W).astype(F32)
-    angles = jnp.concatenate([grid_rows[:, None] * inverse, grid_cols[:, None] * inverse], axis=-1)
-    return (jnp.cos(angles), jnp.sin(angles))
-
-
-def norm_turn(source, scale_gain, cosine_table, sine_table):
-    length = source.shape[0]
-    head_rows = source.astype(F32).reshape(length, -1, HEAD)
-    head_rows = (
-        head_rows
-        * lax.rsqrt(jnp.mean(head_rows * head_rows, axis=-1, keepdims=True) + EPS)
-        * scale_gain
-    )
-    pair_view = head_rows.reshape(length, head_rows.shape[1], HEAD // 2, 2)
-    even_part = pair_view[..., 0]
-    odd_part = pair_view[..., 1]
-    cosine_part = cosine_table[:, None, :]
-    sine_part = sine_table[:, None, :]
-    turned = jnp.stack(
-        [
-            even_part * cosine_part - odd_part * sine_part,
-            even_part * sine_part + odd_part * cosine_part,
-        ],
-        axis=-1,
-    )
-    return turned.reshape(length, -1).astype(BF16)
+    lane = jnp.arange(2 * HEAD, dtype=jnp.int32) % HEAD
+    grid_rows = (positions // GRID_W).astype(F32)[:, None]
+    grid_cols = (positions % GRID_W).astype(F32)[:, None]
+    step = jnp.tile(jnp.repeat(jnp.concatenate([inverse, inverse]), 2), 2)
+    angles = jnp.where(lane < half_width, grid_rows, grid_cols) * step
+    sign = jnp.where(lane % 2 == 0, -1.0, 1.0)
+    return jnp.cos(angles), jnp.sin(angles) * sign
+
+
+def turn_body(q_ref, kv_ref, q_gain_ref, k_gain_ref, cos_ref, sin_ref, q_out, kv_out):
+    shape = q_ref.shape
+    lane = lax.broadcasted_iota(jnp.int32, shape, 1)
+    low = lane < HEAD
+    even = lane % 2 == 0
+
+    def turned(rows, gain):
+        squares = rows * rows
+        first = jnp.sum(jnp.where(low, squares, 0.0), axis=1, keepdims=True) / HEAD
+        second = jnp.sum(jnp.where(low, 0.0, squares), axis=1, keepdims=True) / HEAD
+        gain = jnp.concatenate([gain, gain], axis=1)
+        rows = rows * jnp.where(low, lax.rsqrt(first + EPS), lax.rsqrt(second + EPS)) * gain
+        swapped = jnp.where(even, pltpu.roll(rows, 2 * HEAD - 1, 1), pltpu.roll(rows, 1, 1))
+        return (rows * cos_ref[...] + swapped * sin_ref[...]).astype(BF16)
+
+    q_out[...] = turned(q_ref[...].astype(F32), q_gain_ref[...])
+    both = kv_ref[...]
+    kv_out[...] = jnp.where(low, turned(both.astype(F32), k_gain_ref[...]), both)
+
+
+def turn(queries, key_value, query_gain, key_gain, tables):
+    shape = jax.ShapeDtypeStruct(queries.shape, BF16)
+    return pl.pallas_call(turn_body, out_shape=[shape, shape], name="turn")(
+        queries,
+        key_value,
+        query_gain[None, :],
+        key_gain[None, :],
+        *tables,
+    )
 
 
 def attend_body(q_ref, kv_ref, out_ref):
@@ -94,26 +108,113 @@
     )(query_turned, key_value)
 
 
-def two_parts(value):
-    high = lax.reduce_precision(value, 8, 7)
-    return high.astype(BF16), (value - high).astype(BF16)
-
-
-def stat_rows(sums, count):
-    width = 256
-    flat = jnp.pad(sums, (0, count * width - sums.shape[0])).reshape(count, width)
-    high, low = two_parts(flat)
-    return jnp.concatenate([high, low], axis=0)
+def mix_body(k_rows, base, joined, index_ref, *refs):
+    if joined:
+        pieces, refs = [refs[0].at[q] for q in range(SIDE)], refs[1:]
+        outs = [refs[-1].at[index_ref[2 * SIDE + r]] for r in range(SIDE)]
+    else:
+        pieces, outs, refs = refs[:SIDE], refs[-SIDE:], refs[SIDE:]
+    weights, gain_ref = refs[:SIDE], refs[SIDE]
+    rows = pieces[0].shape[0]
+    scaled = [
+        (pieces[q][...].astype(F32) * gain_ref[pl.ds(index_ref[SIDE + q], 1), :]).astype(BF16)
+        for q in range(SIDE)
+    ]
+    for r in range(SIDE):
+        total = jnp.zeros((rows, weights[r].shape[1]), F32)
+        for q in range(SIDE):
+            block = weights[r][pl.ds(pl.multiple_of(base + index_ref[q] * k_rows, 128), k_rows), :]
+            total += jnp.dot(scaled[q], block, preferred_element_type=F32)
+        outs[r][:rows, :] = total.astype(BF16)
+    squares = jnp.zeros((rows, k_rows), F32)
+    for q in range(SIDE):
+        values = pieces[q][...].astype(F32)
+        squares += values * values
+    high = squares.astype(BF16)
+    low = (squares - high.astype(F32)).astype(BF16)
+    ones = jnp.ones((8, k_rows), BF16)
+    sums = jnp.zeros((8, rows), F32)
+    for part in (high, low):
+        sums += lax.dot_general(ones, part, (((1,), (1,)), ((), ())), preferred_element_type=F32)
+    width = outs[0].shape[1]
+    count = -(-rows // width)
+    if count * width > rows:
+        sums = jnp.concatenate([sums, jnp.zeros((8, count * width - rows), F32)], axis=1)
+    line = lax.broadcasted_iota(jnp.int32, (STAT_ROWS, width), 0)
+    block = jnp.zeros((STAT_ROWS, width), F32)
+    for j in range(count):
+        value = sums[0:1, j * width : (j + 1) * width]
+        high = value.astype(BF16).astype(F32)
+        block = jnp.where(line == j, high, block)
+        block = jnp.where(line == count + j, value - high, block)
+    for r in range(SIDE):
+        outs[r][rows:, :] = block.astype(BF16)
+
+
+def mix(pieces, weights, base, gains, indices):
+    joined = not isinstance(pieces, list)
+    rows, k_rows = pieces[0].shape
+    width = weights[0].shape[1]
+    vmem = pl.BlockSpec(memory_space=pltpu.VMEM)
+    shape = (rows + STAT_ROWS, width)
+    given = [pieces] if joined else pieces
+    return pl.pallas_call(
+        functools.partial(mix_body, k_rows, base, joined),
+        out_shape=jax.ShapeDtypeStruct((SIDE,) + shape, BF16)
+        if joined
+        else [jax.ShapeDtypeStruct(shape, BF16)] * SIDE,
+        in_specs=[pl.BlockSpec(memory_space=pltpu.SMEM)] + [vmem] * (len(given) + SIDE + 1),
+        out_specs=vmem if joined else [vmem] * SIDE,
+        compiler_params=pltpu.CompilerParams(vmem_limit_bytes=48 * 1024 * 1024),
+        cost_estimate=pl.CostEstimate(
+            flops=2 * SIDE * SIDE * rows * k_rows * width,
+            bytes_accessed=SIDE * rows * (k_rows + width) * 2,
+            transcendentals=0,
+        ),
+    )(jnp.concatenate(indices), *given, *weights, gains)
+
+
+def hidden_body(features, in_ref, out_ref):
+    rows = out_ref.shape[1]
+    hid = out_ref.shape[2]
+    width = 2 * hid
+    count = -(-rows // width)
+    stats = sum(in_ref[k, rows:, :].astype(F32) for k in range(SIDE))
+    for j in range(count):
+        first, last = j * width, min(rows, (j + 1) * width)
+        line = stats[j : j + 1, :] + stats[count + j : count + j + 1, :]
+        scale = lax.rsqrt(line / features + EPS)
+        column = jnp.transpose(jnp.broadcast_to(scale, (8, width)))[: last - first, 0:1]
+        sums = sum(in_ref[k, first:last, :].astype(F32) for k in range(SIDE))
+        gate = sums[:, :hid] * column
+        up = sums[:, hid:] * column
+        result = (gate / (1.0 + jnp.exp(-gate)) * up).astype(BF16)
+        for k in range(SIDE):
+            out_ref[k, first:last, :] = result
+
+
+def second_body(index_ref, gathered, *refs):
+    weights, out_ref = refs[:SIDE], refs[-1]
+    hid = gathered.shape[2]
+    wide = jnp.concatenate([gathered[k] for k in range(SIDE)], axis=1)
+    for r in range(SIDE):
+        out_ref[index_ref[r]] = jnp.dot(
+            wide, weights[r][: SIDE * hid, :], preferred_element_type=F32
+        ).astype(BF16)
 
 
 def read_stat(rows, count, size):
     whole = rows.astype(F32)
-    return jnp.sum(whole[:, :count] + whole[:, count:], axis=0).reshape(-1)[:size]
+    return jnp.sum(whole[:, :count] + whole[:, count : 2 * count], axis=0).reshape(-1)[:size]
+
+
+def send_back(parts, axis):
+    return [parts[0]] + [shift(parts[r], axis, SIDE - r) for r in range(1, SIDE)]
 
 
 def copies_to(array, axis):
     wide = jnp.broadcast_to(array[None], (SIDE,) + array.shape)
-    return lax.all_to_all(wide, axis, 0, 0, tiled=True)
+    return swap(wide, axis)
 
 
 def swap(array, axis):
@@ -130,16 +231,7 @@
     landed = [chunk_for(place)]
     for by in range(1, SIDE):
         landed.append(shift(chunk_for((place + by) % SIDE), axis, by))
-    return in_order(jnp.stack(landed), place)
-
-
-def in_order(landed, place):
-    return jnp.stack(
-        [
-            lax.dynamic_index_in_dim(landed, (place - k) % SIDE, 0, keepdims=False)
-            for k in range(SIDE)
-        ]
-    )
+    return landed
 
 
 def forward(
@@ -167,12 +259,12 @@
     piece = expert_input.shape[1]
     hid = expert_gate.shape[2]
 
-    cosine_table, sine_table = turn_tables(lax.axis_index(EP) * length, length)
-    key_turned = norm_turn(key_rows, key_gain, cosine_table, sine_table)
-    key_value = jnp.concatenate([key_turned, values], axis=1)
-    key_value = lax.all_gather(key_value, EP, axis=0, tiled=False)
+    tables = turn_tables(lax.axis_index(EP) * length, length)
+    query_turned, own_rows = turn(
+        queries, jnp.concatenate([key_rows, values], axis=1), query_gain, key_gain, tables
+    )
+    key_value = lax.all_gather(own_rows, EP, axis=0, tiled=False)
     key_value = key_value.reshape(experts_count * length, 2 * HEAD)
-    query_turned = norm_turn(queries, query_gain, cosine_table, sine_table)
 
     copies = length * 2
     flat_ids = route_ids.reshape(copies)
@@ -205,59 +297,47 @@
     first_weights = deal(first_chunk, "x")
     second_weights = deal(second_chunk, "y")
 
-    gathered = copies_to(arrived, "y")
-    gains = lax.dynamic_index_in_dim(
-        expert_gain.reshape(SIDE, SIDE, piece), place_x, axis=1, keepdims=False
-    )
-    gathered_float = gathered.astype(F32)
-    scaled = (gathered_float * gains[:, None, :]).astype(BF16)
-    squares = jnp.sum(gathered_float * gathered_float, axis=(0, 2))
-    partial = jnp.einsum(
-        "ysf,xyfh->xsh",
-        scaled,
-        first_weights.reshape(SIDE, SIDE, piece, 2 * hid),
-        preferred_element_type=F32,
-    ).astype(BF16)
-    stat_count = -(-slot_total // piece)
-    stats = jnp.broadcast_to(stat_rows(squares, stat_count)[None], (SIDE, 2 * stat_count, piece))
-    received = swap(jnp.concatenate([partial, stats], axis=1), "x")
-    sums = jnp.sum(received[:, :slot_total].astype(F32), axis=0)
-    square_sum = read_stat(received[:, slot_total:], stat_count, slot_total)
-    row_stat = lax.rsqrt(square_sum / features + EPS)
-    gate_value = sums[:, :hid] * row_stat[:, None]
-    up_value = sums[:, hid:] * row_stat[:, None]
-    hidden = (jax.nn.silu(gate_value) * up_value).astype(BF16)
-
-    hidden_all = copies_to(hidden, "x")
-    down_rows = second_weights[:, : SIDE * hid].reshape(SIDE, SIDE, hid, piece)
-    out_rows = second_weights[:, SIDE * hid :].reshape(SIDE, SIDE, 2 * HEAD, piece)
-    expert_partial = jnp.einsum(
-        "xsh,yxhf->ysf", hidden_all, down_rows, preferred_element_type=F32
-    ).astype(BF16)
+    ahead = jnp.arange(SIDE, dtype=jnp.int32)
+    from_y = (place_y - ahead) % SIDE
+    from_x = (place_x - ahead) % SIDE
+    partial = mix(
+        copies_to(arrived, "y"),
+        first_weights,
+        0,
+        expert_gain.reshape(SIDE * SIDE, piece),
+        (ahead, ahead * SIDE + place_x, from_x),
+    )
+    sums = swap(partial, "x")
+    hidden = pl.pallas_call(
+        functools.partial(hidden_body, features),
+        out_shape=jax.ShapeDtypeStruct((SIDE, slot_total, hid), BF16),
+        compiler_params=pltpu.CompilerParams(vmem_limit_bytes=48 * 1024 * 1024),
+        name="hidden",
+    )(sums)
+
+    hidden_all = swap(hidden, "x")
+    vmem = pl.BlockSpec(memory_space=pltpu.VMEM)
+    expert_partial = pl.pallas_call(
+        second_body,
+        out_shape=jax.ShapeDtypeStruct((SIDE, slot_total, piece), BF16),
+        in_specs=[pl.BlockSpec(memory_space=pltpu.SMEM)] + [vmem] * (1 + SIDE),
+        out_specs=vmem,
+        compiler_params=pltpu.CompilerParams(vmem_limit_bytes=48 * 1024 * 1024),
+        name="second",
+    )(from_y, hidden_all, *second_weights)
     landed = swap(expert_partial, "y")
     expert_out = jnp.sum(landed.astype(F32), axis=0).astype(BF16)
 
     heads_out = attend(query_turned, key_value)
-    near = jnp.stack([heads_out] + [shift(heads_out, "x", by) for by in range(1, SIDE)])
-    heads = in_order(near, place_x)
-    head_float = heads.astype(F32)
-    mix_gains = lax.dynamic_index_in_dim(
-        mix_gain.reshape(SIDE, SIDE, 2 * HEAD), place_y, axis=0, keepdims=False
-    )
-    mix_in = (head_float * mix_gains[:, None, :]).astype(BF16)
-    mix_squares = jnp.sum(head_float * head_float, axis=(0, 2))
-    mix_partial = jnp.einsum(
-        "xsh,yxhf->ysf", mix_in, out_rows, preferred_element_type=F32
-    ).astype(BF16)
-    mix_stats = jnp.broadcast_to(stat_rows(mix_squares, 1)[None], (SIDE, 2, piece))
-    payload = jnp.concatenate([mix_partial, mix_stats], axis=1)
-
-    def payload_of(k):
-        return lax.dynamic_index_in_dim(payload, k, 0, keepdims=False)
-
-    parts = [payload_of(place_y)] + [
-        shift(payload_of((place_y + by) % SIDE), "y", by) for by in range(1, SIDE)
-    ]
+    heads = [heads_out] + [shift(heads_out, "x", by) for by in range(1, SIDE)]
+    mix_partial = mix(
+        heads,
+        second_weights,
+        SIDE * hid,
+        mix_gain.reshape(SIDE * SIDE, 2 * HEAD),
+        (from_x, place_y * SIDE + from_x),
+    )
+    parts = send_back(mix_partial, "y")
     mix_sum = sum(part[:length].astype(F32) for part in parts)
     mix_square_sum = read_stat(jnp.stack([part[length:] for part in parts]), 1, length)
     mix_scale = lax.rsqrt(mix_square_sum / mix_gain.shape[0] + EPS)

time: 218 us -> 214 us (0.982)
  Pallas kernels: 5.69 us -> 17.1 us
  matrix products: 8.41 us -> 1.56 us
  starting transfers between devices: 89.6 us -> 83.1 us
  waiting for transfers between devices: 68.6 us -> 71.4 us
  other arithmetic: 16.6 us -> 14.1 us
    ppermute x12, waiting for transfers between devices: 5.12 us -> 29.2 us  [shift(): lax.ppermute(array, axis, [(k, (k + by) % size) for k in range(size)])]
    all_to_all x4 -> x6, waiting for transfers between devices: 54.2 us -> 42.1 us  [swap(): return lax.all_to_all(array, axis, 0, 0, tiled=True)]
    pallas_call x0 -> x5, Pallas kernels: none -> 11.4 us  [the longest x2 5.28 us: mix(): pl.pallas_call(functools.partial(mix_body, k_rows, base, joined), out_sha...]
    all_to_all x2 -> x0, waiting for transfers between devices: 9.21 us -> none  [copies_to(): return lax.all_to_all(wide, axis, 0, 0, tiled=True)]
    all_to_all x2 -> x0, starting transfers between devices: 8.69 us -> none  [copies_to(): return lax.all_to_all(wide, axis, 0, 0, tiled=True)]
    dot_general x3 -> x0, matrix products: 6.85 us -> none  [the longest x1 3.25 us: forward(): jnp.einsum('ysf,xyfh->xsh', scaled, first_weights.reshape(SIDE, SIDE, pie...]
    another operation x12 -> x2, other arithmetic: 6.72 us -> 1.2 us  [the longest x3 3.17 us: deal(): return in_order(jnp.stack(landed), place)]
    all_to_all x4 -> x6, starting transfers between devices: 35.5 us -> 40.9 us  [swap(): return lax.all_to_all(array, axis, 0, 0, tiled=True)]
  transfers between devices with their start and end apart: 19 -> 19, of which waited for: 8 -> 10; matrix products, arithmetic and copies ran while one was open for 14% -> 9% of each run, Pallas kernels for 3% -> 8%
where the time goes in v3:
time: 214 us; the launch traced here: 213 us
  starting transfers between devices  83.1 us (39%)
  waiting for transfers between devices  71.4 us (33%)
  Pallas kernels  17.1 us (8%)
  between operations  14.5 us (7%)
  other arithmetic  14.1 us (7%)
  local copies, waits for them, and re-layouts  11 us (5%)
    ppermute x12, starting transfers between devices, shift(): lax.ppermute(array, axis, [(k, (k + by) % size) for k in range(size)])  42.2 us
    all_to_all x6, waiting for transfers between devices, swap(): return lax.all_to_all(array, axis, 0, 0, tiled=True)  42.1 us
    all_to_all x6, starting transfers between devices, swap(): return lax.all_to_all(array, axis, 0, 0, tiled=True)  40.9 us
    ppermute x12, waiting for transfers between devices, shift(): lax.ppermute(array, axis, [(k, (k + by) % size) for k in range(size)])  29.2 us
    pallas_call x1, Pallas kernels, attend(): pl.pallas_call(attend_body, out_shape=jax.ShapeDtypeStruct(query_turned.s...  5.69 us
    pallas_call x2, Pallas kernels, mix(): pl.pallas_call(functools.partial(mix_body, k_rows, base, joined), out_sha...  5.28 us
  transfers between devices with their start and end apart: 19, of which 10 were waited for; matrix products, arithmetic and copies ran while one was open for 9% of the time, Pallas kernels for 8%

profile of v3, /device:TPU:1, one launch (start us, length us, event | category | flops | bytes accessed | tf_op | source)
XLA Modules:
  0.0 212.7 jit_solution(8588705563362630007)
XLA Ops:
  7.2 0.8 copy.58
  8.0 0.1 eq.109
  8.2 0.1 eq.105
  8.3 1.2 reduce-window.6
  9.5 0.2 slice_reduce_fusion
  9.9 0.1 reduce_sum.34
  10.1 0.7 multiply_add_fusion
  10.8 0.3 convolution_convert_fusion
  11.1 0.9 reshape.144
  12.0 16.7 %all-to-all-start = ((bf16[32,22,256]{2,1,0:T(8,128)(2,1)}), bf16[32,22,256]{2,1,0:T(8,128)(2,1)S(1)}, u32[]{:S(2)}, u32[]{:S(2)}) async-start(bf16[32,22,256]{2,1,0:T(8,128)(2,1)} %reshape.144), calls=%async_computation | async-start | bytes 786432 | tf_op jit(solution)/shard_map/all_to_all | solution.py:221
  29.4 0.7 pad_maximum_fusion.8.kv_ref
  30.1 1.3 sine_multiply_fusion
  31.4 2.2 %turn.1 = (bf16[256,128]{1,0:T(8,128)(2,1)}, bf16[256,128]{1,0:T(8,128)(2,1)}) custom-call(bf16[256,128]{1,0:T(8,128)(2,1)} %q_ref.1, bf16[256,128]{1,0:T(8,128)(2,1)} %pad_maximum_fusion.8.kv_ref, f32[1,64]{1,0:T(1,128)} %bitcast.88, f32[1,64]{1,0:T(1,128)} %bitcast.89, f32[256,128]{1,0:T(8,128)} %get-tuple-element.31.cos_ref, ...), custom_call_target="tpu_custom_call" | custom-call | tf_op jit(solution)/shard_map/turn/pallas_call | solution.py:62
  33.6 22.8 %all-to-all-done = bf16[32,22,256]{2,1,0:T(8,128)(2,1)S(1)} async-done(((bf16[32,22,256]{2,1,0:T(8,128)(2,1)}), bf16[32,22,256]{2,1,0:T(8,128)(2,1)S(1)}, u32[]{:S(2)}, u32[]{:S(2)}) %all-to-all-start) | async-done | bytes 360480 | tf_op jit(solution)/shard_map/all_to_all | solution.py:221
  56.6 1.2 broadcast_in_dim.61
  57.8 4.3 %all-to-all-start.1 = ((bf16[4,704,256]{2,1,0:T(8,128)(2,1)}), bf16[4,704,256]{2,1,0:T(8,128)(2,1)S(1)}, u32[]{:S(2)}, u32[]{:S(2)}) async-start(bf16[4,704,256]{2,1,0:T(8,128)(2,1)} %broadcast_in_dim.61), calls=%async_computation.1 | async-start | bytes 2883584 | tf_op jit(solution)/shard_map/all_to_all | solution.py:221
  62.1 2.1 constant_dynamic-slice_fusion
  64.1 0.8 pad_maximum_fusion.6
  65.0 4.6 %collective-permute-start.10 = (bf16[1024,256]{1,0:T(8,128)(2,1)}, bf16[1024,256]{1,0:T(8,128)(2,1)S(1)}, u32[]{:S(2)}, u32[]{:S(2)}) collective-permute-start(bf16[1024,256]{1,0:T(8,128)(2,1)} %pad_maximum_fusion.6), channel_id=1, source_target_pairs={{0,2},{1,3},{2,0},{3,1},{4,6},{5,7},{6,4},{7,5},{8,10},{9,11},{10,... | collective-permute-start | bytes 1572872 | tf_op jit(solution)/shard_map/ppermute | solution.py:226
  69.6 0.9 pad_maximum_fusion.7
  70.5 2.8 %collective-permute-start.11 = (bf16[1024,256]{1,0:T(8,128)(2,1)}, bf16[1024,256]{1,0:T(8,128)(2,1)S(1)}, u32[]{:S(2)}, u32[]{:S(2)}) collective-permute-start(bf16[1024,256]{1,0:T(8,128)(2,1)} %pad_maximum_fusion.7), channel_id=1, source_target_pairs={{0,3},{1,0},{2,1},{3,2},{4,7},{5,4},{6,5},{7,6},{8,11},{9,8},{10,9... | collective-permute-start | bytes 1572872 | tf_op jit(solution)/shard_map/ppermute | solution.py:226
  73.2 0.9 pad_maximum_fusion.5
  74.1 2.5 %collective-permute-start.9 = (bf16[1024,256]{1,0:T(8,128)(2,1)}, bf16[1024,256]{1,0:T(8,128)(2,1)}, u32[]{:S(2)}, u32[]{:S(2)}) collective-permute-start(bf16[1024,256]{1,0:T(8,128)(2,1)} %pad_maximum_fusion.5), channel_id=1, source_target_pairs={{0,1},{1,2},{2,3},{3,0},{4,5},{5,6},{6,7},{7,4},{8,9},{9,10},{10,1... | collective-permute-start | bytes 1572872 | tf_op jit(solution)/shard_map/ppermute | solution.py:226
  76.7 1.0 pad_maximum_fusion.4.refs_1_
  77.8 3.3 %collective-permute-done.10.refs_3_ = bf16[1024,256]{1,0:T(8,128)(2,1)S(1)} collective-permute-done((bf16[1024,256]{1,0:T(8,128)(2,1)}, bf16[1024,256]{1,0:T(8,128)(2,1)S(1)}, u32[]{:S(2)}, u32[]{:S(2)}) %collective-permute-start.10) | collective-permute-done | bytes 524320 | tf_op jit(solution)/shard_map/ppermute | solution.py:226
  81.1 11.7 %collective-permute-done.11.refs_4_ = bf16[1024,256]{1,0:T(8,128)(2,1)S(1)} collective-permute-done((bf16[1024,256]{1,0:T(8,128)(2,1)}, bf16[1024,256]{1,0:T(8,128)(2,1)S(1)}, u32[]{:S(2)}, u32[]{:S(2)}) %collective-permute-start.11) | collective-permute-done | bytes 524320 | tf_op jit(solution)/shard_map/ppermute | solution.py:226
  92.8 0.5 collective-permute-done.9.refs_2_
  93.3 4.0 %shard_map.150 = bf16[4,720,256]{2,1,0:T(8,128)(2,1)} custom-call(s32[12]{0:T(128)S(1)} %pad_add_fusion.1.index_ref, bf16[4,704,256]{2,1,0:T(8,128)(2,1)S(1)} %all-to-all-done.1.refs_0_, bf16[1024,256]{1,0:T(8,128)(2,1)S(1)} %pad_maximum_fusion.4.refs_1_, bf16[1024,256]{1,0:T(8,128)(2,1)} %collective-permute-done.9.refs_2_, ...), custom_call_target="tpu_custom_call" | custom-call | flops 1476395008 | bytes 2883584 | tf_op jit(solution)/shard_map/pallas_call | solution.py:161
  97.4 4.6 %all-to-all-start.2 = ((bf16[4,720,256]{2,1,0:T(8,128)(2,1)}), bf16[4,720,256]{2,1,0:T(8,128)(2,1)S(1)}, u32[]{:S(2)}, u32[]{:S(2)}) async-start(bf16[4,720,256]{2,1,0:T(8,128)(2,1)} %shard_map.150), calls=%async_computation.2 | async-start | bytes 2949120 | tf_op jit(solution)/shard_map/all_to_all | solution.py:221
  102.0 0.8 dynamic-slice_bitcast_fusion
  102.7 0.6 copy-done.5
  103.3 0.9 constant_dynamic-slice_fusion.8
  104.1 0.8 pad_maximum_fusion.2
  104.9 4.9 %collective-permute-start.4 = (bf16[1024,256]{1,0:T(8,128)(2,1)}, bf16[1024,256]{1,0:T(8,128)(2,1)S(1)}, u32[]{:S(2)}, u32[]{:S(2)}) collective-permute-start(bf16[1024,256]{1,0:T(8,128)(2,1)} %pad_maximum_fusion.2), channel_id=1, source_target_pairs={{0,8},{4,12},{8,0},{12,4},{1,9},{5,13},{9,1},{13,5},{2,10},{6,14},... | collective-permute-start | bytes 1572872 | tf_op jit(solution)/shard_map/ppermute | solution.py:226
  109.8 0.8 pad_maximum_fusion.3
  110.7 2.8 %collective-permute-start.5 = (bf16[1024,256]{1,0:T(8,128)(2,1)}, bf16[1024,256]{1,0:T(8,128)(2,1)S(1)}, u32[]{:S(2)}, u32[]{:S(2)}) collective-permute-start(bf16[1024,256]{1,0:T(8,128)(2,1)} %pad_maximum_fusion.3), channel_id=1, source_target_pairs={{0,12},{4,0},{8,4},{12,8},{1,13},{5,1},{9,5},{13,9},{2,14},{6,2},{... | collective-permute-start | bytes 1572872 | tf_op jit(solution)/shard_map/ppermute | solution.py:226
  113.4 7.5 %all-to-all-done.2.in_ref = bf16[4,720,256]{2,1,0:T(8,128)(2,1)S(1)} async-done(((bf16[4,720,256]{2,1,0:T(8,128)(2,1)}), bf16[4,720,256]{2,1,0:T(8,128)(2,1)S(1)}, u32[]{:S(2)}, u32[]{:S(2)}) %all-to-all-start.2) | async-done | bytes 1474592 | tf_op jit(solution)/shard_map/all_to_all | solution.py:221
  120.9 1.3 hidden.1
  122.2 3.5 %all-to-all-start.3 = ((bf16[4,704,128]{2,1,0:T(8,128)(2,1)}), bf16[4,704,128]{2,1,0:T(8,128)(2,1)S(1)}, u32[]{:S(2)}, u32[]{:S(2)}) async-start(bf16[4,704,128]{2,1,0:T(8,128)(2,1)} %hidden.1), calls=%async_computation.3 | async-start | bytes 1441792 | tf_op jit(solution)/shard_map/all_to_all | solution.py:221
  125.7 1.1 pad_maximum_fusion.1
  126.8 3.4 %collective-permute-start.3 = (bf16[1024,256]{1,0:T(8,128)(2,1)S(1)}, bf16[1024,256]{1,0:T(8,128)(2,1)S(1)}, u32[]{:S(2)}, u32[]{:S(2)}) collective-permute-start(bf16[1024,256]{1,0:T(8,128)(2,1)S(1)} %pad_maximum_fusion.1), channel_id=1, source_target_pairs={{0,4},{4,8},{8,12},{12,0},{1,5},{5,9},{9,13},{13,1},{2,6},{6,10},{... | collective-permute-start | bytes 1572872 | tf_op jit(solution)/shard_map/ppermute | solution.py:226
  130.2 1.0 pad_maximum_fusion.refs_4_.refs_0_
  131.2 1.8 collective-permute-done.5.refs_7_.refs_3_
  133.0 8.8 %collective-permute-done.3.refs_5_.refs_1_ = bf16[1024,256]{1,0:T(8,128)(2,1)S(1)} collective-permute-done((bf16[1024,256]{1,0:T(8,128)(2,1)S(1)}, bf16[1024,256]{1,0:T(8,128)(2,1)S(1)}, u32[]{:S(2)}, u32[]{:S(2)}) %collective-permute-start.3) | collective-permute-done | bytes 524320 | tf_op jit(solution)/shard_map/ppermute | solution.py:226
  141.8 2.6 %second.1 = bf16[4,704,256]{2,1,0:T(8,128)(2,1)} custom-call(s32[4]{0:T(128)S(1)} %and_select_fusion.index_ref, bf16[4,704,128]{2,1,0:T(8,128)(2,1)S(1)} %all-to-all-done.3.gathered, bf16[1024,256]{1,0:T(8,128)(2,1)S(1)} %pad_maximum_fusion.refs_4_.refs_0_, bf16[1024,256]{1,0:T(8,128)(2,1)S(1)} %collective-permute-done.3.refs_5_.refs_1_, ...), custom_call_target="tpu_custom_call" | custom-call | tf_op jit(solution)/shard_map/second/pallas_call | solution.py:320
  144.4 4.6 %all-to-all-start.4 = ((bf16[4,704,256]{2,1,0:T(8,128)(2,1)}), bf16[4,704,256]{2,1,0:T(8,128)(2,1)}, u32[]{:S(2)}, u32[]{:S(2)}) async-start(bf16[4,704,256]{2,1,0:T(8,128)(2,1)} %second.1), calls=%async_computation.4 | async-start | bytes 2883584 | tf_op jit(solution)/shard_map/all_to_all | solution.py:221
  149.1 1.6 copy-done.2
  150.7 5.7 %attend.1.refs_0_ = bf16[256,128]{1,0:T(8,128)(2,1)S(1)} custom-call(bf16[256,128]{1,0:T(8,128)(2,1)S(1)} %copy-done.3, bf16[8192,128]{1,0:T(8,128)(2,1)S(1)} %copy-done.2), custom_call_target="tpu_custom_call" | custom-call | flops 2147483648 | bytes 2097152 | tf_op jit(solution)/shard_map/attend/pallas_call | solution.py:98
  156.4 3.1 %collective-permute-start = (bf16[256,128]{1,0:T(8,128)(2,1)S(1)}, bf16[256,128]{1,0:T(8,128)(2,1)S(1)}, u32[]{:S(2)}, u32[]{:S(2)}) collective-permute-start(bf16[256,128]{1,0:T(8,128)(2,1)S(1)} %attend.1.refs_0_), channel_id=1, source_target_pairs={{0,1},{1,2},{2,3},{3,0},{4,5},{5,6},{6,7},{7,4},{8,9},{9,10},{10,1... | collective-permute-start | bytes 196616 | tf_op jit(solution)/shard_map/ppermute | solution.py:226
  159.5 4.3 %collective-permute-start.1 = (bf16[256,128]{1,0:T(8,128)(2,1)S(1)}, bf16[256,128]{1,0:T(8,128)(2,1)S(1)}, u32[]{:S(2)}, u32[]{:S(2)}) collective-permute-start(bf16[256,128]{1,0:T(8,128)(2,1)S(1)} %attend.1.refs_0_), channel_id=1, source_target_pairs={{0,2},{1,3},{2,0},{3,1},{4,6},{5,7},{6,4},{7,5},{8,10},{9,11},{10,... | collective-permute-start | bytes 196616 | tf_op jit(solution)/shard_map/ppermute | solution.py:226
  163.8 3.1 %collective-permute-start.2 = (bf16[256,128]{1,0:T(8,128)(2,1)S(1)}, bf16[256,128]{1,0:T(8,128)(2,1)S(1)}, u32[]{:S(2)}, u32[]{:S(2)}) collective-permute-start(bf16[256,128]{1,0:T(8,128)(2,1)S(1)} %attend.1.refs_0_), channel_id=1, source_target_pairs={{0,3},{1,0},{2,1},{3,2},{4,7},{5,4},{6,5},{7,6},{8,11},{9,8},{10,9... | collective-permute-start | bytes 196616 | tf_op jit(solution)/shard_map/ppermute | solution.py:226
  166.9 1.7 reduce_sum.35
  168.6 0.9 reshape.148
  169.5 7.1 %all-to-all-start.5 = ((bf16[32,22,256]{2,1,0:T(8,128)(2,1)}), bf16[32,22,256]{2,1,0:T(8,128)(2,1)S(1)}, u32[]{:S(2)}, u32[]{:S(2)}) async-start(bf16[32,22,256]{2,1,0:T(8,128)(2,1)} %reshape.148), calls=%async_computation.5 | async-start | bytes 786432 | tf_op jit(solution)/shard_map/all_to_all | solution.py:221
  176.7 1.2 shard_map.149
  178.0 3.4 %collective-permute-start.8 = (bf16[272,256]{1,0:T(8,128)(2,1)S(1)}, bf16[272,256]{1,0:T(8,128)(2,1)S(1)}, u32[]{:S(2)}, u32[]{:S(2)}) collective-permute-start(bf16[272,256]{1,0:T(8,128)(2,1)S(1)} %get-tuple-element.13), channel_id=1, source_target_pairs={{0,4},{4,8},{8,12},{12,0},{1,5},{5,9},{9,13},{13,1},{2,6},{6,10},{... | collective-permute-start | bytes 417800 | tf_op jit(solution)/shard_map/ppermute | solution.py:226
  181.4 4.3 %collective-permute-start.7 = (bf16[272,256]{1,0:T(8,128)(2,1)S(1)}, bf16[272,256]{1,0:T(8,128)(2,1)S(1)}, u32[]{:S(2)}, u32[]{:S(2)}) collective-permute-start(bf16[272,256]{1,0:T(8,128)(2,1)S(1)} %get-tuple-element.12), channel_id=1, source_target_pairs={{0,8},{4,12},{8,0},{12,4},{1,9},{5,13},{9,1},{13,5},{2,10},{6,14},... | collective-permute-start | bytes 417800 | tf_op jit(solution)/shard_map/ppermute | solution.py:226
  185.7 3.1 %collective-permute-start.6 = (bf16[272,256]{1,0:T(8,128)(2,1)S(1)}, bf16[272,256]{1,0:T(8,128)(2,1)S(1)}, u32[]{:S(2)}, u32[]{:S(2)}) collective-permute-start(bf16[272,256]{1,0:T(8,128)(2,1)S(1)} %get-tuple-element.11), channel_id=1, source_target_pairs={{0,12},{4,0},{8,4},{12,8},{1,13},{5,1},{9,5},{13,9},{2,14},{6,2},{... | collective-permute-start | bytes 417800 | tf_op jit(solution)/shard_map/ppermute | solution.py:226
  188.8 1.6 collective-permute-done.7
  190.4 1.5 collective-permute-done.6
  192.0 0.8 multiply_convert_fusion
  192.7 11.7 %all-to-all-done.5 = bf16[32,22,256]{2,1,0:T(8,128)(2,1)S(1)} async-done(((bf16[32,22,256]{2,1,0:T(8,128)(2,1)}), bf16[32,22,256]{2,1,0:T(8,128)(2,1)S(1)}, u32[]{:S(2)}, u32[]{:S(2)}) %all-to-all-start.5) | async-done | bytes 360480 | tf_op jit(solution)/shard_map/all_to_all | solution.py:221
  204.6 0.3 convolution_multiply_fusion.1
  204.9 1.0 fusion.1
  (65 shorter events, 1.4 us)
Async XLA Ops:
  7.2 3.7 %copy-start = (bf16[256,256]{1,0:T(8,128)(2,1)S(1)}, bf16[256,256]{1,0:T(8,128)(2,1)}, u32[]{:S(2)}) copy-start(bf16[256,256]{1,0:T(8,128)(2,1)} %param.21) | copy-start | bytes 393220
  9.5 19.6 %copy-start.7 = (bf16[256,64]{0,1:T(8,128)(2,1)S(1)}, bf16[256,64]{0,1:T(8,128)(2,1)}, u32[]{:S(2)}) copy-start(bf16[256,64]{0,1:T(8,128)(2,1)} %param.15) | copy-start | bytes 98308
  9.8 19.5 %copy-start.8 = (bf16[256,64]{0,1:T(8,128)(2,1)S(1)}, bf16[256,64]{0,1:T(8,128)(2,1)}, u32[]{:S(2)}) copy-start(bf16[256,64]{0,1:T(8,128)(2,1)} %param.16) | copy-start | bytes 98308
  12.0 44.5 %all-to-all-start = ((bf16[32,22,256]{2,1,0:T(8,128)(2,1)}), bf16[32,22,256]{2,1,0:T(8,128)(2,1)S(1)}, u32[]{:S(2)}, u32[]{:S(2)}) async-start(bf16[32,22,256]{2,1,0:T(8,128)(2,1)} %reshape.144), calls=%async_computation | async-start | bytes 786432 | tf_op jit(solution)/shard_map/all_to_all | solution.py:221
  28.7 120.4 %all-gather.3.cloned.1.call-start = ((), (), s32[]{:S(2)}) async-start(), calls=%async_computation.6 | async-start | bytes 2162688 | tf_op jit(solution)/shard_map/all_gather | solution.py:266
  57.8 4.3 %copy-start.6 = (bf16[1,4096,128]{2,1,0:T(8,128)(2,1)S(1)}, bf16[1,4096,128]{2,1,0:T(8,128)(2,1)}, u32[]{:S(2)}) copy-start(bf16[1,4096,128]{2,1,0:T(8,128)(2,1)} %param.26) | copy-start | bytes 3145732
  57.8 35.6 %all-to-all-start.1 = ((bf16[4,704,256]{2,1,0:T(8,128)(2,1)}), bf16[4,704,256]{2,1,0:T(8,128)(2,1)S(1)}, u32[]{:S(2)}, u32[]{:S(2)}) async-start(bf16[4,704,256]{2,1,0:T(8,128)(2,1)} %broadcast_in_dim.61), calls=%async_computation.1 | async-start | bytes 2883584 | tf_op jit(solution)/shard_map/all_to_all | solution.py:221
  64.1 12.5 %copy-start.9 = (f32[4096]{0:T(1024)S(1)}, f32[4096]{0:T(1024)}, u32[]{:S(2)}) copy-start(f32[4096]{0:T(1024)} %param.22) | copy-start | bytes 49156
  65.0 16.1 %collective-permute-start.10 = (bf16[1024,256]{1,0:T(8,128)(2,1)}, bf16[1024,256]{1,0:T(8,128)(2,1)S(1)}, u32[]{:S(2)}, u32[]{:S(2)}) collective-permute-start(bf16[1024,256]{1,0:T(8,128)(2,1)} %pad_maximum_fusion.6), channel_id=1, source_target_pairs={{0,2},{1,3},{2,0},{3,1},{4,6},{5,7},{6,4},{7,5},{8,10},{9,11},{10,... | collective-permute-start | bytes 1572872 | tf_op jit(solution)/shard_map/ppermute | solution.py:226
  70.5 22.3 %collective-permute-start.11 = (bf16[1024,256]{1,0:T(8,128)(2,1)}, bf16[1024,256]{1,0:T(8,128)(2,1)S(1)}, u32[]{:S(2)}, u32[]{:S(2)}) collective-permute-start(bf16[1024,256]{1,0:T(8,128)(2,1)} %pad_maximum_fusion.7), channel_id=1, source_target_pairs={{0,3},{1,0},{2,1},{3,2},{4,7},{5,4},{6,5},{7,6},{8,11},{9,8},{10,9... | collective-permute-start | bytes 1572872 | tf_op jit(solution)/shard_map/ppermute | solution.py:226
  74.1 19.2 %collective-permute-start.9 = (bf16[1024,256]{1,0:T(8,128)(2,1)}, bf16[1024,256]{1,0:T(8,128)(2,1)}, u32[]{:S(2)}, u32[]{:S(2)}) collective-permute-start(bf16[1024,256]{1,0:T(8,128)(2,1)} %pad_maximum_fusion.5), channel_id=1, source_target_pairs={{0,1},{1,2},{2,3},{3,0},{4,5},{5,6},{6,7},{7,4},{8,9},{9,10},{10,1... | collective-permute-start | bytes 1572872 | tf_op jit(solution)/shard_map/ppermute | solution.py:226
  97.4 4.6 %copy-start.4 = (bf16[1,2048,256]{2,1,0:T(8,128)(2,1)S(1)}, bf16[1,2048,256]{2,1,0:T(8,128)(2,1)}, u32[]{:S(2)}) copy-start(bf16[1,2048,256]{2,1,0:T(8,128)(2,1)} %param.27) | copy-start | bytes 3145732
  97.4 23.6 %all-to-all-start.2 = ((bf16[4,720,256]{2,1,0:T(8,128)(2,1)}), bf16[4,720,256]{2,1,0:T(8,128)(2,1)S(1)}, u32[]{:S(2)}, u32[]{:S(2)}) async-start(bf16[4,720,256]{2,1,0:T(8,128)(2,1)} %shard_map.150), calls=%async_computation.2 | async-start | bytes 2949120 | tf_op jit(solution)/shard_map/all_to_all | solution.py:221
  101.9 1.3 copy-start.5
  104.9 26.2 %collective-permute-start.4 = (bf16[1024,256]{1,0:T(8,128)(2,1)}, bf16[1024,256]{1,0:T(8,128)(2,1)S(1)}, u32[]{:S(2)}, u32[]{:S(2)}) collective-permute-start(bf16[1024,256]{1,0:T(8,128)(2,1)} %pad_maximum_fusion.2), channel_id=1, source_target_pairs={{0,8},{4,12},{8,0},{12,4},{1,9},{5,13},{9,1},{13,5},{2,10},{6,14},... | collective-permute-start | bytes 1572872 | tf_op jit(solution)/shard_map/ppermute | solution.py:226
  110.7 22.3 %collective-permute-start.5 = (bf16[1024,256]{1,0:T(8,128)(2,1)}, bf16[1024,256]{1,0:T(8,128)(2,1)S(1)}, u32[]{:S(2)}, u32[]{:S(2)}) collective-permute-start(bf16[1024,256]{1,0:T(8,128)(2,1)} %pad_maximum_fusion.3), channel_id=1, source_target_pairs={{0,12},{4,0},{8,4},{12,8},{1,13},{5,1},{9,5},{13,9},{2,14},{6,2},{... | collective-permute-start | bytes 1572872 | tf_op jit(solution)/shard_map/ppermute | solution.py:226
  122.2 19.5 %all-to-all-start.3 = ((bf16[4,704,128]{2,1,0:T(8,128)(2,1)}), bf16[4,704,128]{2,1,0:T(8,128)(2,1)S(1)}, u32[]{:S(2)}, u32[]{:S(2)}) async-start(bf16[4,704,128]{2,1,0:T(8,128)(2,1)} %hidden.1), calls=%async_computation.3 | async-start | bytes 1441792 | tf_op jit(solution)/shard_map/all_to_all | solution.py:221
  126.8 15.0 %collective-permute-start.3 = (bf16[1024,256]{1,0:T(8,128)(2,1)S(1)}, bf16[1024,256]{1,0:T(8,128)(2,1)S(1)}, u32[]{:S(2)}, u32[]{:S(2)}) collective-permute-start(bf16[1024,256]{1,0:T(8,128)(2,1)S(1)} %pad_maximum_fusion.1), channel_id=1, source_target_pairs={{0,4},{4,8},{8,12},{12,0},{1,5},{5,9},{9,13},{13,1},{2,6},{6,10},{... | collective-permute-start | bytes 1572872 | tf_op jit(solution)/shard_map/ppermute | solution.py:226
  144.4 4.7 %copy-start.10 = (f32[256,2]{0,1:T(2,128)S(1)}, f32[256,2]{0,1:T(2,128)}, u32[]{:S(2)}) copy-start(f32[256,2]{0,1:T(2,128)} %param.24) | copy-start | bytes 6148
  144.4 4.7 %copy-start.3 = (bf16[256,128]{1,0:T(8,128)(2,1)S(1)}, bf16[256,128]{1,0:T(8,128)(2,1)}, u32[]{:S(2)}) copy-start(bf16[256,128]{1,0:T(8,128)(2,1)} %get-tuple-element.8.q_ref) | copy-start | bytes 196612
  144.4 22.5 %all-to-all-start.4 = ((bf16[4,704,256]{2,1,0:T(8,128)(2,1)}), bf16[4,704,256]{2,1,0:T(8,128)(2,1)}, u32[]{:S(2)}, u32[]{:S(2)}) async-start(bf16[4,704,256]{2,1,0:T(8,128)(2,1)} %second.1), calls=%async_computation.4 | async-start | bytes 2883584 | tf_op jit(solution)/shard_map/all_to_all | solution.py:221
  149.1 1.6 copy-start.2
  156.4 20.3 %copy-start.1 = (f32[2048]{0:T(1024)S(1)}, f32[2048]{0:T(1024)}, u32[]{:S(2)}) copy-start(f32[2048]{0:T(1024)} %param.19) | copy-start | bytes 24580
  156.4 20.3 %collective-permute-start = (bf16[256,128]{1,0:T(8,128)(2,1)S(1)}, bf16[256,128]{1,0:T(8,128)(2,1)S(1)}, u32[]{:S(2)}, u32[]{:S(2)}) collective-permute-start(bf16[256,128]{1,0:T(8,128)(2,1)S(1)} %attend.1.refs_0_), channel_id=1, source_target_pairs={{0,1},{1,2},{2,3},{3,0},{4,5},{5,6},{6,7},{7,4},{8,9},{9,10},{10,1... | collective-permute-start | bytes 196616 | tf_op jit(solution)/shard_map/ppermute | solution.py:226
  159.5 17.2 %collective-permute-start.1 = (bf16[256,128]{1,0:T(8,128)(2,1)S(1)}, bf16[256,128]{1,0:T(8,128)(2,1)S(1)}, u32[]{:S(2)}, u32[]{:S(2)}) collective-permute-start(bf16[256,128]{1,0:T(8,128)(2,1)S(1)} %attend.1.refs_0_), channel_id=1, source_target_pairs={{0,2},{1,3},{2,0},{3,1},{4,6},{5,7},{6,4},{7,5},{8,10},{9,11},{10,... | collective-permute-start | bytes 196616 | tf_op jit(solution)/shard_map/ppermute | solution.py:226
  163.8 12.9 %collective-permute-start.2 = (bf16[256,128]{1,0:T(8,128)(2,1)S(1)}, bf16[256,128]{1,0:T(8,128)(2,1)S(1)}, u32[]{:S(2)}, u32[]{:S(2)}) collective-permute-start(bf16[256,128]{1,0:T(8,128)(2,1)S(1)} %attend.1.refs_0_), channel_id=1, source_target_pairs={{0,3},{1,0},{2,1},{3,2},{4,7},{5,4},{6,5},{7,6},{8,11},{9,8},{10,9... | collective-permute-start | bytes 196616 | tf_op jit(solution)/shard_map/ppermute | solution.py:226
  169.5 35.0 %all-to-all-start.5 = ((bf16[32,22,256]{2,1,0:T(8,128)(2,1)}), bf16[32,22,256]{2,1,0:T(8,128)(2,1)S(1)}, u32[]{:S(2)}, u32[]{:S(2)}) async-start(bf16[32,22,256]{2,1,0:T(8,128)(2,1)} %reshape.148), calls=%async_computation.5 | async-start | bytes 786432 | tf_op jit(solution)/shard_map/all_to_all | solution.py:221
  178.0 10.8 %collective-permute-start.8 = (bf16[272,256]{1,0:T(8,128)(2,1)S(1)}, bf16[272,256]{1,0:T(8,128)(2,1)S(1)}, u32[]{:S(2)}, u32[]{:S(2)}) collective-permute-start(bf16[272,256]{1,0:T(8,128)(2,1)S(1)} %get-tuple-element.13), channel_id=1, source_target_pairs={{0,4},{4,8},{8,12},{12,0},{1,5},{5,9},{9,13},{13,1},{2,6},{6,10},{... | collective-permute-start | bytes 417800 | tf_op jit(solution)/shard_map/ppermute | solution.py:226
  181.4 9.0 %collective-permute-start.7 = (bf16[272,256]{1,0:T(8,128)(2,1)S(1)}, bf16[272,256]{1,0:T(8,128)(2,1)S(1)}, u32[]{:S(2)}, u32[]{:S(2)}) collective-permute-start(bf16[272,256]{1,0:T(8,128)(2,1)S(1)} %get-tuple-element.12), channel_id=1, source_target_pairs={{0,8},{4,12},{8,0},{12,4},{1,9},{5,13},{9,1},{13,5},{2,10},{6,14},... | collective-permute-start | bytes 417800 | tf_op jit(solution)/shard_map/ppermute | solution.py:226
  185.7 6.2 %collective-permute-start.6 = (bf16[272,256]{1,0:T(8,128)(2,1)S(1)}, bf16[272,256]{1,0:T(8,128)(2,1)S(1)}, u32[]{:S(2)}, u32[]{:S(2)}) collective-permute-start(bf16[272,256]{1,0:T(8,128)(2,1)S(1)} %get-tuple-element.11), channel_id=1, source_target_pairs={{0,12},{4,0},{8,4},{12,8},{1,13},{5,1},{9,5},{13,9},{2,14},{6,2},{... | collective-permute-start | bytes 417800 | tf_op jit(solution)/shard_map/ppermute | solution.py:226
Sparse Core Ops, SparseCore 0:
  33.7 72.6 all-gather.2

commit v4 on v3

--- a/solution.py
+++ b/solution.py
@@ -68,7 +68,7 @@
     )
 
 
-def attend_body(q_ref, kv_ref, out_ref):
+def attend_body(q_ref, mine_ref, other_ref, out_ref):
     rows = q_ref.shape[0]
     lanes = lax.broadcasted_iota(jnp.int32, (rows, 2 * HEAD), 1)
     both = q_ref[...].astype(F32)
@@ -78,8 +78,11 @@
     top = jnp.full((2 * rows, 1), -jnp.inf, F32)
     total = jnp.zeros((2 * rows, 1), F32)
     acc = jnp.zeros((2 * rows, 2 * HEAD), F32)
-    for at in range(0, kv_ref.shape[0], KEY_STEP):
-        block = kv_ref[at : at + KEY_STEP, :]
+    steps = [
+        (ref, at) for ref in (mine_ref, other_ref) for at in range(0, ref.shape[0], KEY_STEP)
+    ]
+    for ref, at in steps:
+        block = ref[at : at + KEY_STEP, :]
         scores = lax.dot_general(wide, block, (((1,), (1,)), ((), ())), preferred_element_type=F32)
         new_top = jnp.maximum(top, jnp.max(scores, axis=1, keepdims=True))
         factor = jnp.exp(top - new_top)
@@ -92,9 +95,9 @@
     out_ref[...] = jnp.where(lanes < HEAD, first, done[rows:]).astype(BF16)
 
 
-def attend(query_turned, key_value):
+def attend(query_turned, mine, other):
     rows = query_turned.shape[0]
-    keys = key_value.shape[0]
+    keys = mine.shape[0] + other.shape[0]
     return pl.pallas_call(
         attend_body,
         out_shape=jax.ShapeDtypeStruct(query_turned.shape, BF16),
@@ -105,7 +108,32 @@
             transcendentals=2 * rows * keys,
         ),
         name="attend",
-    )(query_turned, key_value)
+    )(query_turned, mine, other)
+
+
+def route_body(ids_ref, rows_ref, out_ref, slot_ref):
+    blocks, cap, _ = out_ref.shape
+    count = rows_ref.shape[0]
+    lane = lax.broadcasted_iota(jnp.int32, (count, blocks), 1)
+    ids = [ids_ref[:, k : k + 1] for k in range(2)]
+    marks = [(lane == ids[k]).astype(F32) for k in range(2)]
+    down = lax.broadcasted_iota(jnp.int32, (count, count), 0)
+    across = lax.broadcasted_iota(jnp.int32, (count, count), 1)
+    below = (across < down).astype(BF16)
+    earlier = jnp.dot(below, (marks[0] + marks[1]).astype(BF16), preferred_element_type=F32)
+    places = [
+        jnp.sum(earlier * marks[0], axis=1, keepdims=True),
+        jnp.sum((earlier + marks[0]) * marks[1], axis=1, keepdims=True),
+    ]
+    slots = [ids[k] * cap + places[k].astype(jnp.int32) for k in range(2)]
+    slot_ref[...] = jnp.concatenate(slots, axis=1)
+    slot = lax.broadcasted_iota(jnp.int32, (count, blocks * cap), 1)
+    pick = ((slot == slots[0]) | (slot == slots[1])).astype(BF16)
+    placed = lax.dot_general(
+        pick, rows_ref[...], (((0,), (0,)), ((), ())), preferred_element_type=F32
+    )
+    for k in range(blocks):
+        out_ref[k] = placed[k * cap : (k + 1) * cap, :].astype(BF16)
 
 
 def mix_body(k_rows, base, joined, index_ref, *refs):
@@ -226,6 +254,15 @@
     return lax.ppermute(array, axis, [(k, (k + by) % size) for k in range(size)])
 
 
+def keys_everywhere(mine):
+    by = lax.axis_size("z") // 2
+    while by:
+        came = shift(mine, "z", by)
+        mine = jnp.concatenate([mine, came], axis=0)
+        by //= 2
+    return mine, shift(mine, "c", 1)
+
+
 def deal(chunk_for, axis):
     place = lax.axis_index(axis)
     landed = [chunk_for(place)]
@@ -263,24 +300,17 @@
     query_turned, own_rows = turn(
         queries, jnp.concatenate([key_rows, values], axis=1), query_gain, key_gain, tables
     )
-    key_value = lax.all_gather(own_rows, EP, axis=0, tiled=False)
-    key_value = key_value.reshape(experts_count * length, 2 * HEAD)
-
-    copies = length * 2
-    flat_ids = route_ids.reshape(copies)
-    hit_marks = (flat_ids[:, None] == jnp.arange(experts_count, dtype=jnp.int32)[None, :]).astype(
-        jnp.int32
-    )
-    earlier = jnp.cumsum(hit_marks, axis=0) - hit_marks
-    places = jnp.sum(earlier * hit_marks, axis=1)
-    slot_index = (flat_ids * CAP + places).reshape(length, 2)
-    slot_axis = jnp.arange(slot_total, dtype=jnp.int32)
-    pick = (
-        (slot_index[:, 0][None, :] == slot_axis[:, None])
-        | (slot_index[:, 1][None, :] == slot_axis[:, None])
-    ).astype(BF16)
-    outgoing = jnp.dot(pick, expert_input, preferred_element_type=F32).astype(BF16)
-    arrived = swap(outgoing.reshape(experts_count, CAP, piece), EP).reshape(slot_total, piece)
+    mine, other = keys_everywhere(own_rows)
+
+    outgoing, slot_index = pl.pallas_call(
+        route_body,
+        out_shape=[
+            jax.ShapeDtypeStruct((experts_count, CAP, piece), BF16),
+            jax.ShapeDtypeStruct((length, 2), jnp.int32),
+        ],
+        name="route",
+    )(route_ids, expert_input)
+    arrived = swap(outgoing, EP).reshape(slot_total, piece)
 
     gate_view = expert_gate.reshape(SIDE, SIDE, piece, hid)
     up_view = expert_up.reshape(SIDE, SIDE, piece, hid)
@@ -327,8 +357,9 @@
     )(from_y, hidden_all, *second_weights)
     landed = swap(expert_partial, "y")
     expert_out = jnp.sum(landed.astype(F32), axis=0).astype(BF16)
-
-    heads_out = attend(query_turned, key_value)
+    expert_out = expert_out.reshape(experts_count, CAP, piece)
+
+    heads_out = attend(query_turned, mine, other)
     heads = [heads_out] + [shift(heads_out, "x", by) for by in range(1, SIDE)]
     mix_partial = mix(
         heads,
@@ -343,8 +374,8 @@
     mix_scale = lax.rsqrt(mix_square_sum / mix_gain.shape[0] + EPS)
     attended = (mix_sum * mix_scale[:, None]).astype(BF16)
 
-    returned = swap(expert_out.reshape(experts_count, CAP, piece), EP).reshape(slot_total, piece)
-    slots = slot_axis[None, :]
+    returned = swap(expert_out, EP).reshape(slot_total, piece)
+    slots = jnp.arange(slot_total, dtype=jnp.int32)[None, :]
     first = jnp.dot(
         (slot_index[:, :1] == slots).astype(BF16), returned, preferred_element_type=F32
     )

time: 214 us -> 202 us (0.944)
  waiting for transfers between devices: 71.4 us -> 43.4 us
  starting transfers between devices: 83.1 us -> 106 us
  between operations: 14.5 us -> 1.28 us
  Pallas kernels: 17.1 us -> 21.2 us
  local copies, waits for them, and re-layouts: 11 us -> 14.8 us
    ppermute x12 -> x17, starting transfers between devices: 42.2 us -> 60.5 us  [shift(): lax.ppermute(array, axis, [(k, (k + by) % size) for k in range(size)])]
    all_to_all x6, waiting for transfers between devices: 42.1 us -> 26.5 us  [swap(): return lax.all_to_all(array, axis, 0, 0, tiled=True)]
    ppermute x12 -> x17, waiting for transfers between devices: 29.2 us -> 17 us  [shift(): lax.ppermute(array, axis, [(k, (k + by) % size) for k in range(size)])]
    all_to_all x6, starting transfers between devices: 40.9 us -> 45.5 us  [swap(): return lax.all_to_all(array, axis, 0, 0, tiled=True)]
    pallas_call x0 -> x1, Pallas kernels: none -> 2.56 us  [forward(): pl.pallas_call(route_body, out_shape=[jax.ShapeDtypeStruct((experts_count...]
    unnamed x25 -> x45, local copies, waits for them, and re-layouts: 3.25 us -> 5.14 us
  transfers between devices with their start and end apart: 19 -> 23, of which waited for: 10 -> 8; matrix products, arithmetic and copies ran while one was open for 9% -> 12% of each run, Pallas kernels for 8% -> 9%
where the time goes in v4:
time: 202 us; the launch traced here: 201 us
  starting transfers between devices  106 us (52%)
  waiting for transfers between devices  43.4 us (21%)
  Pallas kernels  21.2 us (10%)
  local copies, waits for them, and re-layouts  14.8 us (7%)
  other arithmetic  12.6 us (6%)
    ppermute x17, starting transfers between devices, shift(): lax.ppermute(array, axis, [(k, (k + by) % size) for k in range(size)])  60.5 us
    all_to_all x6, starting transfers between devices, swap(): return lax.all_to_all(array, axis, 0, 0, tiled=True)  45.5 us
    all_to_all x6, waiting for transfers between devices, swap(): return lax.all_to_all(array, axis, 0, 0, tiled=True)  26.5 us
    ppermute x17, waiting for transfers between devices, shift(): lax.ppermute(array, axis, [(k, (k + by) % size) for k in range(size)])  17 us
    pallas_call x1, Pallas kernels, attend(): pl.pallas_call(attend_body, out_shape=jax.ShapeDtypeStruct(query_turned.s...  7.2 us
    pallas_call x2, Pallas kernels, mix(): pl.pallas_call(functools.partial(mix_body, k_rows, base, joined), out_sha...  5.32 us
    unnamed x45, local copies, waits for them, and re-layouts  5.14 us
  transfers between devices with their start and end apart: 23, of which 8 were waited for; matrix products, arithmetic and copies ran while one was open for 12% of the time, Pallas kernels for 9%

profile of v4, /device:TPU:1, one launch (start us, length us, event | category | flops | bytes accessed | tf_op | source)
XLA Modules:
  0.0 200.6 jit_solution(17270934524832774475)
XLA Ops:
  0.6 1.6 copy.29.ids_ref
  2.2 2.6 %route.1 = (bf16[32,22,256]{2,1,0:T(8,128)(2,1)}, s32[256,2]{1,0:T(8,128)}) custom-call(s32[256,2]{1,0:T(8,128)} %copy.29.ids_ref, bf16[256,256]{1,0:T(8,128)(2,1)} %rows_ref.1), custom_call_target="tpu_custom_call" | custom-call | tf_op jit(solution)/shard_map/route/pallas_call | solution.py:305
  4.8 16.7 %all-to-all-start = ((bf16[32,22,256]{2,1,0:T(8,128)(2,1)}), bf16[32,22,256]{2,1,0:T(8,128)(2,1)S(1)}, u32[]{:S(2)}, u32[]{:S(2)}) async-start(bf16[32,22,256]{2,1,0:T(8,128)(2,1)} %get-tuple-element.17), calls=%async_computation | async-start | bytes 786432 | tf_op jit(solution)/shard_map/all_to_all | solution.py:249
  21.6 2.1 %constant_dynamic-slice_fusion = (bf16[4,1,256,128]{3,2,1,0:T(8,128)(2,1)S(1)}, bf16[4,1,256,128]{3,2,1,0:T(8,128)(2,1)S(1)}, bf16[4,1,256,128]{3,2,1,0:T(8,128)...) fusion(bf16[4,4,256,128]{3,2,1,0:T(8,128)(2,1)S(1)} %bitcast.50, ...), kind=kLoop, calls=%fused_computation.44 | loop fusion | bytes 4194320 | tf_op jit(solution)/shard_map/jit(dynamic_index_in_dim)/dynamic_slice | solution.py:319
  23.7 0.9 pad_maximum_fusion.6
  24.5 3.1 %collective-permute-start.14 = (bf16[1024,256]{1,0:T(8,128)(2,1)}, bf16[1024,256]{1,0:T(8,128)(2,1)S(1)}, u32[]{:S(2)}, u32[]{:S(2)}) collective-permute-start(bf16[1024,256]{1,0:T(8,128)(2,1)} %pad_maximum_fusion.6), channel_id=1, source_target_pairs={{0,1},{1,2},{2,3},{3,0},{4,5},{5,6},{6,7},{7,4},{8,9},{9,10},{10,1... | collective-permute-start | bytes 1572872 | tf_op jit(solution)/shard_map/ppermute | solution.py:254
  27.6 0.9 pad_maximum_fusion.7
  28.5 4.3 %collective-permute-start.15 = (bf16[1024,256]{1,0:T(8,128)(2,1)}, bf16[1024,256]{1,0:T(8,128)(2,1)S(1)}, u32[]{:S(2)}, u32[]{:S(2)}) collective-permute-start(bf16[1024,256]{1,0:T(8,128)(2,1)} %pad_maximum_fusion.7), channel_id=1, source_target_pairs={{0,2},{1,3},{2,0},{3,1},{4,6},{5,7},{6,4},{7,5},{8,10},{9,11},{10,... | collective-permute-start | bytes 1572872 | tf_op jit(solution)/shard_map/ppermute | solution.py:254
  32.8 0.8 pad_maximum_fusion.8
  33.7 3.0 %collective-permute-start.16 = (bf16[1024,256]{1,0:T(8,128)(2,1)}, bf16[1024,256]{1,0:T(8,128)(2,1)}, u32[]{:S(2)}, u32[]{:S(2)}) collective-permute-start(bf16[1024,256]{1,0:T(8,128)(2,1)} %pad_maximum_fusion.8), channel_id=1, source_target_pairs={{0,3},{1,0},{2,1},{3,2},{4,7},{5,4},{6,5},{7,6},{8,11},{9,8},{10,9... | collective-permute-start | bytes 1572872 | tf_op jit(solution)/shard_map/ppermute | solution.py:254
  36.8 12.5 %all-to-all-done = bf16[32,22,256]{2,1,0:T(8,128)(2,1)S(1)} async-done(((bf16[32,22,256]{2,1,0:T(8,128)(2,1)}), bf16[32,22,256]{2,1,0:T(8,128)(2,1)S(1)}, u32[]{:S(2)}, u32[]{:S(2)}) %all-to-all-start) | async-done | bytes 360480 | tf_op jit(solution)/shard_map/all_to_all | solution.py:249
  49.4 1.3 broadcast_in_dim.58
  50.6 4.3 %all-to-all-start.1 = ((bf16[4,704,256]{2,1,0:T(8,128)(2,1)}), bf16[4,704,256]{2,1,0:T(8,128)(2,1)S(1)}, u32[]{:S(2)}, u32[]{:S(2)}) async-start(bf16[4,704,256]{2,1,0:T(8,128)(2,1)} %broadcast_in_dim.58), calls=%async_computation.1 | async-start | bytes 2883584 | tf_op jit(solution)/shard_map/all_to_all | solution.py:249
  55.6 0.7 pad_maximum_fusion.11.kv_ref
  56.3 1.3 sine_multiply_fusion
  57.5 2.2 %turn.1 = (bf16[256,128]{1,0:T(8,128)(2,1)}, bf16[256,128]{1,0:T(8,128)(2,1)}) custom-call(bf16[256,128]{1,0:T(8,128)(2,1)} %q_ref.1, bf16[256,128]{1,0:T(8,128)(2,1)} %pad_maximum_fusion.11.kv_ref, f32[1,64]{1,0:T(1,128)} %bitcast.62, f32[1,64]{1,0:T(1,128)} %bitcast.63, f32[256,128]{1,0:T(8,128)} %get-tuple-element.37.cos_ref, ...), custom_call_target="tpu_custom_call" | custom-call | tf_op jit(solution)/shard_map/turn/pallas_call | solution.py:62
  59.8 2.5 %collective-permute-start = (bf16[256,128]{1,0:T(8,128)(2,1)}, bf16[256,128]{1,0:T(8,128)(2,1)S(1)}, u32[]{:S(2)}, u32[]{:S(2)}) collective-permute-start(bf16[256,128]{1,0:T(8,128)(2,1)} %get-tuple-element.11), channel_id=1, source_target_pairs={{0,256},{32,288},{64,320},{96,352},{128,384},{160,416},{192,448},{... | collective-permute-start | bytes 196616 | tf_op jit(solution)/shard_map/ppermute | solution.py:254
  62.4 1.1 pad_maximum_fusion.5.refs_1_
  63.4 2.1 %dynamic-slice_bitcast_fusion = (bf16[512,256]{1,0:T(8,128)(2,1)}, bf16[512,256]{1,0:T(8,128)(2,1)}, bf16[512,256]{1,0:T(8,128)(2,1)S(1)}, bf16[512,256]{1,0:T(8,128)(2,1)}) fusion(bf16[1,2048,256]{2,1,0:T(8,128)(2,1)} %param.27, s32[]{:T(128)S(6)} %select_n.134, s32[]{:T(128)S(6)} %select_n.130, s32[]{:T(128)S(6)} %select_n.128, s32[]{:T(128)S(6)} %select_n.132), kind=kLoop, calls=%fused_computation.19 | loop fusion | bytes 2097168 | tf_op jit(solution)/shard_map/dynamic_slice | solution.py:323
  65.6 8.4 %collective-permute-done = bf16[256,128]{1,0:T(8,128)(2,1)S(1)} collective-permute-done((bf16[256,128]{1,0:T(8,128)(2,1)}, bf16[256,128]{1,0:T(8,128)(2,1)S(1)}, u32[]{:S(2)}, u32[]{:S(2)}) %collective-permute-start) | collective-permute-done | bytes 65568 | tf_op jit(solution)/shard_map/ppermute | solution.py:254
  74.0 0.6 copy-done.10
  74.7 0.7 pad_maximum_fusion.10
  75.3 1.9 collective-permute-start.1
  77.3 4.1 %shard_map.150 = bf16[4,720,256]{2,1,0:T(8,128)(2,1)} custom-call(s32[12]{0:T(128)S(1)} %pad_add_fusion.1.index_ref, bf16[4,704,256]{2,1,0:T(8,128)(2,1)S(1)} %all-to-all-done.1.refs_0_, bf16[1024,256]{1,0:T(8,128)(2,1)S(1)} %pad_maximum_fusion.5.refs_1_, bf16[1024,256]{1,0:T(8,128)(2,1)S(1)} %collective-permute-done.14.refs_2_, ...), custom_call_target="tpu_custom_call" | custom-call | flops 1476395008 | bytes 2883584 | tf_op jit(solution)/shard_map/pallas_call | solution.py:189
  81.4 4.0 %all-to-all-start.2 = ((bf16[4,720,256]{2,1,0:T(8,128)(2,1)}), bf16[4,720,256]{2,1,0:T(8,128)(2,1)S(1)}, u32[]{:S(2)}, u32[]{:S(2)}) async-start(bf16[4,720,256]{2,1,0:T(8,128)(2,1)} %shard_map.150), calls=%async_computation.2 | async-start | bytes 2949120 | tf_op jit(solution)/shard_map/all_to_all | solution.py:249
  85.4 2.9 %collective-permute-done.1 = bf16[512,128]{1,0:T(8,128)(2,1)S(1)} collective-permute-done((bf16[512,128]{1,0:T(8,128)(2,1)}, bf16[512,128]{1,0:T(8,128)(2,1)S(1)}, u32[]{:S(2)}, u32[]{:S(2)}) %collective-permute-start.1) | collective-permute-done | bytes 131104 | tf_op jit(solution)/shard_map/ppermute | solution.py:254
  88.3 5.9 %collective-permute-start.2 = (bf16[1024,128]{1,0:T(8,128)(2,1)S(1)}, bf16[1024,128]{1,0:T(8,128)(2,1)S(1)}, u32[]{:S(2)}, u32[]{:S(2)}) collective-permute-start(bf16[1024,128]{1,0:T(8,128)(2,1)S(1)} %pad_maximum_fusion.9), channel_id=1, source_target_pairs={{0,64},{32,96},{64,128},{96,160},{128,192},{160,224},{192,256},{22... | collective-permute-start | bytes 786440 | tf_op jit(solution)/shard_map/ppermute | solution.py:254
  94.2 0.8 constant_dynamic-slice_fusion.8
  95.0 0.8 pad_maximum_fusion.4
  95.8 4.7 %collective-permute-start.10 = (bf16[1024,256]{1,0:T(8,128)(2,1)}, bf16[1024,256]{1,0:T(8,128)(2,1)S(1)}, u32[]{:S(2)}, u32[]{:S(2)}) collective-permute-start(bf16[1024,256]{1,0:T(8,128)(2,1)} %pad_maximum_fusion.4), channel_id=1, source_target_pairs={{0,12},{4,0},{8,4},{12,8},{1,13},{5,1},{9,5},{13,9},{2,14},{6,2},{... | collective-permute-start | bytes 1572872 | tf_op jit(solution)/shard_map/ppermute | solution.py:254
  100.6 0.8 pad_maximum_fusion.2
  101.4 1.9 collective-permute-start.8
  103.3 1.7 collective-permute-done.2
  105.0 0.9 pad_maximum_fusion
  105.9 5.1 %collective-permute-start.3 = (bf16[2048,128]{1,0:T(8,128)(2,1)}, bf16[2048,128]{1,0:T(8,128)(2,1)}, u32[]{:S(2)}, u32[]{:S(2)}) collective-permute-start(bf16[2048,128]{1,0:T(8,128)(2,1)} %pad_maximum_fusion), channel_id=1, source_target_pairs={{0,32},{32,64},{64,96},{96,128},{128,160},{160,192},{192,224},{224... | collective-permute-start | bytes 1572872 | tf_op jit(solution)/shard_map/ppermute | solution.py:254
  111.0 0.8 pad_maximum_fusion.3
  111.8 5.0 %collective-permute-start.9 = (bf16[1024,256]{1,0:T(8,128)(2,1)}, bf16[1024,256]{1,0:T(8,128)(2,1)S(1)}, u32[]{:S(2)}, u32[]{:S(2)}) collective-permute-start(bf16[1024,256]{1,0:T(8,128)(2,1)} %pad_maximum_fusion.3), channel_id=1, source_target_pairs={{0,8},{4,12},{8,0},{12,4},{1,9},{5,13},{9,1},{13,5},{2,10},{6,14},... | collective-permute-start | bytes 1572872 | tf_op jit(solution)/shard_map/ppermute | solution.py:254
  116.8 0.6 constant_dynamic-update-slice_fusion.4
  117.5 0.6 constant_dynamic-update-slice_fusion.3
  118.1 0.7 constant_dynamic-update-slice_fusion.2
  118.8 1.3 hidden.1
  120.1 3.7 %all-to-all-start.3 = ((bf16[4,704,128]{2,1,0:T(8,128)(2,1)}), bf16[4,704,128]{2,1,0:T(8,128)(2,1)S(1)}, u32[]{:S(2)}, u32[]{:S(2)}) async-start(bf16[4,704,128]{2,1,0:T(8,128)(2,1)} %hidden.1), calls=%async_computation.3 | async-start | bytes 1441792 | tf_op jit(solution)/shard_map/all_to_all | solution.py:249
  123.7 0.7 constant_dynamic-update-slice_fusion.1
  124.5 1.9 constant_dynamic-update-slice_fusion.mine_ref
  126.4 4.4 %collective-permute-start.4 = (bf16[4096,128]{1,0:T(8,128)(2,1)}, bf16[4096,128]{1,0:T(8,128)(2,1)}, u32[]{:S(2)}, u32[]{:S(2)}) collective-permute-start(bf16[4096,128]{1,0:T(8,128)(2,1)} %constant_dynamic-update-slice_fusion.mine_ref), channel_id=1, source_target_pairs={{0,16},{16,0},{1,17},{17,1},{2,18},{18,2},{3,19},{19,3},{4,20},{20... | collective-permute-start | bytes 3145736 | tf_op jit(solution)/shard_map/ppermute | solution.py:254
  130.8 1.8 all-to-all-done.3.gathered
  132.7 2.6 %second.1 = bf16[4,704,256]{2,1,0:T(8,128)(2,1)} custom-call(s32[4]{0:T(128)S(1)} %and_select_fusion.index_ref, bf16[4,704,128]{2,1,0:T(8,128)(2,1)S(1)} %all-to-all-done.3.gathered, bf16[1024,256]{1,0:T(8,128)(2,1)S(1)} %pad_maximum_fusion.1.refs_4_.refs_0_, bf16[1024,256]{1,0:T(8,128)(2,1)S(1)} %collective-permute-done.8.refs_5_.refs_1_, ...), custom_call_target="tpu_custom_call" | custom-call | tf_op jit(solution)/shard_map/second/pallas_call | solution.py:350
  135.3 4.6 %all-to-all-start.4 = ((bf16[4,704,256]{2,1,0:T(8,128)(2,1)}), bf16[4,704,256]{2,1,0:T(8,128)(2,1)}, u32[]{:S(2)}, u32[]{:S(2)}) async-start(bf16[4,704,256]{2,1,0:T(8,128)(2,1)} %second.1), calls=%async_computation.4 | async-start | bytes 2883584 | tf_op jit(solution)/shard_map/all_to_all | solution.py:249
  140.2 7.2 %attend.1.refs_0_ = bf16[256,128]{1,0:T(8,128)(2,1)S(1)} custom-call(bf16[256,128]{1,0:T(8,128)(2,1)S(1)} %copy-done.1, bf16[4096,128]{1,0:T(8,128)(2,1)} %constant_dynamic-update-slice_fusion.mine_ref, bf16[4096,128]{1,0:T(8,128)(2,1)} %collective-permute-done.4.other_ref), custom_call_target="tpu_custom_call" | custom-call | flops 2147483648 | bytes 2097152 | tf_op jit(solution)/shard_map/attend/pallas_call | solution.py:101
  147.4 2.2 %collective-permute-start.5 = (bf16[256,128]{1,0:T(8,128)(2,1)S(1)}, bf16[256,128]{1,0:T(8,128)(2,1)S(1)}, u32[]{:S(2)}, u32[]{:S(2)}) collective-permute-start(bf16[256,128]{1,0:T(8,128)(2,1)S(1)} %attend.1.refs_0_), channel_id=1, source_target_pairs={{0,1},{1,2},{2,3},{3,0},{4,5},{5,6},{6,7},{7,4},{8,9},{9,10},{10,1... | collective-permute-start | bytes 196616 | tf_op jit(solution)/shard_map/ppermute | solution.py:254
  149.6 4.0 %collective-permute-start.6 = (bf16[256,128]{1,0:T(8,128)(2,1)S(1)}, bf16[256,128]{1,0:T(8,128)(2,1)S(1)}, u32[]{:S(2)}, u32[]{:S(2)}) collective-permute-start(bf16[256,128]{1,0:T(8,128)(2,1)S(1)} %attend.1.refs_0_), channel_id=1, source_target_pairs={{0,2},{1,3},{2,0},{3,1},{4,6},{5,7},{6,4},{7,5},{8,10},{9,11},{10,... | collective-permute-start | bytes 196616 | tf_op jit(solution)/shard_map/ppermute | solution.py:254
  153.6 3.1 %collective-permute-start.7 = (bf16[256,128]{1,0:T(8,128)(2,1)S(1)}, bf16[256,128]{1,0:T(8,128)(2,1)S(1)}, u32[]{:S(2)}, u32[]{:S(2)}) collective-permute-start(bf16[256,128]{1,0:T(8,128)(2,1)S(1)} %attend.1.refs_0_), channel_id=1, source_target_pairs={{0,3},{1,0},{2,1},{3,2},{4,7},{5,4},{6,5},{7,6},{8,11},{9,8},{10,9... | collective-permute-start | bytes 196616 | tf_op jit(solution)/shard_map/ppermute | solution.py:254
  156.7 1.7 reduce_sum.22
  158.4 0.9 reshape.117
  159.3 12.1 %all-to-all-start.5 = ((bf16[32,22,256]{2,1,0:T(8,128)(2,1)}), bf16[32,22,256]{2,1,0:T(8,128)(2,1)S(1)}, u32[]{:S(2)}, u32[]{:S(2)}) async-start(bf16[32,22,256]{2,1,0:T(8,128)(2,1)} %reshape.117), calls=%async_computation.5 | async-start | bytes 786432 | tf_op jit(solution)/shard_map/all_to_all | solution.py:249
  171.5 1.2 shard_map.149
  172.8 2.2 %collective-permute-start.13 = (bf16[272,256]{1,0:T(8,128)(2,1)S(1)}, bf16[272,256]{1,0:T(8,128)(2,1)S(1)}, u32[]{:S(2)}, u32[]{:S(2)}) collective-permute-start(bf16[272,256]{1,0:T(8,128)(2,1)S(1)} %get-tuple-element.15), channel_id=1, source_target_pairs={{0,4},{4,8},{8,12},{12,0},{1,5},{5,9},{9,13},{13,1},{2,6},{6,10},{... | collective-permute-start | bytes 417800 | tf_op jit(solution)/shard_map/ppermute | solution.py:254
  175.0 4.1 %collective-permute-start.12 = (bf16[272,256]{1,0:T(8,128)(2,1)S(1)}, bf16[272,256]{1,0:T(8,128)(2,1)S(1)}, u32[]{:S(2)}, u32[]{:S(2)}) collective-permute-start(bf16[272,256]{1,0:T(8,128)(2,1)S(1)} %get-tuple-element.14), channel_id=1, source_target_pairs={{0,8},{4,12},{8,0},{12,4},{1,9},{5,13},{9,1},{13,5},{2,10},{6,14},... | collective-permute-start | bytes 417800 | tf_op jit(solution)/shard_map/ppermute | solution.py:254
  179.1 3.1 %collective-permute-start.11 = (bf16[272,256]{1,0:T(8,128)(2,1)S(1)}, bf16[272,256]{1,0:T(8,128)(2,1)S(1)}, u32[]{:S(2)}, u32[]{:S(2)}) collective-permute-start(bf16[272,256]{1,0:T(8,128)(2,1)S(1)} %get-tuple-element.13), channel_id=1, source_target_pairs={{0,12},{4,0},{8,4},{12,8},{1,13},{5,1},{9,5},{13,9},{2,14},{6,2},{... | collective-permute-start | bytes 417800 | tf_op jit(solution)/shard_map/ppermute | solution.py:254
  182.2 1.5 collective-permute-done.12
  183.7 2.5 %collective-permute-done.11 = bf16[272,256]{1,0:T(8,128)(2,1)S(1)} collective-permute-done((bf16[272,256]{1,0:T(8,128)(2,1)S(1)}, bf16[272,256]{1,0:T(8,128)(2,1)S(1)}, u32[]{:S(2)}, u32[]{:S(2)}) %collective-permute-start.11) | collective-permute-done | bytes 139296 | tf_op jit(solution)/shard_map/ppermute | solution.py:254
  186.2 0.8 multiply_convert_fusion
  187.0 12.2 %all-to-all-done.5 = bf16[32,22,256]{2,1,0:T(8,128)(2,1)S(1)} async-done(((bf16[32,22,256]{2,1,0:T(8,128)(2,1)}), bf16[32,22,256]{2,1,0:T(8,128)(2,1)S(1)}, u32[]{:S(2)}, u32[]{:S(2)}) %all-to-all-start.5) | async-done | bytes 360480 | tf_op jit(solution)/shard_map/all_to_all | solution.py:249
  199.6 1.0 fusion.1
  (84 shorter events, 1.8 us)
Async XLA Ops:
  0.6 20.9 %copy-start.13 = (bf16[1,4096,128]{2,1,0:T(8,128)(2,1)S(1)}, bf16[1,4096,128]{2,1,0:T(8,128)(2,1)}, u32[]{:S(2)}) copy-start(bf16[1,4096,128]{2,1,0:T(8,128)(2,1)} %param.26) | copy-start | bytes 3145732
  4.8 44.5 %all-to-all-start = ((bf16[32,22,256]{2,1,0:T(8,128)(2,1)}), bf16[32,22,256]{2,1,0:T(8,128)(2,1)S(1)}, u32[]{:S(2)}, u32[]{:S(2)}) async-start(bf16[32,22,256]{2,1,0:T(8,128)(2,1)} %get-tuple-element.17), calls=%async_computation | async-start | bytes 786432 | tf_op jit(solution)/shard_map/all_to_all | solution.py:249
  24.5 52.7 %collective-permute-start.14 = (bf16[1024,256]{1,0:T(8,128)(2,1)}, bf16[1024,256]{1,0:T(8,128)(2,1)S(1)}, u32[]{:S(2)}, u32[]{:S(2)}) collective-permute-start(bf16[1024,256]{1,0:T(8,128)(2,1)} %pad_maximum_fusion.6), channel_id=1, source_target_pairs={{0,1},{1,2},{2,3},{3,0},{4,5},{5,6},{6,7},{7,4},{8,9},{9,10},{10,1... | collective-permute-start | bytes 1572872 | tf_op jit(solution)/shard_map/ppermute | solution.py:254
  28.5 48.8 %collective-permute-start.15 = (bf16[1024,256]{1,0:T(8,128)(2,1)}, bf16[1024,256]{1,0:T(8,128)(2,1)S(1)}, u32[]{:S(2)}, u32[]{:S(2)}) collective-permute-start(bf16[1024,256]{1,0:T(8,128)(2,1)} %pad_maximum_fusion.7), channel_id=1, source_target_pairs={{0,2},{1,3},{2,0},{3,1},{4,6},{5,7},{6,4},{7,5},{8,10},{9,11},{10,... | collective-permute-start | bytes 1572872 | tf_op jit(solution)/shard_map/ppermute | solution.py:254
  33.7 43.6 %collective-permute-start.16 = (bf16[1024,256]{1,0:T(8,128)(2,1)}, bf16[1024,256]{1,0:T(8,128)(2,1)}, u32[]{:S(2)}, u32[]{:S(2)}) collective-permute-start(bf16[1024,256]{1,0:T(8,128)(2,1)} %pad_maximum_fusion.8), channel_id=1, source_target_pairs={{0,3},{1,0},{2,1},{3,2},{4,7},{5,4},{6,5},{7,6},{8,11},{9,8},{10,9... | collective-permute-start | bytes 1572872 | tf_op jit(solution)/shard_map/ppermute | solution.py:254
  50.6 4.7 %copy-start.15 = (bf16[256,64]{0,1:T(8,128)(2,1)S(1)}, bf16[256,64]{0,1:T(8,128)(2,1)}, u32[]{:S(2)}) copy-start(bf16[256,64]{0,1:T(8,128)(2,1)} %param.15) | copy-start | bytes 98308
  50.6 4.8 %copy-start.16 = (bf16[256,64]{0,1:T(8,128)(2,1)S(1)}, bf16[256,64]{0,1:T(8,128)(2,1)}, u32[]{:S(2)}) copy-start(bf16[256,64]{0,1:T(8,128)(2,1)} %param.16) | copy-start | bytes 98308
  50.6 11.7 %copy-start.17 = (f32[4096]{0:T(1024)S(1)}, f32[4096]{0:T(1024)}, u32[]{:S(2)}) copy-start(f32[4096]{0:T(1024)} %param.22) | copy-start | bytes 49156
  50.6 26.6 %all-to-all-start.1 = ((bf16[4,704,256]{2,1,0:T(8,128)(2,1)}), bf16[4,704,256]{2,1,0:T(8,128)(2,1)S(1)}, u32[]{:S(2)}, u32[]{:S(2)}) async-start(bf16[4,704,256]{2,1,0:T(8,128)(2,1)} %broadcast_in_dim.58), calls=%async_computation.1 | async-start | bytes 2883584 | tf_op jit(solution)/shard_map/all_to_all | solution.py:249
  59.8 14.3 %collective-permute-start = (bf16[256,128]{1,0:T(8,128)(2,1)}, bf16[256,128]{1,0:T(8,128)(2,1)S(1)}, u32[]{:S(2)}, u32[]{:S(2)}) collective-permute-start(bf16[256,128]{1,0:T(8,128)(2,1)} %get-tuple-element.11), channel_id=1, source_target_pairs={{0,256},{32,288},{64,320},{96,352},{128,384},{160,416},{192,448},{... | collective-permute-start | bytes 196616 | tf_op jit(solution)/shard_map/ppermute | solution.py:254
  62.3 12.3 %copy-start.9 = (bf16[256,128]{1,0:T(8,128)(2,1)S(1)}, bf16[256,128]{1,0:T(8,128)(2,1)}, u32[]{:S(2)}) copy-start(bf16[256,128]{1,0:T(8,128)(2,1)} %get-tuple-element.11) | copy-start | bytes 196612
  74.0 0.6 copy-start.10
  75.3 12.9 %collective-permute-start.1 = (bf16[512,128]{1,0:T(8,128)(2,1)}, bf16[512,128]{1,0:T(8,128)(2,1)S(1)}, u32[]{:S(2)}, u32[]{:S(2)}) collective-permute-start(bf16[512,128]{1,0:T(8,128)(2,1)} %pad_maximum_fusion.10), channel_id=1, source_target_pairs={{0,128},{32,160},{64,192},{96,224},{128,256},{160,288},{192,320},{... | collective-permute-start | bytes 393224 | tf_op jit(solution)/shard_map/ppermute | solution.py:254
  81.4 6.9 %copy-start.11 = (bf16[256,128]{1,0:T(8,128)(2,1)S(1)}, bf16[256,128]{1,0:T(8,128)(2,1)}, u32[]{:S(2)}) copy-start(bf16[256,128]{1,0:T(8,128)(2,1)} %copy-done.10) | copy-start | bytes 196612
  81.4 12.8 %copy-start.2 = (bf16[2048,256]{1,0:T(8,128)(2,1)S(1)}, bf16[2048,256]{1,0:T(8,128)(2,1)}, u32[]{:S(2)}) copy-start(bf16[2048,256]{1,0:T(8,128)(2,1)} %param.20) | copy-start | bytes 3145732
  81.4 37.4 %all-to-all-start.2 = ((bf16[4,720,256]{2,1,0:T(8,128)(2,1)}), bf16[4,720,256]{2,1,0:T(8,128)(2,1)S(1)}, u32[]{:S(2)}, u32[]{:S(2)}) async-start(bf16[4,720,256]{2,1,0:T(8,128)(2,1)} %shard_map.150), calls=%async_computation.2 | async-start | bytes 2949120 | tf_op jit(solution)/shard_map/all_to_all | solution.py:249
  85.4 9.6 %copy-start.6 = (bf16[512,256]{1,0:T(8,128)(2,1)S(1)}, bf16[512,256]{1,0:T(8,128)(2,1)}, u32[]{:S(2)}) copy-start(bf16[512,256]{1,0:T(8,128)(2,1)} %get-tuple-element.28) | copy-start | bytes 786436
  88.3 12.3 %copy-start.5 = (bf16[512,256]{1,0:T(8,128)(2,1)S(1)}, bf16[512,256]{1,0:T(8,128)(2,1)}, u32[]{:S(2)}) copy-start(bf16[512,256]{1,0:T(8,128)(2,1)} %get-tuple-element.29) | copy-start | bytes 786436
  88.3 16.7 %collective-permute-start.2 = (bf16[1024,128]{1,0:T(8,128)(2,1)S(1)}, bf16[1024,128]{1,0:T(8,128)(2,1)S(1)}, u32[]{:S(2)}, u32[]{:S(2)}) collective-permute-start(bf16[1024,128]{1,0:T(8,128)(2,1)S(1)} %pad_maximum_fusion.9), channel_id=1, source_target_pairs={{0,64},{32,96},{64,128},{96,160},{128,192},{160,224},{192,256},{22... | collective-permute-start | bytes 786440 | tf_op jit(solution)/shard_map/ppermute | solution.py:254
  95.0 10.0 %copy-start.12 = (bf16[256,128]{1,0:T(8,128)(2,1)S(1)}, bf16[256,128]{1,0:T(8,128)(2,1)}, u32[]{:S(2)}) copy-start(bf16[256,128]{1,0:T(8,128)(2,1)} %copy-done.10) | copy-start | bytes 196612
  95.0 15.9 %copy-start.3 = (bf16[512,256]{1,0:T(8,128)(2,1)S(1)}, bf16[512,256]{1,0:T(8,128)(2,1)}, u32[]{:S(2)}) copy-start(bf16[512,256]{1,0:T(8,128)(2,1)} %get-tuple-element.31) | copy-start | bytes 786436
  95.8 35.0 %collective-permute-start.10 = (bf16[1024,256]{1,0:T(8,128)(2,1)}, bf16[1024,256]{1,0:T(8,128)(2,1)S(1)}, u32[]{:S(2)}, u32[]{:S(2)}) collective-permute-start(bf16[1024,256]{1,0:T(8,128)(2,1)} %pad_maximum_fusion.4), channel_id=1, source_target_pairs={{0,12},{4,0},{8,4},{12,8},{1,13},{5,1},{9,5},{13,9},{2,14},{6,2},{... | collective-permute-start | bytes 1572872 | tf_op jit(solution)/shard_map/ppermute | solution.py:254
  101.4 29.4 %collective-permute-start.8 = (bf16[1024,256]{1,0:T(8,128)(2,1)}, bf16[1024,256]{1,0:T(8,128)(2,1)S(1)}, u32[]{:S(2)}, u32[]{:S(2)}) collective-permute-start(bf16[1024,256]{1,0:T(8,128)(2,1)} %pad_maximum_fusion.2), channel_id=1, source_target_pairs={{0,4},{4,8},{8,12},{12,0},{1,5},{5,9},{9,13},{13,1},{2,6},{6,10},{... | collective-permute-start | bytes 1572872 | tf_op jit(solution)/shard_map/ppermute | solution.py:254
  105.0 13.1 %copy-start.7 = (bf16[1024,128]{1,0:T(8,128)(2,1)}, bf16[1024,128]{1,0:T(8,128)(2,1)S(1)}, u32[]{:S(2)}) copy-start(bf16[1024,128]{1,0:T(8,128)(2,1)S(1)} %collective-permute-done.2) | copy-start | bytes 786436
  105.9 18.6 %collective-permute-start.3 = (bf16[2048,128]{1,0:T(8,128)(2,1)}, bf16[2048,128]{1,0:T(8,128)(2,1)}, u32[]{:S(2)}, u32[]{:S(2)}) collective-permute-start(bf16[2048,128]{1,0:T(8,128)(2,1)} %pad_maximum_fusion), channel_id=1, source_target_pairs={{0,32},{32,64},{64,96},{96,128},{128,160},{160,192},{192,224},{224... | collective-permute-start | bytes 1572872 | tf_op jit(solution)/shard_map/ppermute | solution.py:254
  111.8 19.1 %collective-permute-start.9 = (bf16[1024,256]{1,0:T(8,128)(2,1)}, bf16[1024,256]{1,0:T(8,128)(2,1)S(1)}, u32[]{:S(2)}, u32[]{:S(2)}) collective-permute-start(bf16[1024,256]{1,0:T(8,128)(2,1)} %pad_maximum_fusion.3), channel_id=1, source_target_pairs={{0,8},{4,12},{8,0},{12,4},{1,9},{5,13},{9,1},{13,5},{2,10},{6,14},... | collective-permute-start | bytes 1572872 | tf_op jit(solution)/shard_map/ppermute | solution.py:254
  120.1 3.7 %copy-start.8 = (bf16[1024,128]{1,0:T(8,128)(2,1)S(1)}, bf16[1024,128]{1,0:T(8,128)(2,1)}, u32[]{:S(2)}) copy-start(bf16[1024,128]{1,0:T(8,128)(2,1)} %copy-done.7) | copy-start | bytes 786436
  120.1 10.7 %copy-start.4 = (bf16[512,256]{1,0:T(8,128)(2,1)S(1)}, bf16[512,256]{1,0:T(8,128)(2,1)}, u32[]{:S(2)}) copy-start(bf16[512,256]{1,0:T(8,128)(2,1)} %get-tuple-element.34) | copy-start | bytes 786436
  120.1 12.6 %all-to-all-start.3 = ((bf16[4,704,128]{2,1,0:T(8,128)(2,1)}), bf16[4,704,128]{2,1,0:T(8,128)(2,1)S(1)}, u32[]{:S(2)}, u32[]{:S(2)}) async-start(bf16[4,704,128]{2,1,0:T(8,128)(2,1)} %hidden.1), calls=%async_computation.3 | async-start | bytes 1441792 | tf_op jit(solution)/shard_map/all_to_all | solution.py:249
  126.4 13.8 %collective-permute-start.4 = (bf16[4096,128]{1,0:T(8,128)(2,1)}, bf16[4096,128]{1,0:T(8,128)(2,1)}, u32[]{:S(2)}, u32[]{:S(2)}) collective-permute-start(bf16[4096,128]{1,0:T(8,128)(2,1)} %constant_dynamic-update-slice_fusion.mine_ref), channel_id=1, source_target_pairs={{0,16},{16,0},{1,17},{17,1},{2,18},{18,2},{3,19},{19,3},{4,20},{20... | collective-permute-start | bytes 3145736 | tf_op jit(solution)/shard_map/ppermute | solution.py:254
  135.3 4.7 %copy-start.14 = (s32[256,2]{1,0:T(8,128)S(1)}, s32[256,2]{1,0:T(8,128)}, u32[]{:S(2)}) copy-start(s32[256,2]{1,0:T(8,128)} %get-tuple-element.16) | copy-start | bytes 6148
  135.3 4.9 %copy-start.18 = (f32[256,2]{0,1:T(2,128)S(1)}, f32[256,2]{0,1:T(2,128)}, u32[]{:S(2)}) copy-start(f32[256,2]{0,1:T(2,128)} %param.24) | copy-start | bytes 6148
  135.3 4.9 %copy-start.1 = (bf16[256,128]{1,0:T(8,128)(2,1)S(1)}, bf16[256,128]{1,0:T(8,128)(2,1)}, u32[]{:S(2)}) copy-start(bf16[256,128]{1,0:T(8,128)(2,1)} %get-tuple-element.10.q_ref) | copy-start | bytes 196612
  135.3 21.4 %all-to-all-start.4 = ((bf16[4,704,256]{2,1,0:T(8,128)(2,1)}), bf16[4,704,256]{2,1,0:T(8,128)(2,1)}, u32[]{:S(2)}, u32[]{:S(2)}) async-start(bf16[4,704,256]{2,1,0:T(8,128)(2,1)} %second.1), calls=%async_computation.4 | async-start | bytes 2883584 | tf_op jit(solution)/shard_map/all_to_all | solution.py:249
  147.4 24.1 %copy-start = (f32[2048]{0:T(1024)S(1)}, f32[2048]{0:T(1024)}, u32[]{:S(2)}) copy-start(f32[2048]{0:T(1024)} %param.19) | copy-start | bytes 24580
  147.4 24.1 %collective-permute-start.5 = (bf16[256,128]{1,0:T(8,128)(2,1)S(1)}, bf16[256,128]{1,0:T(8,128)(2,1)S(1)}, u32[]{:S(2)}, u32[]{:S(2)}) collective-permute-start(bf16[256,128]{1,0:T(8,128)(2,1)S(1)} %attend.1.refs_0_), channel_id=1, source_target_pairs={{0,1},{1,2},{2,3},{3,0},{4,5},{5,6},{6,7},{7,4},{8,9},{9,10},{10,1... | collective-permute-start | bytes 196616 | tf_op jit(solution)/shard_map/ppermute | solution.py:254
  149.6 21.9 %collective-permute-start.6 = (bf16[256,128]{1,0:T(8,128)(2,1)S(1)}, bf16[256,128]{1,0:T(8,128)(2,1)S(1)}, u32[]{:S(2)}, u32[]{:S(2)}) collective-permute-start(bf16[256,128]{1,0:T(8,128)(2,1)S(1)} %attend.1.refs_0_), channel_id=1, source_target_pairs={{0,2},{1,3},{2,0},{3,1},{4,6},{5,7},{6,4},{7,5},{8,10},{9,11},{10,... | collective-permute-start | bytes 196616 | tf_op jit(solution)/shard_map/ppermute | solution.py:254
  153.6 17.9 %collective-permute-start.7 = (bf16[256,128]{1,0:T(8,128)(2,1)S(1)}, bf16[256,128]{1,0:T(8,128)(2,1)S(1)}, u32[]{:S(2)}, u32[]{:S(2)}) collective-permute-start(bf16[256,128]{1,0:T(8,128)(2,1)S(1)} %attend.1.refs_0_), channel_id=1, source_target_pairs={{0,3},{1,0},{2,1},{3,2},{4,7},{5,4},{6,5},{7,6},{8,11},{9,8},{10,9... | collective-permute-start | bytes 196616 | tf_op jit(solution)/shard_map/ppermute | solution.py:254
  159.3 39.9 %all-to-all-start.5 = ((bf16[32,22,256]{2,1,0:T(8,128)(2,1)}), bf16[32,22,256]{2,1,0:T(8,128)(2,1)S(1)}, u32[]{:S(2)}, u32[]{:S(2)}) async-start(bf16[32,22,256]{2,1,0:T(8,128)(2,1)} %reshape.117), calls=%async_computation.5 | async-start | bytes 786432 | tf_op jit(solution)/shard_map/all_to_all | solution.py:249
  172.8 9.4 %collective-permute-start.13 = (bf16[272,256]{1,0:T(8,128)(2,1)S(1)}, bf16[272,256]{1,0:T(8,128)(2,1)S(1)}, u32[]{:S(2)}, u32[]{:S(2)}) collective-permute-start(bf16[272,256]{1,0:T(8,128)(2,1)S(1)} %get-tuple-element.15), channel_id=1, source_target_pairs={{0,4},{4,8},{8,12},{12,0},{1,5},{5,9},{9,13},{13,1},{2,6},{6,10},{... | collective-permute-start | bytes 417800 | tf_op jit(solution)/shard_map/ppermute | solution.py:254
  175.0 8.7 %collective-permute-start.12 = (bf16[272,256]{1,0:T(8,128)(2,1)S(1)}, bf16[272,256]{1,0:T(8,128)(2,1)S(1)}, u32[]{:S(2)}, u32[]{:S(2)}) collective-permute-start(bf16[272,256]{1,0:T(8,128)(2,1)S(1)} %get-tuple-element.14), channel_id=1, source_target_pairs={{0,8},{4,12},{8,0},{12,4},{1,9},{5,13},{9,1},{13,5},{2,10},{6,14},... | collective-permute-start | bytes 417800 | tf_op jit(solution)/shard_map/ppermute | solution.py:254
  179.1 7.1 %collective-permute-start.11 = (bf16[272,256]{1,0:T(8,128)(2,1)S(1)}, bf16[272,256]{1,0:T(8,128)(2,1)S(1)}, u32[]{:S(2)}, u32[]{:S(2)}) collective-permute-start(bf16[272,256]{1,0:T(8,128)(2,1)S(1)} %get-tuple-element.13), channel_id=1, source_target_pairs={{0,12},{4,0},{8,4},{12,8},{1,13},{5,1},{9,5},{13,9},{2,14},{6,2},{... | collective-permute-start | bytes 417800 | tf_op jit(solution)/shard_map/ppermute | solution.py:254

commit v5 on v4

--- a/solution.py
+++ b/solution.py
@@ -115,7 +115,9 @@
     blocks, cap, _ = out_ref.shape
     count = rows_ref.shape[0]
     lane = lax.broadcasted_iota(jnp.int32, (count, blocks), 1)
-    ids = [ids_ref[:, k : k + 1] for k in range(2)]
+    ids = [
+        jnp.transpose(jnp.broadcast_to(ids_ref[k : k + 1, :], (8, count)))[:, 0:1] for k in range(2)
+    ]
     marks = [(lane == ids[k]).astype(F32) for k in range(2)]
     down = lax.broadcasted_iota(jnp.int32, (count, count), 0)
     across = lax.broadcasted_iota(jnp.int32, (count, count), 1)
@@ -255,11 +257,10 @@
 
 
 def keys_everywhere(mine):
-    by = lax.axis_size("z") // 2
-    while by:
+    size = lax.axis_size("z")
+    for by in (size // 4, size // 2, size // 8, size // 16):
         came = shift(mine, "z", by)
         mine = jnp.concatenate([mine, came], axis=0)
-        by //= 2
     return mine, shift(mine, "c", 1)
 
 
@@ -309,7 +310,7 @@
             jax.ShapeDtypeStruct((length, 2), jnp.int32),
         ],
         name="route",
-    )(route_ids, expert_input)
+    )(route_ids.T, expert_input)
     arrived = swap(outgoing, EP).reshape(slot_total, piece)
 
     gate_view = expert_gate.reshape(SIDE, SIDE, piece, hid)
@@ -360,7 +361,8 @@
     expert_out = expert_out.reshape(experts_count, CAP, piece)
 
     heads_out = attend(query_turned, mine, other)
-    heads = [heads_out] + [shift(heads_out, "x", by) for by in range(1, SIDE)]
+    heads = [heads_out, shift(heads_out, "x", 1)]
+    heads += [shift(heads_out, "x", by) for by in range(2, SIDE)]
     mix_partial = mix(
         heads,
         second_weights,

time: 202 us -> 198 us (0.980)
  waiting for transfers between devices: 43.4 us -> 36.7 us
  starting transfers between devices: 106 us -> 110 us
    ppermute x17, starting transfers between devices: 60.5 us -> 67.2 us  [shift(): lax.ppermute(array, axis, [(k, (k + by) % size) for k in range(size)])]
    ppermute x17, waiting for transfers between devices: 17 us -> 12.4 us  [shift(): lax.ppermute(array, axis, [(k, (k + by) % size) for k in range(size)])]
    all_to_all x6, starting transfers between devices: 45.5 us -> 43.3 us  [swap(): return lax.all_to_all(array, axis, 0, 0, tiled=True)]
    all_to_all x6, waiting for transfers between devices: 26.5 us -> 24.4 us  [swap(): return lax.all_to_all(array, axis, 0, 0, tiled=True)]
    unnamed x45 -> x42, local copies, waits for them, and re-layouts: 5.14 us -> 3.55 us
  transfers between devices with their start and end apart: 23 -> 23, of which waited for: 8 -> 6; matrix products, arithmetic and copies ran while one was open for 12% -> 13% of each run, Pallas kernels for 9% -> 9%
where the time goes in v5:
time: 198 us; the launch traced here: 197 us
  starting transfers between devices  110 us (56%)
  waiting for transfers between devices  36.7 us (19%)
  Pallas kernels  21.2 us (11%)
  local copies, waits for them, and re-layouts  13.6 us (7%)
  other arithmetic  12.5 us (6%)
    ppermute x17, starting transfers between devices, shift(): lax.ppermute(array, axis, [(k, (k + by) % size) for k in range(size)])  67.2 us
    all_to_all x6, starting transfers between devices, swap(): return lax.all_to_all(array, axis, 0, 0, tiled=True)  43.3 us
    all_to_all x6, waiting for transfers between devices, swap(): return lax.all_to_all(array, axis, 0, 0, tiled=True)  24.4 us
    ppermute x17, waiting for transfers between devices, shift(): lax.ppermute(array, axis, [(k, (k + by) % size) for k in range(size)])  12.4 us
    pallas_call x1, Pallas kernels, attend(): pl.pallas_call(attend_body, out_shape=jax.ShapeDtypeStruct(query_turned.s...  7.2 us
    pallas_call x2, Pallas kernels, mix(): pl.pallas_call(functools.partial(mix_body, k_rows, base, joined), out_sha...  5.32 us
  transfers between devices with their start and end apart: 23, of which 6 were waited for; matrix products, arithmetic and copies ran while one was open for 13% of the time, Pallas kernels for 9%

profile of v5, /device:TPU:1, one launch (start us, length us, event | category | flops | bytes accessed | tf_op | source)
XLA Modules:
  0.0 197.1 jit_solution(3702529259399318500)
XLA Ops:
  0.6 2.6 %route.1 = (bf16[32,22,256]{2,1,0:T(8,128)(2,1)}, s32[256,2]{1,0:T(8,128)}) custom-call(s32[2,256]{1,0:T(2,128)} %bitcast.61, bf16[256,256]{1,0:T(8,128)(2,1)} %rows_ref.1), custom_call_target="tpu_custom_call" | custom-call | tf_op jit(solution)/shard_map/route/pallas_call | solution.py:306
  3.2 16.7 %all-to-all-start = ((bf16[32,22,256]{2,1,0:T(8,128)(2,1)}), bf16[32,22,256]{2,1,0:T(8,128)(2,1)S(1)}, u32[]{:S(2)}, u32[]{:S(2)}) async-start(bf16[32,22,256]{2,1,0:T(8,128)(2,1)} %get-tuple-element.17), calls=%async_computation | async-start | bytes 786432 | tf_op jit(solution)/shard_map/all_to_all | solution.py:251
  20.0 2.4 %constant_dynamic-slice_fusion = (bf16[4,1,256,128]{3,2,1,0:T(8,128)(2,1)S(1)}, bf16[4,1,256,128]{3,2,1,0:T(8,128)(2,1)S(1)}, bf16[4,1,256,128]{3,2,1,0:T(8,128)...) fusion(bf16[4,4,256,128]{3,2,1,0:T(8,128)(2,1)} %bitcast.51, ...), kind=kLoop, calls=%fused_computation.44 | loop fusion | bytes 4194320 | tf_op jit(solution)/shard_map/jit(dynamic_index_in_dim)/dynamic_slice | solution.py:320
  22.4 0.9 pad_maximum_fusion.6
  23.2 3.1 %collective-permute-start.14 = (bf16[1024,256]{1,0:T(8,128)(2,1)}, bf16[1024,256]{1,0:T(8,128)(2,1)S(1)}, u32[]{:S(2)}, u32[]{:S(2)}) collective-permute-start(bf16[1024,256]{1,0:T(8,128)(2,1)} %pad_maximum_fusion.6), channel_id=1, source_target_pairs={{0,1},{1,2},{2,3},{3,0},{4,5},{5,6},{6,7},{7,4},{8,9},{9,10},{10,1... | collective-permute-start | bytes 1572872 | tf_op jit(solution)/shard_map/ppermute | solution.py:256
  26.4 0.8 pad_maximum_fusion.7
  27.2 4.3 %collective-permute-start.15 = (bf16[1024,256]{1,0:T(8,128)(2,1)}, bf16[1024,256]{1,0:T(8,128)(2,1)S(1)}, u32[]{:S(2)}, u32[]{:S(2)}) collective-permute-start(bf16[1024,256]{1,0:T(8,128)(2,1)} %pad_maximum_fusion.7), channel_id=1, source_target_pairs={{0,2},{1,3},{2,0},{3,1},{4,6},{5,7},{6,4},{7,5},{8,10},{9,11},{10,... | collective-permute-start | bytes 1572872 | tf_op jit(solution)/shard_map/ppermute | solution.py:256
  31.6 0.8 pad_maximum_fusion.8
  32.4 3.1 %collective-permute-start.16 = (bf16[1024,256]{1,0:T(8,128)(2,1)}, bf16[1024,256]{1,0:T(8,128)(2,1)}, u32[]{:S(2)}, u32[]{:S(2)}) collective-permute-start(bf16[1024,256]{1,0:T(8,128)(2,1)} %pad_maximum_fusion.8), channel_id=1, source_target_pairs={{0,3},{1,0},{2,1},{3,2},{4,7},{5,4},{6,5},{7,6},{8,11},{9,8},{10,9... | collective-permute-start | bytes 1572872 | tf_op jit(solution)/shard_map/ppermute | solution.py:256
  35.5 12.2 %all-to-all-done = bf16[32,22,256]{2,1,0:T(8,128)(2,1)S(1)} async-done(((bf16[32,22,256]{2,1,0:T(8,128)(2,1)}), bf16[32,22,256]{2,1,0:T(8,128)(2,1)S(1)}, u32[]{:S(2)}, u32[]{:S(2)}) %all-to-all-start) | async-done | bytes 360480 | tf_op jit(solution)/shard_map/all_to_all | solution.py:251
  47.8 1.2 broadcast_in_dim.58
  49.0 4.3 %all-to-all-start.1 = ((bf16[4,704,256]{2,1,0:T(8,128)(2,1)}), bf16[4,704,256]{2,1,0:T(8,128)(2,1)S(1)}, u32[]{:S(2)}, u32[]{:S(2)}) async-start(bf16[4,704,256]{2,1,0:T(8,128)(2,1)} %broadcast_in_dim.58), calls=%async_computation.1 | async-start | bytes 2883584 | tf_op jit(solution)/shard_map/all_to_all | solution.py:251
  53.8 0.1 copy.27
  54.0 0.7 pad_maximum_fusion.11.kv_ref
  54.7 1.3 sine_multiply_fusion
  55.9 2.2 %turn.1 = (bf16[256,128]{1,0:T(8,128)(2,1)}, bf16[256,128]{1,0:T(8,128)(2,1)}) custom-call(bf16[256,128]{1,0:T(8,128)(2,1)} %q_ref.1, bf16[256,128]{1,0:T(8,128)(2,1)} %pad_maximum_fusion.11.kv_ref, f32[1,64]{1,0:T(1,128)} %bitcast.64, f32[1,64]{1,0:T(1,128)} %bitcast.65, f32[256,128]{1,0:T(8,128)} %get-tuple-element.37.cos_ref, ...), custom_call_target="tpu_custom_call" | custom-call | tf_op jit(solution)/shard_map/turn/pallas_call | solution.py:62
  58.1 1.9 collective-permute-start
  60.2 1.1 pad_maximum_fusion.5.refs_1_
  61.2 2.1 %dynamic-slice_bitcast_fusion = (bf16[512,256]{1,0:T(8,128)(2,1)}, bf16[512,256]{1,0:T(8,128)(2,1)}, bf16[512,256]{1,0:T(8,128)(2,1)S(1)}, bf16[512,256]{1,0:T(8,128)(2,1)}) fusion(bf16[1,2048,256]{2,1,0:T(8,128)(2,1)} %param.27, s32[]{:T(128)S(6)} %select_n.134, s32[]{:T(128)S(6)} %select_n.130, s32[]{:T(128)S(6)} %select_n.128, s32[]{:T(128)S(6)} %select_n.132), kind=kLoop, calls=%fused_computation.19 | loop fusion | bytes 2097168 | tf_op jit(solution)/shard_map/dynamic_slice | solution.py:324
  63.5 4.6 %collective-permute-done = bf16[256,128]{1,0:T(8,128)(2,1)S(1)} collective-permute-done((bf16[256,128]{1,0:T(8,128)(2,1)}, bf16[256,128]{1,0:T(8,128)(2,1)S(1)}, u32[]{:S(2)}, u32[]{:S(2)}) %collective-permute-start) | collective-permute-done | bytes 65568 | tf_op jit(solution)/shard_map/ppermute | solution.py:256
  68.0 0.6 copy-done.10
  68.7 0.7 pad_maximum_fusion.10
  69.3 2.8 %collective-permute-start.1 = (bf16[512,128]{1,0:T(8,128)(2,1)}, bf16[512,128]{1,0:T(8,128)(2,1)S(1)}, u32[]{:S(2)}, u32[]{:S(2)}) collective-permute-start(bf16[512,128]{1,0:T(8,128)(2,1)} %pad_maximum_fusion.10), channel_id=1, source_target_pairs={{0,256},{32,288},{64,320},{96,352},{128,384},{160,416},{192,448},{... | collective-permute-start | bytes 393224 | tf_op jit(solution)/shard_map/ppermute | solution.py:256
  72.2 4.1 %shard_map.150 = bf16[4,720,256]{2,1,0:T(8,128)(2,1)} custom-call(s32[12]{0:T(128)S(1)} %pad_add_fusion.1.index_ref, bf16[4,704,256]{2,1,0:T(8,128)(2,1)S(1)} %all-to-all-done.1.refs_0_, bf16[1024,256]{1,0:T(8,128)(2,1)S(1)} %pad_maximum_fusion.5.refs_1_, bf16[1024,256]{1,0:T(8,128)(2,1)S(1)} %collective-permute-done.14.refs_2_, ...), custom_call_target="tpu_custom_call" | custom-call | flops 1476395008 | bytes 2883584 | tf_op jit(solution)/shard_map/pallas_call | solution.py:191
  76.3 4.1 %all-to-all-start.2 = ((bf16[4,720,256]{2,1,0:T(8,128)(2,1)}), bf16[4,720,256]{2,1,0:T(8,128)(2,1)S(1)}, u32[]{:S(2)}, u32[]{:S(2)}) async-start(bf16[4,720,256]{2,1,0:T(8,128)(2,1)} %shard_map.150), calls=%async_computation.2 | async-start | bytes 2949120 | tf_op jit(solution)/shard_map/all_to_all | solution.py:251
  80.4 3.8 %collective-permute-done.1 = bf16[512,128]{1,0:T(8,128)(2,1)S(1)} collective-permute-done((bf16[512,128]{1,0:T(8,128)(2,1)}, bf16[512,128]{1,0:T(8,128)(2,1)S(1)}, u32[]{:S(2)}, u32[]{:S(2)}) %collective-permute-start.1) | collective-permute-done | bytes 131104 | tf_op jit(solution)/shard_map/ppermute | solution.py:256
  84.3 12.9 %collective-permute-start.2 = (bf16[1024,128]{1,0:T(8,128)(2,1)S(1)}, bf16[1024,128]{1,0:T(8,128)(2,1)S(1)}, u32[]{:S(2)}, u32[]{:S(2)}) collective-permute-start(bf16[1024,128]{1,0:T(8,128)(2,1)S(1)} %pad_maximum_fusion.9), channel_id=1, source_target_pairs={{0,64},{32,96},{64,128},{96,160},{128,192},{160,224},{192,256},{22... | collective-permute-start | bytes 786440 | tf_op jit(solution)/shard_map/ppermute | solution.py:256
  97.2 0.8 constant_dynamic-slice_fusion.8
  98.0 0.8 pad_maximum_fusion.4
  98.9 1.9 collective-permute-start.10
  100.8 0.8 pad_maximum_fusion.2
  101.6 3.3 %collective-permute-start.8 = (bf16[1024,256]{1,0:T(8,128)(2,1)}, bf16[1024,256]{1,0:T(8,128)(2,1)S(1)}, u32[]{:S(2)}, u32[]{:S(2)}) collective-permute-start(bf16[1024,256]{1,0:T(8,128)(2,1)} %pad_maximum_fusion.2), channel_id=1, source_target_pairs={{0,4},{4,8},{8,12},{12,0},{1,5},{5,9},{9,13},{13,1},{2,6},{6,10},{... | collective-permute-start | bytes 1572872 | tf_op jit(solution)/shard_map/ppermute | solution.py:256
  105.0 0.9 pad_maximum_fusion
  105.9 1.9 collective-permute-start.3
  107.8 0.8 pad_maximum_fusion.3
  108.6 4.1 %collective-permute-start.9 = (bf16[1024,256]{1,0:T(8,128)(2,1)}, bf16[1024,256]{1,0:T(8,128)(2,1)S(1)}, u32[]{:S(2)}, u32[]{:S(2)}) collective-permute-start(bf16[1024,256]{1,0:T(8,128)(2,1)} %pad_maximum_fusion.3), channel_id=1, source_target_pairs={{0,8},{4,12},{8,0},{12,4},{1,9},{5,13},{9,1},{13,5},{2,10},{6,14},... | collective-permute-start | bytes 1572872 | tf_op jit(solution)/shard_map/ppermute | solution.py:256
  112.8 0.6 constant_dynamic-update-slice_fusion.4
  113.4 0.6 constant_dynamic-update-slice_fusion.3
  114.0 0.7 constant_dynamic-update-slice_fusion.2
  114.7 1.3 hidden.1
  116.0 4.1 %all-to-all-start.3 = ((bf16[4,704,128]{2,1,0:T(8,128)(2,1)}), bf16[4,704,128]{2,1,0:T(8,128)(2,1)S(1)}, u32[]{:S(2)}, u32[]{:S(2)}) async-start(bf16[4,704,128]{2,1,0:T(8,128)(2,1)} %hidden.1), calls=%async_computation.3 | async-start | bytes 1441792 | tf_op jit(solution)/shard_map/all_to_all | solution.py:251
  120.0 0.7 constant_dynamic-update-slice_fusion.1
  120.8 1.9 constant_dynamic-update-slice_fusion.mine_ref
  122.7 7.3 %collective-permute-start.4 = (bf16[4096,128]{1,0:T(8,128)(2,1)}, bf16[4096,128]{1,0:T(8,128)(2,1)}, u32[]{:S(2)}, u32[]{:S(2)}) collective-permute-start(bf16[4096,128]{1,0:T(8,128)(2,1)} %constant_dynamic-update-slice_fusion.mine_ref), channel_id=1, source_target_pairs={{0,16},{16,0},{1,17},{17,1},{2,18},{18,2},{3,19},{19,3},{4,20},{20... | collective-permute-start | bytes 3145736 | tf_op jit(solution)/shard_map/ppermute | solution.py:256
  130.1 2.6 %second.1 = bf16[4,704,256]{2,1,0:T(8,128)(2,1)} custom-call(s32[4]{0:T(128)S(1)} %and_select_fusion.index_ref, bf16[4,704,128]{2,1,0:T(8,128)(2,1)S(1)} %all-to-all-done.3.gathered, bf16[1024,256]{1,0:T(8,128)(2,1)S(1)} %pad_maximum_fusion.1.refs_4_.refs_0_, bf16[1024,256]{1,0:T(8,128)(2,1)S(1)} %collective-permute-done.8.refs_5_.refs_1_, ...), custom_call_target="tpu_custom_call" | custom-call | tf_op jit(solution)/shard_map/second/pallas_call | solution.py:351
  132.7 4.6 %all-to-all-start.4 = ((bf16[4,704,256]{2,1,0:T(8,128)(2,1)}), bf16[4,704,256]{2,1,0:T(8,128)(2,1)}, u32[]{:S(2)}, u32[]{:S(2)}) async-start(bf16[4,704,256]{2,1,0:T(8,128)(2,1)} %second.1), calls=%async_computation.4 | async-start | bytes 2883584 | tf_op jit(solution)/shard_map/all_to_all | solution.py:251
  137.3 0.2 slice_reduce_fusion
  137.6 7.2 %attend.1.refs_0_ = bf16[256,128]{1,0:T(8,128)(2,1)S(1)} custom-call(bf16[256,128]{1,0:T(8,128)(2,1)S(1)} %copy-done.1, bf16[4096,128]{1,0:T(8,128)(2,1)} %constant_dynamic-update-slice_fusion.mine_ref, bf16[4096,128]{1,0:T(8,128)(2,1)} %collective-permute-done.4.other_ref), custom_call_target="tpu_custom_call" | custom-call | flops 2147483648 | bytes 2097152 | tf_op jit(solution)/shard_map/attend/pallas_call | solution.py:101
  144.8 3.7 %collective-permute-start.5 = (bf16[256,128]{1,0:T(8,128)(2,1)S(1)}, bf16[256,128]{1,0:T(8,128)(2,1)S(1)}, u32[]{:S(2)}, u32[]{:S(2)}) collective-permute-start(bf16[256,128]{1,0:T(8,128)(2,1)S(1)} %attend.1.refs_0_), channel_id=1, source_target_pairs={{0,1},{1,2},{2,3},{3,0},{4,5},{5,6},{6,7},{7,4},{8,9},{9,10},{10,1... | collective-permute-start | bytes 196616 | tf_op jit(solution)/shard_map/ppermute | solution.py:256
  148.5 4.3 %collective-permute-start.6 = (bf16[256,128]{1,0:T(8,128)(2,1)S(1)}, bf16[256,128]{1,0:T(8,128)(2,1)S(1)}, u32[]{:S(2)}, u32[]{:S(2)}) collective-permute-start(bf16[256,128]{1,0:T(8,128)(2,1)S(1)} %attend.1.refs_0_), channel_id=1, source_target_pairs={{0,2},{1,3},{2,0},{3,1},{4,6},{5,7},{6,4},{7,5},{8,10},{9,11},{10,... | collective-permute-start | bytes 196616 | tf_op jit(solution)/shard_map/ppermute | solution.py:256
  152.8 3.1 %collective-permute-start.7 = (bf16[256,128]{1,0:T(8,128)(2,1)S(1)}, bf16[256,128]{1,0:T(8,128)(2,1)S(1)}, u32[]{:S(2)}, u32[]{:S(2)}) collective-permute-start(bf16[256,128]{1,0:T(8,128)(2,1)S(1)} %attend.1.refs_0_), channel_id=1, source_target_pairs={{0,3},{1,0},{2,1},{3,2},{4,7},{5,4},{6,5},{7,6},{8,11},{9,8},{10,9... | collective-permute-start | bytes 196616 | tf_op jit(solution)/shard_map/ppermute | solution.py:256
  155.9 1.7 reduce_sum.22
  157.7 0.8 reshape.117
  158.5 9.4 %all-to-all-start.5 = ((bf16[32,22,256]{2,1,0:T(8,128)(2,1)}), bf16[32,22,256]{2,1,0:T(8,128)(2,1)S(1)}, u32[]{:S(2)}, u32[]{:S(2)}) async-start(bf16[32,22,256]{2,1,0:T(8,128)(2,1)} %reshape.117), calls=%async_computation.5 | async-start | bytes 786432 | tf_op jit(solution)/shard_map/all_to_all | solution.py:251
  168.0 1.2 shard_map.149
  169.2 2.2 %collective-permute-start.13 = (bf16[272,256]{1,0:T(8,128)(2,1)S(1)}, bf16[272,256]{1,0:T(8,128)(2,1)S(1)}, u32[]{:S(2)}, u32[]{:S(2)}) collective-permute-start(bf16[272,256]{1,0:T(8,128)(2,1)S(1)} %get-tuple-element.15), channel_id=1, source_target_pairs={{0,4},{4,8},{8,12},{12,0},{1,5},{5,9},{9,13},{13,1},{2,6},{6,10},{... | collective-permute-start | bytes 417800 | tf_op jit(solution)/shard_map/ppermute | solution.py:256
  171.4 4.1 %collective-permute-start.12 = (bf16[272,256]{1,0:T(8,128)(2,1)S(1)}, bf16[272,256]{1,0:T(8,128)(2,1)S(1)}, u32[]{:S(2)}, u32[]{:S(2)}) collective-permute-start(bf16[272,256]{1,0:T(8,128)(2,1)S(1)} %get-tuple-element.14), channel_id=1, source_target_pairs={{0,8},{4,12},{8,0},{12,4},{1,9},{5,13},{9,1},{13,5},{2,10},{6,14},... | collective-permute-start | bytes 417800 | tf_op jit(solution)/shard_map/ppermute | solution.py:256
  175.6 3.1 %collective-permute-start.11 = (bf16[272,256]{1,0:T(8,128)(2,1)S(1)}, bf16[272,256]{1,0:T(8,128)(2,1)S(1)}, u32[]{:S(2)}, u32[]{:S(2)}) collective-permute-start(bf16[272,256]{1,0:T(8,128)(2,1)S(1)} %get-tuple-element.13), channel_id=1, source_target_pairs={{0,12},{4,0},{8,4},{12,8},{1,13},{5,1},{9,5},{13,9},{2,14},{6,2},{... | collective-permute-start | bytes 417800 | tf_op jit(solution)/shard_map/ppermute | solution.py:256
  178.7 1.5 collective-permute-done.12
  180.2 2.4 %collective-permute-done.11 = bf16[272,256]{1,0:T(8,128)(2,1)S(1)} collective-permute-done((bf16[272,256]{1,0:T(8,128)(2,1)S(1)}, bf16[272,256]{1,0:T(8,128)(2,1)S(1)}, u32[]{:S(2)}, u32[]{:S(2)}) %collective-permute-start.11) | collective-permute-done | bytes 139296 | tf_op jit(solution)/shard_map/ppermute | solution.py:256
  182.7 0.8 multiply_convert_fusion
  183.4 12.2 %all-to-all-done.5 = bf16[32,22,256]{2,1,0:T(8,128)(2,1)S(1)} async-done(((bf16[32,22,256]{2,1,0:T(8,128)(2,1)}), bf16[32,22,256]{2,1,0:T(8,128)(2,1)S(1)}, u32[]{:S(2)}, u32[]{:S(2)}) %all-to-all-start.5) | async-done | bytes 360480 | tf_op jit(solution)/shard_map/all_to_all | solution.py:251
  195.8 0.3 convolution_multiply_fusion.1
  196.1 1.0 fusion.1
  (81 shorter events, 1.1 us)
Async XLA Ops:
  3.2 44.5 %all-to-all-start = ((bf16[32,22,256]{2,1,0:T(8,128)(2,1)}), bf16[32,22,256]{2,1,0:T(8,128)(2,1)S(1)}, u32[]{:S(2)}, u32[]{:S(2)}) async-start(bf16[32,22,256]{2,1,0:T(8,128)(2,1)} %get-tuple-element.17), calls=%async_computation | async-start | bytes 786432 | tf_op jit(solution)/shard_map/all_to_all | solution.py:251
  23.2 48.9 %collective-permute-start.14 = (bf16[1024,256]{1,0:T(8,128)(2,1)}, bf16[1024,256]{1,0:T(8,128)(2,1)S(1)}, u32[]{:S(2)}, u32[]{:S(2)}) collective-permute-start(bf16[1024,256]{1,0:T(8,128)(2,1)} %pad_maximum_fusion.6), channel_id=1, source_target_pairs={{0,1},{1,2},{2,3},{3,0},{4,5},{5,6},{6,7},{7,4},{8,9},{9,10},{10,1... | collective-permute-start | bytes 1572872 | tf_op jit(solution)/shard_map/ppermute | solution.py:256
  27.2 45.0 %collective-permute-start.15 = (bf16[1024,256]{1,0:T(8,128)(2,1)}, bf16[1024,256]{1,0:T(8,128)(2,1)S(1)}, u32[]{:S(2)}, u32[]{:S(2)}) collective-permute-start(bf16[1024,256]{1,0:T(8,128)(2,1)} %pad_maximum_fusion.7), channel_id=1, source_target_pairs={{0,2},{1,3},{2,0},{3,1},{4,6},{5,7},{6,4},{7,5},{8,10},{9,11},{10,... | collective-permute-start | bytes 1572872 | tf_op jit(solution)/shard_map/ppermute | solution.py:256
  32.4 39.8 %collective-permute-start.16 = (bf16[1024,256]{1,0:T(8,128)(2,1)}, bf16[1024,256]{1,0:T(8,128)(2,1)}, u32[]{:S(2)}, u32[]{:S(2)}) collective-permute-start(bf16[1024,256]{1,0:T(8,128)(2,1)} %pad_maximum_fusion.8), channel_id=1, source_target_pairs={{0,3},{1,0},{2,1},{3,2},{4,7},{5,4},{6,5},{7,6},{8,11},{9,8},{10,9... | collective-permute-start | bytes 1572872 | tf_op jit(solution)/shard_map/ppermute | solution.py:256
  49.0 4.7 %copy-start.14 = (bf16[256,64]{0,1:T(8,128)(2,1)S(1)}, bf16[256,64]{0,1:T(8,128)(2,1)}, u32[]{:S(2)}) copy-start(bf16[256,64]{0,1:T(8,128)(2,1)} %param.15) | copy-start | bytes 98308
  49.0 4.8 %copy-start.15 = (bf16[256,64]{0,1:T(8,128)(2,1)S(1)}, bf16[256,64]{0,1:T(8,128)(2,1)}, u32[]{:S(2)}) copy-start(bf16[256,64]{0,1:T(8,128)(2,1)} %param.16) | copy-start | bytes 98308
  49.0 11.1 %copy-start.16 = (f32[4096]{0:T(1024)S(1)}, f32[4096]{0:T(1024)}, u32[]{:S(2)}) copy-start(f32[4096]{0:T(1024)} %param.22) | copy-start | bytes 49156
  49.0 23.2 %all-to-all-start.1 = ((bf16[4,704,256]{2,1,0:T(8,128)(2,1)}), bf16[4,704,256]{2,1,0:T(8,128)(2,1)S(1)}, u32[]{:S(2)}, u32[]{:S(2)}) async-start(bf16[4,704,256]{2,1,0:T(8,128)(2,1)} %broadcast_in_dim.58), calls=%async_computation.1 | async-start | bytes 2883584 | tf_op jit(solution)/shard_map/all_to_all | solution.py:251
  58.1 9.9 %collective-permute-start = (bf16[256,128]{1,0:T(8,128)(2,1)}, bf16[256,128]{1,0:T(8,128)(2,1)S(1)}, u32[]{:S(2)}, u32[]{:S(2)}) collective-permute-start(bf16[256,128]{1,0:T(8,128)(2,1)} %get-tuple-element.11), channel_id=1, source_target_pairs={{0,128},{32,160},{64,192},{96,224},{128,256},{160,288},{192,320},{... | collective-permute-start | bytes 196616 | tf_op jit(solution)/shard_map/ppermute | solution.py:256
  60.2 8.5 %copy-start.9 = (bf16[256,128]{1,0:T(8,128)(2,1)S(1)}, bf16[256,128]{1,0:T(8,128)(2,1)}, u32[]{:S(2)}) copy-start(bf16[256,128]{1,0:T(8,128)(2,1)} %get-tuple-element.11) | copy-start | bytes 196612
  68.0 0.6 copy-start.10
  69.3 14.9 %collective-permute-start.1 = (bf16[512,128]{1,0:T(8,128)(2,1)}, bf16[512,128]{1,0:T(8,128)(2,1)S(1)}, u32[]{:S(2)}, u32[]{:S(2)}) collective-permute-start(bf16[512,128]{1,0:T(8,128)(2,1)} %pad_maximum_fusion.10), channel_id=1, source_target_pairs={{0,256},{32,288},{64,320},{96,352},{128,384},{160,416},{192,448},{... | collective-permute-start | bytes 393224 | tf_op jit(solution)/shard_map/ppermute | solution.py:256
  76.3 8.0 %copy-start.11 = (bf16[256,128]{1,0:T(8,128)(2,1)S(1)}, bf16[256,128]{1,0:T(8,128)(2,1)}, u32[]{:S(2)}) copy-start(bf16[256,128]{1,0:T(8,128)(2,1)} %copy-done.10) | copy-start | bytes 196612
  76.3 20.9 %copy-start.2 = (bf16[2048,256]{1,0:T(8,128)(2,1)S(1)}, bf16[2048,256]{1,0:T(8,128)(2,1)}, u32[]{:S(2)}) copy-start(bf16[2048,256]{1,0:T(8,128)(2,1)} %param.20) | copy-start | bytes 3145732
  76.3 38.4 %all-to-all-start.2 = ((bf16[4,720,256]{2,1,0:T(8,128)(2,1)}), bf16[4,720,256]{2,1,0:T(8,128)(2,1)S(1)}, u32[]{:S(2)}, u32[]{:S(2)}) async-start(bf16[4,720,256]{2,1,0:T(8,128)(2,1)} %shard_map.150), calls=%async_computation.2 | async-start | bytes 2949120 | tf_op jit(solution)/shard_map/all_to_all | solution.py:251
  80.4 17.6 %copy-start.6 = (bf16[512,256]{1,0:T(8,128)(2,1)S(1)}, bf16[512,256]{1,0:T(8,128)(2,1)}, u32[]{:S(2)}) copy-start(bf16[512,256]{1,0:T(8,128)(2,1)} %get-tuple-element.28) | copy-start | bytes 786436
  84.3 16.5 %copy-start.5 = (bf16[512,256]{1,0:T(8,128)(2,1)S(1)}, bf16[512,256]{1,0:T(8,128)(2,1)}, u32[]{:S(2)}) copy-start(bf16[512,256]{1,0:T(8,128)(2,1)} %get-tuple-element.29) | copy-start | bytes 786436
  84.3 20.7 %collective-permute-start.2 = (bf16[1024,128]{1,0:T(8,128)(2,1)S(1)}, bf16[1024,128]{1,0:T(8,128)(2,1)S(1)}, u32[]{:S(2)}, u32[]{:S(2)}) collective-permute-start(bf16[1024,128]{1,0:T(8,128)(2,1)S(1)} %pad_maximum_fusion.9), channel_id=1, source_target_pairs={{0,64},{32,96},{64,128},{96,160},{128,192},{160,224},{192,256},{22... | collective-permute-start | bytes 786440 | tf_op jit(solution)/shard_map/ppermute | solution.py:256
  98.0 7.0 %copy-start.12 = (bf16[256,128]{1,0:T(8,128)(2,1)S(1)}, bf16[256,128]{1,0:T(8,128)(2,1)}, u32[]{:S(2)}) copy-start(bf16[256,128]{1,0:T(8,128)(2,1)} %copy-done.10) | copy-start | bytes 196612
  98.0 9.8 %copy-start.3 = (bf16[512,256]{1,0:T(8,128)(2,1)S(1)}, bf16[512,256]{1,0:T(8,128)(2,1)}, u32[]{:S(2)}) copy-start(bf16[512,256]{1,0:T(8,128)(2,1)} %get-tuple-element.31) | copy-start | bytes 786436
  98.9 31.2 %collective-permute-start.10 = (bf16[1024,256]{1,0:T(8,128)(2,1)}, bf16[1024,256]{1,0:T(8,128)(2,1)S(1)}, u32[]{:S(2)}, u32[]{:S(2)}) collective-permute-start(bf16[1024,256]{1,0:T(8,128)(2,1)} %pad_maximum_fusion.4), channel_id=1, source_target_pairs={{0,12},{4,0},{8,4},{12,8},{1,13},{5,1},{9,5},{13,9},{2,14},{6,2},{... | collective-permute-start | bytes 1572872 | tf_op jit(solution)/shard_map/ppermute | solution.py:256
  101.6 28.4 %collective-permute-start.8 = (bf16[1024,256]{1,0:T(8,128)(2,1)}, bf16[1024,256]{1,0:T(8,128)(2,1)S(1)}, u32[]{:S(2)}, u32[]{:S(2)}) collective-permute-start(bf16[1024,256]{1,0:T(8,128)(2,1)} %pad_maximum_fusion.2), channel_id=1, source_target_pairs={{0,4},{4,8},{8,12},{12,0},{1,5},{5,9},{9,13},{13,1},{2,6},{6,10},{... | collective-permute-start | bytes 1572872 | tf_op jit(solution)/shard_map/ppermute | solution.py:256
  105.0 9.0 %copy-start.7 = (bf16[1024,128]{1,0:T(8,128)(2,1)}, bf16[1024,128]{1,0:T(8,128)(2,1)S(1)}, u32[]{:S(2)}) copy-start(bf16[1024,128]{1,0:T(8,128)(2,1)S(1)} %collective-permute-done.2) | copy-start | bytes 786436
  105.9 14.9 %collective-permute-start.3 = (bf16[2048,128]{1,0:T(8,128)(2,1)}, bf16[2048,128]{1,0:T(8,128)(2,1)}, u32[]{:S(2)}, u32[]{:S(2)}) collective-permute-start(bf16[2048,128]{1,0:T(8,128)(2,1)} %pad_maximum_fusion), channel_id=1, source_target_pairs={{0,32},{32,64},{64,96},{96,128},{128,160},{160,192},{192,224},{224... | collective-permute-start | bytes 1572872 | tf_op jit(solution)/shard_map/ppermute | solution.py:256
  108.6 21.4 %collective-permute-start.9 = (bf16[1024,256]{1,0:T(8,128)(2,1)}, bf16[1024,256]{1,0:T(8,128)(2,1)S(1)}, u32[]{:S(2)}, u32[]{:S(2)}) collective-permute-start(bf16[1024,256]{1,0:T(8,128)(2,1)} %pad_maximum_fusion.3), channel_id=1, source_target_pairs={{0,8},{4,12},{8,0},{12,4},{1,9},{5,13},{9,1},{13,5},{2,10},{6,14},... | collective-permute-start | bytes 1572872 | tf_op jit(solution)/shard_map/ppermute | solution.py:256
  116.0 4.1 %copy-start.8 = (bf16[1024,128]{1,0:T(8,128)(2,1)S(1)}, bf16[1024,128]{1,0:T(8,128)(2,1)}, u32[]{:S(2)}) copy-start(bf16[1024,128]{1,0:T(8,128)(2,1)} %copy-done.7) | copy-start | bytes 786436
  116.0 14.0 %copy-start.4 = (bf16[512,256]{1,0:T(8,128)(2,1)S(1)}, bf16[512,256]{1,0:T(8,128)(2,1)}, u32[]{:S(2)}) copy-start(bf16[512,256]{1,0:T(8,128)(2,1)} %get-tuple-element.34) | copy-start | bytes 786436
  116.0 14.1 %all-to-all-start.3 = ((bf16[4,704,128]{2,1,0:T(8,128)(2,1)}), bf16[4,704,128]{2,1,0:T(8,128)(2,1)S(1)}, u32[]{:S(2)}, u32[]{:S(2)}) async-start(bf16[4,704,128]{2,1,0:T(8,128)(2,1)} %hidden.1), calls=%async_computation.3 | async-start | bytes 1441792 | tf_op jit(solution)/shard_map/all_to_all | solution.py:251
  122.7 14.9 %collective-permute-start.4 = (bf16[4096,128]{1,0:T(8,128)(2,1)}, bf16[4096,128]{1,0:T(8,128)(2,1)}, u32[]{:S(2)}, u32[]{:S(2)}) collective-permute-start(bf16[4096,128]{1,0:T(8,128)(2,1)} %constant_dynamic-update-slice_fusion.mine_ref), channel_id=1, source_target_pairs={{0,16},{16,0},{1,17},{17,1},{2,18},{18,2},{3,19},{19,3},{4,20},{20... | collective-permute-start | bytes 3145736 | tf_op jit(solution)/shard_map/ppermute | solution.py:256
  132.7 4.7 %copy-start.13 = (s32[256,2]{1,0:T(8,128)S(1)}, s32[256,2]{1,0:T(8,128)}, u32[]{:S(2)}) copy-start(s32[256,2]{1,0:T(8,128)} %get-tuple-element.16) | copy-start | bytes 6148
  132.7 4.9 %copy-start.17 = (f32[256,2]{0,1:T(2,128)S(1)}, f32[256,2]{0,1:T(2,128)}, u32[]{:S(2)}) copy-start(f32[256,2]{0,1:T(2,128)} %param.24) | copy-start | bytes 6148
  132.7 4.9 %copy-start.1 = (bf16[256,128]{1,0:T(8,128)(2,1)S(1)}, bf16[256,128]{1,0:T(8,128)(2,1)}, u32[]{:S(2)}) copy-start(bf16[256,128]{1,0:T(8,128)(2,1)} %get-tuple-element.10.q_ref) | copy-start | bytes 196612
  132.7 23.2 %all-to-all-start.4 = ((bf16[4,704,256]{2,1,0:T(8,128)(2,1)}), bf16[4,704,256]{2,1,0:T(8,128)(2,1)}, u32[]{:S(2)}, u32[]{:S(2)}) async-start(bf16[4,704,256]{2,1,0:T(8,128)(2,1)} %second.1), calls=%async_computation.4 | async-start | bytes 2883584 | tf_op jit(solution)/shard_map/all_to_all | solution.py:251
  144.8 23.2 %copy-start = (f32[2048]{0:T(1024)S(1)}, f32[2048]{0:T(1024)}, u32[]{:S(2)}) copy-start(f32[2048]{0:T(1024)} %param.19) | copy-start | bytes 24580
  144.8 23.1 %collective-permute-start.5 = (bf16[256,128]{1,0:T(8,128)(2,1)S(1)}, bf16[256,128]{1,0:T(8,128)(2,1)S(1)}, u32[]{:S(2)}, u32[]{:S(2)}) collective-permute-start(bf16[256,128]{1,0:T(8,128)(2,1)S(1)} %attend.1.refs_0_), channel_id=1, source_target_pairs={{0,1},{1,2},{2,3},{3,0},{4,5},{5,6},{6,7},{7,4},{8,9},{9,10},{10,1... | collective-permute-start | bytes 196616 | tf_op jit(solution)/shard_map/ppermute | solution.py:256
  148.5 19.5 %collective-permute-start.6 = (bf16[256,128]{1,0:T(8,128)(2,1)S(1)}, bf16[256,128]{1,0:T(8,128)(2,1)S(1)}, u32[]{:S(2)}, u32[]{:S(2)}) collective-permute-start(bf16[256,128]{1,0:T(8,128)(2,1)S(1)} %attend.1.refs_0_), channel_id=1, source_target_pairs={{0,2},{1,3},{2,0},{3,1},{4,6},{5,7},{6,4},{7,5},{8,10},{9,11},{10,... | collective-permute-start | bytes 196616 | tf_op jit(solution)/shard_map/ppermute | solution.py:256
  152.8 15.2 %collective-permute-start.7 = (bf16[256,128]{1,0:T(8,128)(2,1)S(1)}, bf16[256,128]{1,0:T(8,128)(2,1)S(1)}, u32[]{:S(2)}, u32[]{:S(2)}) collective-permute-start(bf16[256,128]{1,0:T(8,128)(2,1)S(1)} %attend.1.refs_0_), channel_id=1, source_target_pairs={{0,3},{1,0},{2,1},{3,2},{4,7},{5,4},{6,5},{7,6},{8,11},{9,8},{10,9... | collective-permute-start | bytes 196616 | tf_op jit(solution)/shard_map/ppermute | solution.py:256
  158.5 37.2 %all-to-all-start.5 = ((bf16[32,22,256]{2,1,0:T(8,128)(2,1)}), bf16[32,22,256]{2,1,0:T(8,128)(2,1)S(1)}, u32[]{:S(2)}, u32[]{:S(2)}) async-start(bf16[32,22,256]{2,1,0:T(8,128)(2,1)} %reshape.117), calls=%async_computation.5 | async-start | bytes 786432 | tf_op jit(solution)/shard_map/all_to_all | solution.py:251
  169.2 9.4 %collective-permute-start.13 = (bf16[272,256]{1,0:T(8,128)(2,1)S(1)}, bf16[272,256]{1,0:T(8,128)(2,1)S(1)}, u32[]{:S(2)}, u32[]{:S(2)}) collective-permute-start(bf16[272,256]{1,0:T(8,128)(2,1)S(1)} %get-tuple-element.15), channel_id=1, source_target_pairs={{0,4},{4,8},{8,12},{12,0},{1,5},{5,9},{9,13},{13,1},{2,6},{6,10},{... | collective-permute-start | bytes 417800 | tf_op jit(solution)/shard_map/ppermute | solution.py:256
  171.4 8.7 %collective-permute-start.12 = (bf16[272,256]{1,0:T(8,128)(2,1)S(1)}, bf16[272,256]{1,0:T(8,128)(2,1)S(1)}, u32[]{:S(2)}, u32[]{:S(2)}) collective-permute-start(bf16[272,256]{1,0:T(8,128)(2,1)S(1)} %get-tuple-element.14), channel_id=1, source_target_pairs={{0,8},{4,12},{8,0},{12,4},{1,9},{5,13},{9,1},{13,5},{2,10},{6,14},... | collective-permute-start | bytes 417800 | tf_op jit(solution)/shard_map/ppermute | solution.py:256
  175.6 7.1 %collective-permute-start.11 = (bf16[272,256]{1,0:T(8,128)(2,1)S(1)}, bf16[272,256]{1,0:T(8,128)(2,1)S(1)}, u32[]{:S(2)}, u32[]{:S(2)}) collective-permute-start(bf16[272,256]{1,0:T(8,128)(2,1)S(1)} %get-tuple-element.13), channel_id=1, source_target_pairs={{0,12},{4,0},{8,4},{12,8},{1,13},{5,1},{9,5},{13,9},{2,14},{6,2},{... | collective-permute-start | bytes 417800 | tf_op jit(solution)/shard_map/ppermute | solution.py:256
